TPU v7x, 256 devices: a whole 4x4x8 slice. The times are simulated.
256 devices in a mesh: ep: 64 (over z, x, core), tp: 4 (over y).
Axes of the slice: x: 4, y: 4, z: 8, core: 2. Of those that a mesh axis runs over, the one named last changes fastest.
Arguments:
- receptance: bfloat16 [32768, 2048], P('ep', 'tp'), may hold values from -6 to 6
- key_rows: bfloat16 [32768, 2048], P('ep', 'tp'), may hold values from -6 to 6
- value_rows: bfloat16 [32768, 2048], P('ep', 'tp'), may hold values from -6 to 6
- decay_input: bfloat16 [32768, 2048], P('ep', 'tp'), may hold values from -2.796875 to 2.796875
- learn_input: bfloat16 [32768, 2048], P('ep', 'tp'), may hold values from -12 to 4
- decay_base: float32 [2048], P('tp'), may hold values from -20 to -2
- decay_shift: float32 [32768, 32], P('ep', 'tp'), may hold values from -1 to 20
- channel_gain: float32 [2048], P('tp'), may hold values from 0.1 to 1.9
- out_weight: bfloat16 [2048, 2048], P('tp'), may hold values from -0.125 to 0.125
- expert_input: bfloat16 [32768, 2048], P(('ep', 'tp')), may hold values from -6 to 6
- expert_gain: float32 [2048], replicated, may hold values from 0.1 to 1.9
- routes: int32 [32768, 2], P(('ep', 'tp')), may hold values from 0 to 63, all different within a row; in each aligned block of 128 rows (0 to 127, 128 to 255, ...) at most 8 rows name the same one
- route_weight: float32 [32768, 2], P(('ep', 'tp')), may hold values from 0.1 to 1
- gate_weight: bfloat16 [64, 2048, 1024], P('ep', None, 'tp'), may hold values from -0.125 to 0.125
- up_weight: bfloat16 [64, 2048, 1024], P('ep', None, 'tp'), may hold values from -0.125 to 0.125
- down_weight: bfloat16 [64, 1024, 2048], P('ep', 'tp'), may hold values from -0.1875 to 0.1875
Outputs:
- mixer_out: bfloat16 [32768, 2048], P(('ep', 'tp'))
- expert_out: bfloat16 [32768, 2048], P(('ep', 'tp'))
Inputs may be any that keep to these rules, and one draw needn't show every extreme that they name: `routes`: within the rows of one device (aligned blocks of 128 rows) no expert is named by more than 8 rows, and in every draw some block names some expert exactly 8 times. Each row names 2 different experts.
All inputs are finite; a program needn't handle non-finite values.
Results may differ from a plain program's by a relative error of at most 0.024.
Values may be sent and summed in bfloat16 or wider, within the bound.
No kernel may reach another device: no remote copies, remote signals or barrier semaphores. Data moves between devices by JAX's collectives and lax.ppermute only.
A program may use at most 128 MiB of HBM per device.

v0:
```python
import jax
import jax.numpy as jnp
from jax import lax
from jax.experimental import pallas as pl
from jax.experimental.pallas import tpu as pltpu
from jax.sharding import Mesh
from jax.sharding import PartitionSpec as P


SPAN = 128
EP = ("ep_0", "ep_1", "ep_2")
GROUP = ("ep_1", "ep_2")
EP_TP = ("ep_0", "ep_1", "ep_2", "tp")
GROUPS = 8
HEAD = 64
PAIR = 128
MSG_ROWS = 80
CAPACITY = 8

NORM_EPS = 1e-06
GROUP_EPS = 0.00064
KEY_EPS = 1e-06
DECAY_SCALE = 0.6065306597126334

F32 = jnp.float32
BF16 = jnp.bfloat16


def dot(a, b):
    return lax.dot_general(a, b, (((1,), (0,)), ((), ())), preferred_element_type=F32)


def dot_nt(a, b):
    return lax.dot_general(a, b, (((1,), (1,)), ((), ())), preferred_element_type=F32)


def dot_tn(a, b):
    return lax.dot_general(a, b, (((0,), (0,)), ((), ())), preferred_element_type=F32)


def two_parts(x):
    high = x.astype(BF16)
    return high, (x - high.astype(F32)).astype(BF16)


def iota(shape, dim):
    return lax.broadcasted_iota(jnp.int32, shape, dim)


def block_ones():
    rows, cols = iota((PAIR, PAIR), 0), iota((PAIR, PAIR), 1)
    return (rows // HEAD) == (cols // HEAD)


def unit_lower_inverses(parts):
    size = parts[0].shape[0]
    rows, cols = iota((size, size), 0), iota((size, size), 1)
    eye = (rows == cols).astype(F32)
    start = 16
    inside = (rows // start) == (cols // start)
    powers = [jnp.where(inside, -a, 0.0) for a in parts]
    inverses = [eye + p for p in powers]
    reach = 2
    while reach < start:
        narrow = [p.astype(BF16) for p in powers]
        powers = [dot(p, p) for p in narrow]
        inverses = [
            inv + dot(inv.astype(BF16), p.astype(BF16))
            for inv, p in zip(inverses, powers)
        ]
        reach *= 2
    block = start
    while block < size:
        joined = ((rows // (2 * block)) == (cols // (2 * block))) & (
            (rows // block) != (cols // block)
        )
        narrow = [inv.astype(BF16) for inv in inverses]
        corners = [jnp.where(joined, a, 0.0).astype(BF16) for a in parts]
        moved = [dot(c, inv).astype(BF16) for c, inv in zip(corners, narrow)]
        inverses = [
            inv - dot(short, m) for inv, short, m in zip(inverses, narrow, moved)
        ]
        block *= 2
    return inverses


def summary_kernel(
    q_ref, k_ref, v_ref, di_ref, li_ref, base_ref, shift_ref,
    reader_ref, local_ref, gather_ref, add_ref, fade_ref, msg_ref,
    maps_ref, total_ref,
):
    step = pl.program_id(0)
    rows, channels = q_ref.shape
    heads = shift_ref.shape[1]
    pairs = heads // 2
    same = block_ones()
    same_f = same.astype(F32)
    same_b = same_f.astype(BF16)
    row2, col2 = iota((PAIR, PAIR), 0), iota((PAIR, PAIR), 1)
    eye = (row2 == col2).astype(F32)

    @pl.when(step == 0)
    def _():
        for p in range(pairs):
            maps_ref[p, :PAIR, :] = eye
            maps_ref[p, PAIR:, :] = jnp.zeros((PAIR, PAIR), F32)
        total_ref[...] = jnp.ones_like(total_ref)

    spread = (
        (iota((heads, channels), 1) // HEAD) == iota((heads, channels), 0)
    ).astype(F32).astype(BF16)
    shift_high, shift_low = two_parts(shift_ref[...])
    pre = (
        di_ref[...].astype(F32)
        + base_ref[...]
        + (dot(shift_high, spread) + dot(shift_low, spread))
    )
    log_decay = -DECAY_SCALE / (1.0 + jnp.exp(-pre))
    tri_rows, tri_cols = iota((rows, rows), 0), iota((rows, rows), 1)
    inclusive = tri_rows >= tri_cols
    strict = tri_rows > tri_cols
    tri = inclusive.astype(F32).astype(BF16)
    decay_high, decay_low = two_parts(log_decay)
    cum = dot(tri, decay_high) + dot(tri, decay_low)
    middle = cum[rows // 2 - 1 : rows // 2, :]
    ending = cum[rows - 1 : rows, :]
    grow = jnp.exp(cum - middle)
    grow_before = grow * jnp.exp(-log_decay)
    shrink = jnp.exp(middle - cum)
    from_start = jnp.exp(middle)
    to_end = jnp.exp(ending - middle)
    fade = jnp.exp(ending)
    fade_ref[0] = fade

    keys = k_ref[...].astype(F32)
    recept = q_ref[...].astype(F32)
    squares_high, squares_low = two_parts(keys * keys)
    lengths = jnp.concatenate(
        [
            dot(squares_high[:, p * PAIR : (p + 1) * PAIR], same_b)
            + dot(squares_low[:, p * PAIR : (p + 1) * PAIR], same_b)
            for p in range(pairs)
        ],
        axis=1,
    )
    unit = keys * lax.rsqrt(lengths + KEY_EPS)
    removal = unit / (1.0 + jnp.exp(-li_ref[...].astype(F32)))

    probes_f = unit * grow_before
    queries_f = recept * grow
    back_removal_f = removal * shrink
    back_keys_f = keys * shrink
    probes = probes_f.astype(BF16)
    queries = queries_f.astype(BF16)
    back_removal = back_removal_f.astype(BF16)
    back_keys = back_keys_f.astype(BF16)
    carried_in = (probes_f * from_start).astype(BF16)
    read_in = queries_f * from_start
    tail_removal = (back_removal_f * to_end).astype(BF16)
    tail_keys = (back_keys_f * to_end).astype(BF16)
    values = v_ref[...]

    first = iota((rows, PAIR), 1) < HEAD
    none = jnp.zeros((rows, PAIR), BF16)

    def left(x):
        return jnp.where(first, x, none)

    def right(x):
        return jnp.where(first, none, x)

    kept = []
    strict_parts = []
    for p in range(pairs):
        lanes = slice(p * PAIR, (p + 1) * PAIR)
        pr, qu = probes[:, lanes], queries[:, lanes]
        outer = jnp.concatenate([left(pr), right(pr), left(qu), right(qu)], axis=0)
        inner = jnp.concatenate([back_removal[:, lanes], back_keys[:, lanes]], axis=0)
        products = dot_nt(outer, inner)
        strict_parts.append(jnp.where(strict, products[0:rows, 0:rows], 0.0))
        strict_parts.append(jnp.where(strict, products[rows : 2 * rows, 0:rows], 0.0))
        pair_keys = jnp.concatenate(
            [
                jnp.where(strict, products[0:rows, rows:], 0.0),
                jnp.where(strict, products[rows : 2 * rows, rows:], 0.0),
            ],
            axis=1,
        ).astype(BF16)
        read_keys = jnp.concatenate(
            [
                jnp.where(inclusive, products[2 * rows : 3 * rows, rows:], 0.0),
                jnp.where(inclusive, products[3 * rows :, rows:], 0.0),
            ],
            axis=1,
        ).astype(BF16)
        read_removal = jnp.concatenate(
            [
                jnp.where(inclusive, products[2 * rows : 3 * rows, 0:rows], 0.0),
                jnp.where(inclusive, products[3 * rows :, 0:rows], 0.0),
            ],
            axis=1,
        ).astype(BF16)
        va = values[:, lanes]
        stacked = jnp.concatenate([left(va), right(va)], axis=0)
        sums = dot(jnp.concatenate([pair_keys, read_keys], axis=0), stacked)
        kept.append((read_removal, sums))

    inverses = unit_lower_inverses(strict_parts)

    for p in range(pairs):
        lanes = slice(p * PAIR, (p + 1) * PAIR)
        read_removal, sums = kept[p]
        weights = sums[:rows].astype(BF16)
        carry = carried_in[:, lanes]
        sides = jnp.concatenate(
            [
                jnp.concatenate([left(carry), left(weights)], axis=1),
                jnp.concatenate([right(carry), right(weights)], axis=1),
            ],
            axis=0,
        )
        inverse = jnp.concatenate([inverses[2 * p], inverses[2 * p + 1]], axis=1)
        solved = dot(inverse.astype(BF16), sides).astype(BF16)
        carried, local = solved[:, :PAIR], solved[:, PAIR:]
        halves = jnp.concatenate(
            [
                jnp.concatenate([left(carried), left(local)], axis=1),
                jnp.concatenate([right(carried), right(local)], axis=1),
            ],
            axis=0,
        )
        taken = dot(read_removal, halves)
        reader_ref[:, lanes] = (read_in[:, lanes] - taken[:, :PAIR]).astype(BF16)
        local_ref[:, lanes] = sums[rows:] - taken[:, PAIR:]
        ends = dot_tn(solved, tail_removal[:, lanes])
        gathered = jnp.where(same, ends[:PAIR], 0.0).astype(BF16)
        added = jnp.where(
            same, dot_tn(values[:, lanes], tail_keys[:, lanes]) - ends[PAIR:], 0.0
        )
        gather_ref[0, p] = gathered
        add_ref[0, p] = added
        maps = maps_ref[p]
        maps = maps * fade[:, lanes] - dot(maps.astype(BF16), gathered)
        maps_ref[p, :PAIR, :] = maps[:PAIR]
        maps_ref[p, PAIR:, :] = maps[PAIR:] + added
    total_ref[...] = total_ref[...] * fade

    @pl.when(step == pl.num_programs(0) - 1)
    def _():
        low = iota((PAIR, PAIR), 1) < HEAD
        low_row = iota((1, PAIR), 1) < HEAD
        for p in range(pairs):
            lanes = slice(p * PAIR, (p + 1) * PAIR)
            total = total_ref[:, lanes]
            lost = eye * total - maps_ref[p, :PAIR, :]
            gained = maps_ref[p, PAIR:, :]
            lost = lost + pltpu.roll(lost, HEAD, 1)
            gained = gained + pltpu.roll(gained, HEAD, 1)
            both = jnp.where(low, lost, gained).astype(BF16)
            msg_ref[2 * p, :HEAD, :] = both[:HEAD]
            msg_ref[2 * p + 1, :HEAD, :] = both[HEAD:]
            for side in range(2):
                own = jnp.where(low_row == (side == 0), total, 0.0)
                own = jnp.broadcast_to(own, (16, PAIR))
                own = own + pltpu.roll(own, HEAD, 1)
                high, rest = two_parts(own)
                msg_ref[2 * p + side, HEAD:, :] = jnp.where(
                    iota((16, PAIR), 1) < HEAD, high.astype(F32), rest.astype(F32)
                ).astype(BF16)


def message_parts(message):
    lost = message[:HEAD, :HEAD]
    gained = message[:HEAD, HEAD:].astype(F32)
    fades = message[HEAD : HEAD + 1, :].astype(F32)
    return lost, gained, fades[:, :HEAD] + fades[:, HEAD:]


def group_kernel(in_ref, prefix_ref, out_ref):
    rows, cols = iota((HEAD, HEAD), 0), iota((HEAD, HEAD), 1)
    eye = (rows == cols).astype(F32)
    maps = jnp.concatenate([eye, jnp.zeros((HEAD, HEAD), F32)], axis=0)
    total = jnp.ones((1, HEAD), F32)
    for m in range(in_ref.shape[0]):
        lost, gained, fade = message_parts(in_ref[m])
        prefix_ref[m] = maps
        moved = maps * fade - dot(maps.astype(BF16), lost)
        maps = jnp.concatenate([moved[:HEAD], moved[HEAD:] + gained], axis=0)
        total = total * fade
    both = jnp.concatenate([eye * total - maps[:HEAD], maps[HEAD:]], axis=1).astype(BF16)
    high, rest = two_parts(jnp.broadcast_to(total, (16, HEAD)))
    ends = jnp.concatenate([high.astype(F32), rest.astype(F32)], axis=1).astype(BF16)
    for z in range(out_ref.shape[0]):
        out_ref[z, :HEAD, :] = both
        out_ref[z, HEAD:, :] = ends


def enter_kernel(here_ref, in_ref, prefix_ref, out_ref):
    here = here_ref[0]
    state = jnp.zeros((HEAD, HEAD), F32)
    for z in range(in_ref.shape[0]):
        lost, gained, fade = message_parts(in_ref[z])
        passed = state * fade - dot(state.astype(BF16), lost) + gained
        state = jnp.where(z < here, passed, state)
    narrow = state.astype(BF16)
    for m in range(out_ref.shape[0]):
        entering = dot(narrow, prefix_ref[m, :HEAD, :].astype(BF16)) + prefix_ref[m, HEAD:, :]
        out_ref[m] = jnp.concatenate([entering, entering], axis=1).astype(BF16)


def readout_kernel(
    enter_ref, reader_ref, local_ref, gather_ref, add_ref, fade_ref, gain_ref, weight_ref,
    out_ref, state_ref,
):
    step = pl.program_id(0)
    channels = reader_ref.shape[1]
    pairs = channels // PAIR
    same = block_ones()
    means = jnp.where(same, 1.0 / HEAD, 0.0).astype(BF16)

    @pl.when(step == 0)
    def _():
        for p in range(pairs):
            entering = jnp.concatenate([enter_ref[2 * p], enter_ref[2 * p + 1]], axis=0)
            state_ref[p] = jnp.where(same, entering.astype(F32), 0.0)

    pieces = []
    for p in range(pairs):
        lanes = slice(p * PAIR, (p + 1) * PAIR)
        state = state_ref[p]
        narrow = state.astype(BF16)
        read = dot_nt(reader_ref[:, lanes], narrow) + local_ref[:, lanes]
        state_ref[p] = state * fade_ref[0, :, lanes] - dot(narrow, gather_ref[0, p]) + add_ref[0, p]
        centred = read - dot(read.astype(BF16), means)
        spread = dot((centred * centred).astype(BF16), means)
        pieces.append(
            (centred * lax.rsqrt(spread + GROUP_EPS) * gain_ref[:, lanes]).astype(BF16)
        )
    normed = jnp.concatenate(pieces, axis=1)
    out_ref[...] = dot(normed, weight_ref[...]).astype(BF16)


def hidden_kernel(x_ref, gate_ref, up_ref, out_ref):
    x = x_ref[...]
    gates = dot(x, gate_ref[...])
    uppers = dot(x, up_ref[...])
    out_ref[...] = (gates / (1.0 + jnp.exp(-gates)) * uppers).astype(BF16)


def down_kernel(h0, h1, h2, h3, own, top_r, low_r, top_l, low_l, top_f, low_f, out_ref):
    units = jnp.concatenate([h0[...], h1[...], h2[...], h3[...]], axis=1)
    weights = jnp.concatenate(
        [w[...] for w in (own, top_r, low_r, top_l, low_l, top_f, low_f)], axis=0
    )
    out_ref[...] = dot(units, weights).astype(BF16)


def pack_kernel(x_ref, gain_ref, routes_ref, mix_ref, out_ref, high_ref, rest_ref):
    tokens = x_ref.shape[0]
    places = out_ref.shape[0]
    x = x_ref[...].astype(F32)
    normed = (
        x * lax.rsqrt(jnp.mean(x * x, axis=1, keepdims=True) + NORM_EPS) * gain_ref[...]
    ).astype(BF16)
    experts = places // CAPACITY
    listed = iota((tokens, experts), 1)
    first, second = routes_ref[:, 0:1], routes_ref[:, 1:2]
    first_mark = (first == listed).astype(F32)
    second_mark = (second == listed).astype(F32)
    before = (iota((tokens, tokens), 0) > iota((tokens, tokens), 1)).astype(F32).astype(BF16)
    earlier = dot(before, (first_mark + second_mark).astype(BF16))
    columns = iota((tokens, places), 1)
    table = jnp.zeros((tokens, places), F32)
    mix = jnp.zeros((tokens, places), F32)
    for named, mark, weight in (
        (first, first_mark, mix_ref[:, 0:1]),
        (second, second_mark, mix_ref[:, 1:2]),
    ):
        slot = jnp.sum(earlier * mark, axis=1, keepdims=True).astype(jnp.int32)
        here = columns == named * CAPACITY + slot
        table = table + here.astype(F32)
        mix = jnp.where(here, weight, mix)
    out_ref[...] = dot_tn(table.astype(BF16), normed).astype(BF16)
    high, rest = two_parts(mix)
    high_ref[...] = high
    rest_ref[...] = rest


def combine_kernel(high_ref, rest_ref, rows_ref, out_ref):
    rows = rows_ref[...]
    out_ref[...] = (dot(high_ref[...], rows) + dot(rest_ref[...], rows)).astype(BF16)


def whole(shape):
    return pl.BlockSpec(shape, lambda *_: (0,) * len(shape))


def estimate(flops, moved, transcendentals=0):
    return pl.CostEstimate(
        flops=int(flops), bytes_accessed=int(moved), transcendentals=int(transcendentals)
    )


def summarize(q, k, v, di, li, base, shift):
    rows, channels = q.shape
    heads = shift.shape[1]
    pairs = heads // 2
    spans = rows // SPAN
    block = pl.BlockSpec((SPAN, channels), lambda i: (i, 0))
    square = (1, pairs, PAIR, PAIR)
    return pl.pallas_call(
        summary_kernel,
        grid=(spans,),
        in_specs=[block] * 5
        + [whole((1, channels)), pl.BlockSpec((SPAN, heads), lambda i: (i, 0))],
        out_specs=[
            block,
            block,
            pl.BlockSpec(square, lambda i: (i, 0, 0, 0)),
            pl.BlockSpec(square, lambda i: (i, 0, 0, 0)),
            pl.BlockSpec((1, 1, channels), lambda i: (i, 0, 0)),
            whole((heads, MSG_ROWS, PAIR)),
        ],
        out_shape=[
            jax.ShapeDtypeStruct((rows, channels), BF16),
            jax.ShapeDtypeStruct((rows, channels), F32),
            jax.ShapeDtypeStruct((spans, pairs, PAIR, PAIR), BF16),
            jax.ShapeDtypeStruct((spans, pairs, PAIR, PAIR), F32),
            jax.ShapeDtypeStruct((spans, 1, channels), F32),
            jax.ShapeDtypeStruct((heads, MSG_ROWS, PAIR), BF16),
        ],
        scratch_shapes=[
            pltpu.VMEM((pairs, 2 * PAIR, PAIR), F32),
            pltpu.VMEM((1, channels), F32),
        ],
        compiler_params=pltpu.CompilerParams(dimension_semantics=("arbitrary",)),
        cost_estimate=estimate(2.0e10, 6 << 20, 2 << 20),
        name="summary",
    )(q, k, v, di, li, base, shift)


def group_scan(messages):
    count = messages.shape[0]
    return pl.pallas_call(
        group_kernel,
        out_shape=[
            jax.ShapeDtypeStruct((count, 2 * HEAD, HEAD), F32),
            jax.ShapeDtypeStruct((GROUPS, MSG_ROWS, PAIR), BF16),
        ],
        cost_estimate=estimate(2.0e9, 1 << 20),
        name="group_scan",
    )(messages)


def enter_states(here, totals, prefixes):
    return pl.pallas_call(
        enter_kernel,
        in_specs=[
            pl.BlockSpec(memory_space=pltpu.SMEM),
            pl.BlockSpec(memory_space=pltpu.VMEM),
            pl.BlockSpec(memory_space=pltpu.VMEM),
        ],
        out_shape=jax.ShapeDtypeStruct((prefixes.shape[0], HEAD, PAIR), BF16),
        cost_estimate=estimate(2.0e9, 1 << 20),
        name="enter_states",
    )(here, totals, prefixes)


def read_and_project(entering, reader, local, gather, add, fade, gain, weight):
    rows, channels = reader.shape
    pairs = channels // PAIR
    spans = rows // SPAN
    width = weight.shape[1]
    block = pl.BlockSpec((SPAN, channels), lambda i: (i, 0))
    square = pl.BlockSpec((1, pairs, PAIR, PAIR), lambda i: (i, 0, 0, 0))
    return pl.pallas_call(
        readout_kernel,
        grid=(spans,),
        in_specs=[
            whole(entering.shape),
            block,
            block,
            square,
            square,
            pl.BlockSpec((1, 1, channels), lambda i: (i, 0, 0)),
            whole((1, channels)),
            whole(weight.shape),
        ],
        out_specs=pl.BlockSpec((SPAN, width), lambda i: (i, 0)),
        out_shape=jax.ShapeDtypeStruct((rows, width), BF16),
        scratch_shapes=[pltpu.VMEM((pairs, PAIR, PAIR), F32)],
        compiler_params=pltpu.CompilerParams(dimension_semantics=("arbitrary",)),
        cost_estimate=estimate(5.0e9, 8 << 20),
        name="readout",
    )(entering, reader, local, gather, add, fade, gain, weight)


def expert_hidden(x, gate, up):
    rows, width = x.shape
    units = gate.shape[1]
    tile = rows // 2
    return pl.pallas_call(
        hidden_kernel,
        grid=(2,),
        in_specs=[
            pl.BlockSpec((tile, width), lambda i: (i, 0)),
            whole(gate.shape),
            whole(up.shape),
        ],
        out_specs=pl.BlockSpec((tile, units), lambda i: (i, 0)),
        out_shape=jax.ShapeDtypeStruct((rows, units), BF16),
        compiler_params=pltpu.CompilerParams(dimension_semantics=("arbitrary",)),
        cost_estimate=estimate(4 * rows * width * units, 5 << 20, rows * units),
        name="hidden",
    )(x, gate, up)


def expert_down(hiddens, weights):
    rows = hiddens[0].shape[0]
    width = weights[0].shape[1]
    tile = width // 4
    return pl.pallas_call(
        down_kernel,
        grid=(4,),
        in_specs=[whole(h.shape) for h in hiddens]
        + [pl.BlockSpec((w.shape[0], tile), lambda i: (0, i)) for w in weights],
        out_specs=pl.BlockSpec((rows, tile), lambda i: (0, i)),
        out_shape=jax.ShapeDtypeStruct((rows, width), BF16),
        compiler_params=pltpu.CompilerParams(dimension_semantics=("arbitrary",)),
        cost_estimate=estimate(8 * rows * 256 * width, 7 << 20),
        name="down",
    )(*hiddens, *weights)


def pack_rows(x, gain, routes, mix, places):
    tokens, width = x.shape
    return pl.pallas_call(
        pack_kernel,
        out_shape=[
            jax.ShapeDtypeStruct((places, width), BF16),
            jax.ShapeDtypeStruct((tokens, places), BF16),
            jax.ShapeDtypeStruct((tokens, places), BF16),
        ],
        cost_estimate=estimate(2.0e9, 3 << 20),
        name="pack",
    )(x, gain, routes, mix)


def combine_rows(high, rest, rows):
    tokens, places = high.shape
    width = rows.shape[1]
    tile = width // 4
    return pl.pallas_call(
        combine_kernel,
        grid=(4,),
        in_specs=[
            whole(high.shape),
            whole(rest.shape),
            pl.BlockSpec((places, tile), lambda i: (0, i)),
        ],
        out_specs=pl.BlockSpec((tokens, tile), lambda i: (0, i)),
        out_shape=jax.ShapeDtypeStruct((tokens, width), BF16),
        compiler_params=pltpu.CompilerParams(dimension_semantics=("arbitrary",)),
        cost_estimate=estimate(1.0e9, 3 << 20),
        name="combine",
    )(high, rest, rows)


def ring(x, shift):
    count = lax.axis_size("tp")
    return lax.ppermute(x, "tp", [(i, (i + shift) % count) for i in range(count)])


def exchange(x, axis):
    return lax.all_to_all(x, axis, 0, 0, tiled=True)


def on_device(
    receptance,
    key_rows,
    value_rows,
    decay_input,
    learn_input,
    decay_base,
    decay_shift,
    channel_gain,
    out_weight,
    expert_input,
    expert_gain,
    routes,
    route_weight,
    gate_weight,
    up_weight,
    down_weight,
):
    ep_count = lax.axis_size(EP)
    token_rows, model_width = expert_input.shape
    experts = gate_weight.shape[0] * ep_count
    places = experts * CAPACITY

    w_gate = gate_weight[0]
    w_up = up_weight[0]
    w_down = down_weight[0]
    cut = w_down.shape[0] // 2
    down_top, down_low = w_down[:cut], w_down[cut:]
    gate_r, up_l = ring(w_gate, 1), ring(w_up, -1)
    gate_l, up_r = ring(w_gate, -1), ring(w_up, 1)
    top_r, low_l = ring(down_top, 1), ring(down_low, -1)
    low_r, top_l = ring(down_low, 1), ring(down_top, -1)
    gate_f, up_f = ring(gate_r, 1), ring(up_l, -1)
    top_f, low_f = ring(top_r, 1), ring(low_l, -1)

    outgoing, high, rest = pack_rows(
        expert_input, expert_gain.reshape(1, -1), routes, route_weight, places
    )
    arrived = exchange(
        outgoing.reshape(experts, CAPACITY, model_width), EP
    ).reshape(places, model_width)

    reader, local, gather, add, fade, messages = summarize(
        receptance,
        key_rows,
        value_rows,
        decay_input,
        learn_input,
        decay_base.reshape(1, -1),
        decay_shift,
    )
    prefixes, totals = group_scan(exchange(messages, GROUP))
    entered = enter_states(
        lax.axis_index("ep_0").astype(jnp.int32).reshape(1),
        exchange(totals, "ep_0"),
        prefixes,
    )
    partial = read_and_project(
        exchange(entered, GROUP),
        reader,
        local,
        gather,
        add,
        fade,
        channel_gain.reshape(1, -1),
        out_weight,
    )
    tp_count = lax.axis_size("tp")
    shares = exchange(partial.reshape(tp_count, token_rows, model_width), "tp")
    mixer_out = jnp.sum(shares.astype(F32), axis=0).astype(BF16)

    hiddens = []
    for g, u in ((w_gate, w_up), (gate_r, up_r), (gate_l, up_l), (gate_f, up_f)):
        hiddens.append(expert_hidden(arrived, g, u))
    returning = expert_down(hiddens, [w_down, top_r, low_r, top_l, low_l, top_f, low_f])
    returned = exchange(returning.reshape(ep_count, CAPACITY, model_width), EP)
    combined = combine_rows(high, rest, returned.reshape(places, model_width))
    return (mixer_out, combined)


def solution(mesh):
    finer = Mesh(mesh.devices.reshape(8, 4, 2, mesh.shape["tp"]), ("ep_0", "ep_1", "ep_2", "tp"))
    placed = (
        P(EP, "tp"),
        P(EP, "tp"),
        P(EP, "tp"),
        P(EP, "tp"),
        P(EP, "tp"),
        P("tp"),
        P(EP, "tp"),
        P("tp"),
        P("tp", None),
        P(EP_TP, None),
        P(),
        P(EP_TP, None),
        P(EP_TP, None),
        P(EP, None, "tp"),
        P(EP, None, "tp"),
        P(EP, "tp", None),
    )

    return jax.shard_map(
        on_device,
        mesh=finer,
        in_specs=placed,
        out_specs=(P(EP_TP, None), P(EP_TP, None)),
        check_vma=False,
    )
```

profile of v0, /device:TPU:2, one launch (start us, length us, event | category | flops | bytes accessed | tf_op | source)
XLA Modules:
  0.0 283.0 jit_solution(5122858556161096515)
XLA Ops:
  2.2 19.3 %summary.1 = (bf16[512,512]{1,0:T(8,128)(2,1)}, f32[512,512]{1,0:T(8,128)}, bf16[4,4,128,128]{3,2,1,0:T(8,128)(2,1)}, f32[4,4,128,128]{3,2,1,0:T(8,128)}, f32[4,...) custom-call(bf16[512,512]{1,0:T(8,128)(2,1)} %q_ref.1, bf16[512,512]{1,0:T(8,128)(2,1)} %k_ref.1, bf16[512,512]{1,0:T(8,128)(2,1)} %v_ref.1, ...), custom_call_target="tpu_custom_call" | custom-call | flops 20000000000 | bytes 6291456 | tf_op jit(solution)/shard_map/summary/pallas_call | solution.py:411
  21.5 11.3 %all_to_all.30.in_ref = bf16[8,80,128]{2,1,0:T(8,128)(2,1)} all-to-all(bf16[8,80,128]{2,1,0:T(8,128)(2,1)} %get-tuple-element.13), channel_id=1, replica_groups=mesh['ep_0'=8,'ep_1'=4,'ep_2'=2,'tp'=4] {'ep_1','ep_2'}, dimensions={0} | all-to-all | bytes 327680 | tf_op jit(solution)/shard_map/all_to_all | solution.py:575
  35.4 7.1 %all-to-all-start.1 = ((bf16[8,80,128]{2,1,0:T(8,128)(2,1)}), bf16[8,80,128]{2,1,0:T(8,128)(2,1)S(1)}, u32[]{:S(2)}, u32[]{:S(2)}) async-start(bf16[8,80,128]{2,1,0:T(8,128)(2,1)} %get-tuple-element.14), calls=%async_computation.1 | async-start | bytes 327680 | tf_op jit(solution)/shard_map/all_to_all | solution.py:575
  44.0 8.1 %all-to-all-done.1.in_ref = bf16[8,80,128]{2,1,0:T(8,128)(2,1)S(1)} async-done(((bf16[8,80,128]{2,1,0:T(8,128)(2,1)}), bf16[8,80,128]{2,1,0:T(8,128)(2,1)S(1)}, u32[]{:S(2)}, u32[]{:S(2)}) %all-to-all-start.1) | async-done | bytes 163872 | tf_op jit(solution)/shard_map/all_to_all | solution.py:575
  52.8 3.0 %enter_states.1 = bf16[8,64,128]{2,1,0:T(8,128)(2,1)} custom-call(s32[1]{0:T(128)} %bitcast.here_ref, bf16[8,80,128]{2,1,0:T(8,128)(2,1)} %copy-done.4, f32[8,128,64]{2,1,0:T(8,128)} %get-tuple-element.15.prefix_ref), custom_call_target="tpu_custom_call" | custom-call | flops 2000000000 | bytes 1048576 | tf_op jit(solution)/shard_map/enter_states/pallas_call | solution.py:456
  55.7 4.7 %all-to-all-start.2 = ((bf16[8,64,128]{2,1,0:T(8,128)(2,1)}), bf16[8,64,128]{2,1,0:T(8,128)(2,1)S(1)}, u32[]{:S(2)}, u32[]{:S(2)}) async-start(bf16[8,64,128]{2,1,0:T(8,128)(2,1)} %enter_states.1), calls=%async_computation.2 | async-start | bytes 262144 | tf_op jit(solution)/shard_map/all_to_all | solution.py:575
  60.5 3.6 %pack.1 = (bf16[512,2048]{1,0:T(8,128)(2,1)}, bf16[128,512]{1,0:T(8,128)(2,1)}, bf16[128,512]{1,0:T(8,128)(2,1)}) custom-call(bf16[128,2048]{1,0:T(8,128)(2,1)} %x_ref.1, f32[1,2048]{1,0:T(1,128)} %bitcast.31, s32[128,2]{1,0:T(8,128)} %copy.19.routes_ref, f32[128,2]{1,0:T(8,128)} %copy.20.mix_ref), custom_call_target="tpu_custom_call" | custom-call | flops 2000000000 | bytes 3145728 | tf_op jit(solution)/shard_map/pack/pallas_call | solution.py:537
  65.8 5.6 %all-to-all-start.4 = ((bf16[64,8,2048]{2,1,0:T(8,128)(2,1)}), bf16[64,8,2048]{2,1,0:T(8,128)(2,1)S(1)}, u32[]{:S(2)}, u32[]{:S(2)}) async-start(bf16[64,8,2048]{2,1,0:T(8,128)(2,1)} %bitcast.21), calls=%async_computation.4 | async-start | bytes 4194304 | tf_op jit(solution)/shard_map/all_to_all | solution.py:575
  80.3 18.5 %collective-permute-done.gate_ref = bf16[2048,256]{1,0:T(8,128)(2,1)} collective-permute-done((bf16[2048,256]{1,0:T(8,128)(2,1)S(1)}, bf16[2048,256]{1,0:T(8,128)(2,1)}, u32[]{:S(2)}, u32[]{:S(2)}) %collective-permute-start) | collective-permute-done | bytes 1048608 | tf_op jit(solution)/shard_map/ppermute | solution.py:571
  99.2 8.1 %readout.1 = bf16[512,2048]{1,0:T(8,128)(2,1)} custom-call(bf16[8,64,128]{2,1,0:T(8,128)(2,1)} %copy-done.5, bf16[512,512]{1,0:T(8,128)(2,1)} %get-tuple-element.16.reader_ref, f32[512,512]{1,0:T(8,128)} %get-tuple-element.17.local_ref, bf16[4,4,128,128]{3,2,1,0:T(8,128)(2,1)} %get-tuple-element.18.gather_ref, f32[4,4,128,128]{3,2,1,0:T(8,128)} %get-tuple-element.19.add_ref, ...), custom_call_target="tpu_custom_call" | custom-call | flops 5000000000 | bytes 8388608 | tf_op jit(solution)/shard_map/readout/pallas_call | solution.py:476
  107.3 15.5 %all-to-all-done.4 = bf16[64,8,2048]{2,1,0:T(8,128)(2,1)S(1)} async-done(((bf16[64,8,2048]{2,1,0:T(8,128)(2,1)}), bf16[64,8,2048]{2,1,0:T(8,128)(2,1)S(1)}, u32[]{:S(2)}, u32[]{:S(2)}) %all-to-all-start.4) | async-done | bytes 2097184 | tf_op jit(solution)/shard_map/all_to_all | solution.py:575
  124.1 4.5 %all-to-all-start.3 = ((bf16[4,128,2048]{2,1,0:T(8,128)(2,1)}), bf16[4,128,2048]{2,1,0:T(8,128)(2,1)}, u32[]{:S(2)}, u32[]{:S(2)}) async-start(bf16[4,128,2048]{2,1,0:T(8,128)(2,1)} %bitcast.20), calls=%async_computation.3 | async-start | bytes 4194304 | tf_op jit(solution)/shard_map/all_to_all | solution.py:575
  128.6 3.2 %collective-permute-start.5 = (bf16[2048,256]{1,0:T(8,128)(2,1)}, bf16[2048,256]{1,0:T(8,128)(2,1)S(1)}, u32[]{:S(2)}, u32[]{:S(2)}) collective-permute-start(bf16[2048,256]{1,0:T(8,128)(2,1)} %collective-permute-done.3.up_ref), channel_id=1, source_target_pairs={{0,3},{1,0},{2,1},{3,2},{4,7},{5,4},{6,5},{7,6},{8,11},{9,8},{10,9... | collective-permute-start | bytes 3145736 | tf_op jit(solution)/shard_map/ppermute | solution.py:571
  134.4 51.5 %collective-permute-done.9.low_l = bf16[128,2048]{1,0:T(8,128)(2,1)S(1)} collective-permute-done((bf16[128,2048]{1,0:T(8,128)(2,1)}, bf16[128,2048]{1,0:T(8,128)(2,1)S(1)}, u32[]{:S(2)}, u32[]{:S(2)}) %collective-permute-start.9) | collective-permute-done | bytes 524320 | tf_op jit(solution)/shard_map/ppermute | solution.py:571
  189.3 3.0 %collective-permute-start.11 = (bf16[128,2048]{1,0:T(8,128)(2,1)S(1)}, bf16[128,2048]{1,0:T(8,128)(2,1)S(1)}, u32[]{:S(2)}, u32[]{:S(2)}) collective-permute-start(bf16[128,2048]{1,0:T(8,128)(2,1)S(1)} %collective-permute-done.9.low_l), channel_id=1, source_target_pairs={{0,3},{1,0},{2,1},{3,2},{4,7},{5,4},{6,5},{7,6},{8,11},{9,8},{10,9... | collective-permute-start | bytes 1572872 | tf_op jit(solution)/shard_map/ppermute | solution.py:571
  192.3 4.0 %hidden.4.h0 = bf16[512,256]{1,0:T(8,128)(2,1)} custom-call(bf16[512,2048]{1,0:T(8,128)(2,1)} %bitcast.16, bf16[2048,256]{1,0:T(8,128)(2,1)} %bitcast.24, bf16[2048,256]{1,0:T(8,128)(2,1)} %bitcast.29), custom_call_target="tpu_custom_call" | custom-call | flops 1073741824 | bytes 5242880 | tf_op jit(solution)/shard_map/hidden/pallas_call | solution.py:502
  196.3 4.0 %hidden.5.h1 = bf16[512,256]{1,0:T(8,128)(2,1)} custom-call(bf16[512,2048]{1,0:T(8,128)(2,1)} %bitcast.17, bf16[2048,256]{1,0:T(8,128)(2,1)} %collective-permute-done.gate_ref, bf16[2048,256]{1,0:T(8,128)(2,1)} %collective-permute-done.1.up_ref), custom_call_target="tpu_custom_call" | custom-call | flops 1073741824 | bytes 5242880 | tf_op jit(solution)/shard_map/hidden/pallas_call | solution.py:502
  200.3 4.0 %hidden.6.h2 = bf16[512,256]{1,0:T(8,128)(2,1)} custom-call(bf16[512,2048]{1,0:T(8,128)(2,1)} %bitcast.18, bf16[2048,256]{1,0:T(8,128)(2,1)} %collective-permute-done.2.gate_ref, bf16[2048,256]{1,0:T(8,128)(2,1)} %collective-permute-done.3.up_ref), custom_call_target="tpu_custom_call" | custom-call | flops 1073741824 | bytes 5242880 | tf_op jit(solution)/shard_map/hidden/pallas_call | solution.py:502
  205.2 4.0 %hidden.7.h3 = bf16[512,256]{1,0:T(8,128)(2,1)} custom-call(bf16[512,2048]{1,0:T(8,128)(2,1)} %bitcast.19, bf16[2048,256]{1,0:T(8,128)(2,1)} %collective-permute-done.4.gate_ref, bf16[2048,256]{1,0:T(8,128)(2,1)} %copy-done.3), custom_call_target="tpu_custom_call" | custom-call | flops 1073741824 | bytes 5242880 | tf_op jit(solution)/shard_map/hidden/pallas_call | solution.py:502
  210.6 6.2 %down.1 = bf16[512,2048]{1,0:T(8,128)(2,1)} custom-call(bf16[512,256]{1,0:T(8,128)(2,1)} %hidden.4.h0, bf16[512,256]{1,0:T(8,128)(2,1)} %hidden.5.h1, bf16[512,256]{1,0:T(8,128)(2,1)} %hidden.6.h2, bf16[512,256]{1,0:T(8,128)(2,1)} %hidden.7.h3, bf16[256,2048]{1,0:T(8,128)(2,1)} %bitcast.30, bf16[128,2048]{1,0:T(8,128)(2,1)} %collective-permute-done.6.top_r, ...), custom_call_target="tpu_custom_call" | custom-call | flops 2147483648 | bytes 7340032 | tf_op jit(solution)/shard_map/down/pallas_call | solution.py:522
  216.9 9.4 %all-to-all-start.5 = ((bf16[64,8,2048]{2,1,0:T(8,128)(2,1)}), bf16[64,8,2048]{2,1,0:T(8,128)(2,1)S(1)}, u32[]{:S(2)}, u32[]{:S(2)}) async-start(bf16[64,8,2048]{2,1,0:T(8,128)(2,1)} %bitcast.22), calls=%async_computation.5 | async-start | bytes 4194304 | tf_op jit(solution)/shard_map/all_to_all | solution.py:575
  226.3 2.9 %reduce_sum.12 = bf16[128,2048]{1,0:T(8,128)(2,1)} reduce(bf16[4,128,2048]{2,1,0:T(8,128)(2,1)} %all-to-all-done.3, bf16[]{:T(256)} %constant.8.clone.1), dimensions={0}, to_apply=%region_0.0 | reduce | flops 786432 | bytes 2621442 | tf_op jit(solution)/shard_map/reduce_sum | solution.py:647
  229.2 48.3 %all-to-all-done.5 = bf16[64,8,2048]{2,1,0:T(8,128)(2,1)S(1)} async-done(((bf16[64,8,2048]{2,1,0:T(8,128)(2,1)}), bf16[64,8,2048]{2,1,0:T(8,128)(2,1)S(1)}, u32[]{:S(2)}, u32[]{:S(2)}) %all-to-all-start.5) | async-done | bytes 2097184 | tf_op jit(solution)/shard_map/all_to_all | solution.py:575
  278.9 4.1 %combine.1 = bf16[128,2048]{1,0:T(8,128)(2,1)} custom-call(bf16[128,512]{1,0:T(8,128)(2,1)} %get-tuple-element.21.high_ref, bf16[128,512]{1,0:T(8,128)(2,1)} %get-tuple-element.22.rest_ref, bf16[512,2048]{1,0:T(8,128)(2,1)} %bitcast.23), custom_call_target="tpu_custom_call" | custom-call | flops 1000000000 | bytes 3145728 | tf_op jit(solution)/shard_map/combine/pallas_call | solution.py:553
  (51 shorter events, 28.4 us)
Async XLA Ops:
  32.8 9.8 %copy-start.6 = (s32[128,2]{0,1:T(2,128)S(1)}, s32[128,2]{0,1:T(2,128)}, u32[]{:S(2)}) copy-start(s32[128,2]{0,1:T(2,128)} %param.27) | copy-start | bytes 3076
  32.8 10.5 %copy-start.7 = (f32[128,2]{0,1:T(2,128)S(1)}, f32[128,2]{0,1:T(2,128)}, u32[]{:S(2)}) copy-start(f32[128,2]{0,1:T(2,128)} %param.28) | copy-start | bytes 3076
  35.4 16.7 %all-to-all-start.1 = ((bf16[8,80,128]{2,1,0:T(8,128)(2,1)}), bf16[8,80,128]{2,1,0:T(8,128)(2,1)S(1)}, u32[]{:S(2)}, u32[]{:S(2)}) async-start(bf16[8,80,128]{2,1,0:T(8,128)(2,1)} %get-tuple-element.14), calls=%async_computation.1 | async-start | bytes 327680 | tf_op jit(solution)/shard_map/all_to_all | solution.py:575
  55.7 9.4 %all-to-all-start.2 = ((bf16[8,64,128]{2,1,0:T(8,128)(2,1)}), bf16[8,64,128]{2,1,0:T(8,128)(2,1)S(1)}, u32[]{:S(2)}, u32[]{:S(2)}) async-start(bf16[8,64,128]{2,1,0:T(8,128)(2,1)} %enter_states.1), calls=%async_computation.2 | async-start | bytes 262144 | tf_op jit(solution)/shard_map/all_to_all | solution.py:575
  65.2 6.2 %copy-start.2 = (bf16[1,2048,256]{2,1,0:T(8,128)(2,1)S(1)}, bf16[1,2048,256]{2,1,0:T(8,128)(2,1)}, u32[]{:S(2)}) copy-start(bf16[1,2048,256]{2,1,0:T(8,128)(2,1)} %param.29) | copy-start | bytes 3145732
  65.8 56.9 %all-to-all-start.4 = ((bf16[64,8,2048]{2,1,0:T(8,128)(2,1)}), bf16[64,8,2048]{2,1,0:T(8,128)(2,1)S(1)}, u32[]{:S(2)}, u32[]{:S(2)}) async-start(bf16[64,8,2048]{2,1,0:T(8,128)(2,1)} %bitcast.21), calls=%async_computation.4 | async-start | bytes 4194304 | tf_op jit(solution)/shard_map/all_to_all | solution.py:575
  71.4 27.4 %collective-permute-start = (bf16[2048,256]{1,0:T(8,128)(2,1)S(1)}, bf16[2048,256]{1,0:T(8,128)(2,1)}, u32[]{:S(2)}, u32[]{:S(2)}) collective-permute-start(bf16[2048,256]{1,0:T(8,128)(2,1)S(1)} %bitcast.25), channel_id=1, source_target_pairs={{0,1},{1,2},{2,3},{3,0},{4,5},{5,6},{6,7},{7,4},{8,9},{9,10},{10,1... | collective-permute-start | bytes 3145736 | tf_op jit(solution)/shard_map/ppermute | solution.py:571
  73.1 55.5 %collective-permute-start.3 = (bf16[2048,256]{1,0:T(8,128)(2,1)}, bf16[2048,256]{1,0:T(8,128)(2,1)}, u32[]{:S(2)}, u32[]{:S(2)}) collective-permute-start(bf16[2048,256]{1,0:T(8,128)(2,1)} %bitcast.27), channel_id=1, source_target_pairs={{0,3},{1,0},{2,1},{3,2},{4,7},{5,4},{6,5},{7,6},{8,11},{9,8},{10,9... | collective-permute-start | bytes 3145736 | tf_op jit(solution)/shard_map/ppermute | solution.py:571
  74.7 112.5 %collective-permute-start.1 = (bf16[2048,256]{1,0:T(8,128)(2,1)}, bf16[2048,256]{1,0:T(8,128)(2,1)}, u32[]{:S(2)}, u32[]{:S(2)}) collective-permute-start(bf16[2048,256]{1,0:T(8,128)(2,1)} %bitcast.28), channel_id=1, source_target_pairs={{0,1},{1,2},{2,3},{3,0},{4,5},{5,6},{6,7},{7,4},{8,9},{9,10},{10,1... | collective-permute-start | bytes 3145736 | tf_op jit(solution)/shard_map/ppermute | solution.py:571
  75.1 114.0 %collective-permute-start.2 = (bf16[2048,256]{1,0:T(8,128)(2,1)S(1)}, bf16[2048,256]{1,0:T(8,128)(2,1)}, u32[]{:S(2)}, u32[]{:S(2)}) collective-permute-start(bf16[2048,256]{1,0:T(8,128)(2,1)S(1)} %bitcast.26), channel_id=1, source_target_pairs={{0,3},{1,0},{2,1},{3,2},{4,7},{5,4},{6,5},{7,6},{8,11},{9,8},{10,9... | collective-permute-start | bytes 3145736 | tf_op jit(solution)/shard_map/ppermute | solution.py:571
  80.3 52.2 %collective-permute-start.6 = (bf16[128,2048]{1,0:T(8,128)(2,1)}, bf16[128,2048]{1,0:T(8,128)(2,1)}, u32[]{:S(2)}, u32[]{:S(2)}) collective-permute-start(bf16[128,2048]{1,0:T(8,128)(2,1)} %get-tuple-element.25), channel_id=1, source_target_pairs={{0,1},{1,2},{2,3},{3,0},{4,5},{5,6},{6,7},{7,4},{8,9},{9,10},{10,1... | collective-permute-start | bytes 1572872 | tf_op jit(solution)/shard_map/ppermute | solution.py:571
  98.8 90.4 %collective-permute-start.4 = (bf16[2048,256]{1,0:T(8,128)(2,1)}, bf16[2048,256]{1,0:T(8,128)(2,1)}, u32[]{:S(2)}, u32[]{:S(2)}) collective-permute-start(bf16[2048,256]{1,0:T(8,128)(2,1)} %collective-permute-done.gate_ref), channel_id=1, source_target_pairs={{0,1},{1,2},{2,3},{3,0},{4,5},{5,6},{6,7},{7,4},{8,9},{9,10},{10,1... | collective-permute-start | bytes 3145736 | tf_op jit(solution)/shard_map/ppermute | solution.py:571
  122.7 1.4 copy-start
  124.1 92.8 %all-to-all-start.3 = ((bf16[4,128,2048]{2,1,0:T(8,128)(2,1)}), bf16[4,128,2048]{2,1,0:T(8,128)(2,1)}, u32[]{:S(2)}, u32[]{:S(2)}) async-start(bf16[4,128,2048]{2,1,0:T(8,128)(2,1)} %bitcast.20), calls=%async_computation.3 | async-start | bytes 4194304 | tf_op jit(solution)/shard_map/all_to_all | solution.py:575
  128.6 75.7 %collective-permute-start.5 = (bf16[2048,256]{1,0:T(8,128)(2,1)}, bf16[2048,256]{1,0:T(8,128)(2,1)S(1)}, u32[]{:S(2)}, u32[]{:S(2)}) collective-permute-start(bf16[2048,256]{1,0:T(8,128)(2,1)} %collective-permute-done.3.up_ref), channel_id=1, source_target_pairs={{0,3},{1,0},{2,1},{3,2},{4,7},{5,4},{6,5},{7,6},{8,11},{9,8},{10,9... | collective-permute-start | bytes 3145736 | tf_op jit(solution)/shard_map/ppermute | solution.py:571
  132.5 53.3 %collective-permute-start.9 = (bf16[128,2048]{1,0:T(8,128)(2,1)}, bf16[128,2048]{1,0:T(8,128)(2,1)S(1)}, u32[]{:S(2)}, u32[]{:S(2)}) collective-permute-start(bf16[128,2048]{1,0:T(8,128)(2,1)} %get-tuple-element.24), channel_id=1, source_target_pairs={{0,3},{1,0},{2,1},{3,2},{4,7},{5,4},{6,5},{7,6},{8,11},{9,8},{10,9... | collective-permute-start | bytes 1572872 | tf_op jit(solution)/shard_map/ppermute | solution.py:571
  185.8 10.5 %copy-start.8 = (bf16[128,2048]{1,0:T(8,128)(2,1)}, bf16[128,2048]{1,0:T(8,128)(2,1)S(1)}, u32[]{:S(2)}) copy-start(bf16[128,2048]{1,0:T(8,128)(2,1)S(1)} %collective-permute-done.9.low_l) | copy-start | bytes 1572868
  185.8 23.4 %collective-permute-start.7 = (bf16[128,2048]{1,0:T(8,128)(2,1)}, bf16[128,2048]{1,0:T(8,128)(2,1)S(1)}, u32[]{:S(2)}, u32[]{:S(2)}) collective-permute-start(bf16[128,2048]{1,0:T(8,128)(2,1)} %get-tuple-element.24), channel_id=1, source_target_pairs={{0,1},{1,2},{2,3},{3,0},{4,5},{5,6},{6,7},{7,4},{8,9},{9,10},{10,1... | collective-permute-start | bytes 1572872 | tf_op jit(solution)/shard_map/ppermute | solution.py:571
  187.2 22.0 %collective-permute-start.8 = (bf16[128,2048]{1,0:T(8,128)(2,1)}, bf16[128,2048]{1,0:T(8,128)(2,1)}, u32[]{:S(2)}, u32[]{:S(2)}) collective-permute-start(bf16[128,2048]{1,0:T(8,128)(2,1)} %get-tuple-element.25), channel_id=1, source_target_pairs={{0,3},{1,0},{2,1},{3,2},{4,7},{5,4},{6,5},{7,6},{8,11},{9,8},{10,9... | collective-permute-start | bytes 1572872 | tf_op jit(solution)/shard_map/ppermute | solution.py:571
  189.1 20.6 %collective-permute-start.10 = (bf16[128,2048]{1,0:T(8,128)(2,1)}, bf16[128,2048]{1,0:T(8,128)(2,1)S(1)}, u32[]{:S(2)}, u32[]{:S(2)}) collective-permute-start(bf16[128,2048]{1,0:T(8,128)(2,1)} %collective-permute-done.6.top_r), channel_id=1, source_target_pairs={{0,1},{1,2},{2,3},{3,0},{4,5},{5,6},{6,7},{7,4},{8,9},{9,10},{10,1... | collective-permute-start | bytes 1572872 | tf_op jit(solution)/shard_map/ppermute | solution.py:571
  189.3 20.4 %collective-permute-start.11 = (bf16[128,2048]{1,0:T(8,128)(2,1)S(1)}, bf16[128,2048]{1,0:T(8,128)(2,1)S(1)}, u32[]{:S(2)}, u32[]{:S(2)}) collective-permute-start(bf16[128,2048]{1,0:T(8,128)(2,1)S(1)} %collective-permute-done.9.low_l), channel_id=1, source_target_pairs={{0,3},{1,0},{2,1},{3,2},{4,7},{5,4},{6,5},{7,6},{8,11},{9,8},{10,9... | collective-permute-start | bytes 1572872 | tf_op jit(solution)/shard_map/ppermute | solution.py:571
  209.6 1.0 copy-start.11
  216.9 60.6 %all-to-all-start.5 = ((bf16[64,8,2048]{2,1,0:T(8,128)(2,1)}), bf16[64,8,2048]{2,1,0:T(8,128)(2,1)S(1)}, u32[]{:S(2)}, u32[]{:S(2)}) async-start(bf16[64,8,2048]{2,1,0:T(8,128)(2,1)} %bitcast.22), calls=%async_computation.5 | async-start | bytes 4194304 | tf_op jit(solution)/shard_map/all_to_all | solution.py:575
  277.5 1.3 copy-start.1
  (5 other events, 3.9 us)
where the time goes:
time: 284 us; the launch traced here: 283 us
  waiting for transfers between devices  144 us (51%)
  Pallas kernels  62.9 us (22%)
  starting transfers between devices  49.8 us (18%)
  local copies, waits for them, and re-layouts  11.3 us (4%)
  blocking collectives  11.3 us (4%)
  other arithmetic  2.92 us (1%)
    all_to_all x5, waiting for transfers between devices, exchange(): return lax.all_to_all(x, axis, 0, 0, tiled=True)  72.9 us
    ppermute x12, waiting for transfers between devices, ring(): lax.ppermute(x, 'tp', [(i, (i + shift) % count) for i in range(count)])  71.1 us
    all_to_all x5, starting transfers between devices, exchange(): return lax.all_to_all(x, axis, 0, 0, tiled=True)  31.3 us
    pallas_call x1, Pallas kernels, summarize(): pl.pallas_call(summary_kernel, grid=(spans,), in_specs=[block] * 5 + [who...  19.3 us
    ppermute x12, starting transfers between devices, ring(): lax.ppermute(x, 'tp', [(i, (i + shift) % count) for i in range(count)])  18.5 us
    pallas_call x4, Pallas kernels, expert_hidden(): pl.pallas_call(hidden_kernel, grid=(2,), in_specs=[pl.BlockSpec((tile, wi...  15.9 us
    all_to_all x1, blocking collectives, exchange(): return lax.all_to_all(x, axis, 0, 0, tiled=True)  11.3 us
    unnamed x27, local copies, waits for them, and re-layouts  9 us
  transfers between devices with their start and end apart: 17, of which 8 were waited for; matrix products, arithmetic and copies ran while one was open for 2% of the time, Pallas kernels for 12%

commit v1 on v0

--- a/solution.py
+++ b/solution.py
@@ -85,10 +85,10 @@
 
 
 def summary_kernel(
-    q_ref, k_ref, v_ref, di_ref, li_ref, base_ref, shift_ref,
-    reader_ref, local_ref, gather_ref, add_ref, fade_ref, msg_ref,
-    maps_ref, total_ref,
+    here_ref, q_ref, k_ref, v_ref, di_ref, li_ref, base_ref, shift_ref,
+    reader_ref, local_ref, gather_ref, add_ref, fade_ref, *rest_refs,
 ):
+    sent_refs, (maps_ref, total_ref, msg_ref) = rest_refs[:GROUPS], rest_refs[GROUPS:]
     step = pl.program_id(0)
     rows, channels = q_ref.shape
     heads = shift_ref.shape[1]
@@ -267,6 +267,8 @@
                 msg_ref[2 * p + side, HEAD:, :] = jnp.where(
                     iota((16, PAIR), 1) < HEAD, high.astype(F32), rest.astype(F32)
                 ).astype(BF16)
+        for s in range(GROUPS):
+            sent_refs[s][...] = msg_ref[lax.rem(here_ref[0] + s, GROUPS)]
 
 
 def message_parts(message):
@@ -276,13 +278,16 @@
     return lost, gained, fades[:, :HEAD] + fades[:, HEAD:]
 
 
-def group_kernel(in_ref, prefix_ref, out_ref):
+def group_kernel(here_ref, *refs):
+    in_refs, (prefix_ref, out_ref, met_ref) = refs[:GROUPS], refs[GROUPS:]
+    for s in range(GROUPS):
+        met_ref[lax.rem(here_ref[0] + GROUPS - s, GROUPS)] = in_refs[s][...]
     rows, cols = iota((HEAD, HEAD), 0), iota((HEAD, HEAD), 1)
     eye = (rows == cols).astype(F32)
     maps = jnp.concatenate([eye, jnp.zeros((HEAD, HEAD), F32)], axis=0)
     total = jnp.ones((1, HEAD), F32)
-    for m in range(in_ref.shape[0]):
-        lost, gained, fade = message_parts(in_ref[m])
+    for m in range(GROUPS):
+        lost, gained, fade = message_parts(met_ref[m])
         prefix_ref[m] = maps
         moved = maps * fade - dot(maps.astype(BF16), lost)
         maps = jnp.concatenate([moved[:HEAD], moved[HEAD:] + gained], axis=0)
@@ -290,29 +295,36 @@
     both = jnp.concatenate([eye * total - maps[:HEAD], maps[HEAD:]], axis=1).astype(BF16)
     high, rest = two_parts(jnp.broadcast_to(total, (16, HEAD)))
     ends = jnp.concatenate([high.astype(F32), rest.astype(F32)], axis=1).astype(BF16)
-    for z in range(out_ref.shape[0]):
-        out_ref[z, :HEAD, :] = both
-        out_ref[z, HEAD:, :] = ends
-
-
-def enter_kernel(here_ref, in_ref, prefix_ref, out_ref):
-    here = here_ref[0]
+    out_ref[:HEAD, :] = both
+    out_ref[HEAD:, :] = ends
+
+
+def enter_kernel(place_ref, *refs):
+    in_refs = refs[: GROUPS - 1]
+    prefix_ref = refs[GROUPS - 1]
+    sent_refs, made_ref = refs[GROUPS:-1], refs[-1]
     state = jnp.zeros((HEAD, HEAD), F32)
-    for z in range(in_ref.shape[0]):
-        lost, gained, fade = message_parts(in_ref[z])
+    for s in range(GROUPS - 1, 0, -1):
+        lost, gained, fade = message_parts(in_refs[s - 1][...])
         passed = state * fade - dot(state.astype(BF16), lost) + gained
-        state = jnp.where(z < here, passed, state)
+        state = jnp.where(s <= place_ref[0], passed, state)
     narrow = state.astype(BF16)
-    for m in range(out_ref.shape[0]):
+    for m in range(GROUPS):
         entering = dot(narrow, prefix_ref[m, :HEAD, :].astype(BF16)) + prefix_ref[m, HEAD:, :]
-        out_ref[m] = jnp.concatenate([entering, entering], axis=1).astype(BF16)
-
-
-def readout_kernel(
-    enter_ref, reader_ref, local_ref, gather_ref, add_ref, fade_ref, gain_ref, weight_ref,
-    out_ref, state_ref,
-):
+        made_ref[m] = jnp.concatenate([entering, entering], axis=1).astype(BF16)
+    for s in range(GROUPS):
+        sent_refs[s][...] = made_ref[lax.rem(place_ref[1] + s, GROUPS)]
+
+
+def readout_kernel(place_ref, *refs):
+    enter_refs = refs[:GROUPS]
+    reader_ref, local_ref, gather_ref, add_ref, fade_ref, gain_ref, weight_ref = refs[
+        GROUPS : GROUPS + 7
+    ]
+    out_refs = refs[GROUPS + 7 : -2]
+    state_ref, heads_ref = refs[-2:]
     step = pl.program_id(0)
+    spans = len(out_refs)
     channels = reader_ref.shape[1]
     pairs = channels // PAIR
     same = block_ones()
@@ -320,8 +332,10 @@
 
     @pl.when(step == 0)
     def _():
+        for s in range(GROUPS):
+            heads_ref[lax.rem(place_ref[1] + GROUPS - s, GROUPS)] = enter_refs[s][...]
         for p in range(pairs):
-            entering = jnp.concatenate([enter_ref[2 * p], enter_ref[2 * p + 1]], axis=0)
+            entering = jnp.concatenate([heads_ref[2 * p], heads_ref[2 * p + 1]], axis=0)
             state_ref[p] = jnp.where(same, entering.astype(F32), 0.0)
 
     pieces = []
@@ -337,7 +351,12 @@
             (centred * lax.rsqrt(spread + GROUP_EPS) * gain_ref[:, lanes]).astype(BF16)
         )
     normed = jnp.concatenate(pieces, axis=1)
-    out_ref[...] = dot(normed, weight_ref[...]).astype(BF16)
+    result = dot(normed, weight_ref[...]).astype(BF16)
+    for s in range(spans):
+
+        @pl.when(lax.rem(step + spans - place_ref[2], spans) == s)
+        def _():
+            out_refs[s][...] = result
 
 
 def hidden_kernel(x_ref, gate_ref, up_ref, out_ref):
@@ -347,11 +366,9 @@
     out_ref[...] = (gates / (1.0 + jnp.exp(-gates)) * uppers).astype(BF16)
 
 
-def down_kernel(h0, h1, h2, h3, own, top_r, low_r, top_l, low_l, top_f, low_f, out_ref):
+def down_kernel(h0, h1, h2, h3, own, before, after, far, out_ref):
     units = jnp.concatenate([h0[...], h1[...], h2[...], h3[...]], axis=1)
-    weights = jnp.concatenate(
-        [w[...] for w in (own, top_r, low_r, top_l, low_l, top_f, low_f)], axis=0
-    )
+    weights = jnp.concatenate([own[...], before[...], after[...], far[...]], axis=0)
     out_ref[...] = dot(units, weights).astype(BF16)
 
 
@@ -386,9 +403,9 @@
     rest_ref[...] = rest
 
 
-def combine_kernel(high_ref, rest_ref, rows_ref, out_ref):
+def combine_kernel(high_ref, rest_ref, rows_ref, *refs):
     rows = rows_ref[...]
-    out_ref[...] = (dot(high_ref[...], rows) + dot(rest_ref[...], rows)).astype(BF16)
+    refs[-1][...] = (dot(high_ref[...], rows) + dot(rest_ref[...], rows)).astype(BF16)
 
 
 def whole(shape):
@@ -401,7 +418,10 @@
     )
 
 
-def summarize(q, k, v, di, li, base, shift):
+SCALARS = pl.BlockSpec(memory_space=pltpu.SMEM)
+
+
+def summarize(here, q, k, v, di, li, base, shift):
     rows, channels = q.shape
     heads = shift.shape[1]
     pairs = heads // 2
@@ -411,7 +431,8 @@
     return pl.pallas_call(
         summary_kernel,
         grid=(spans,),
-        in_specs=[block] * 5
+        in_specs=[SCALARS]
+        + [block] * 5
         + [whole((1, channels)), pl.BlockSpec((SPAN, heads), lambda i: (i, 0))],
         out_specs=[
             block,
@@ -419,54 +440,53 @@
             pl.BlockSpec(square, lambda i: (i, 0, 0, 0)),
             pl.BlockSpec(square, lambda i: (i, 0, 0, 0)),
             pl.BlockSpec((1, 1, channels), lambda i: (i, 0, 0)),
-            whole((heads, MSG_ROWS, PAIR)),
-        ],
+        ]
+        + [whole((MSG_ROWS, PAIR))] * GROUPS,
         out_shape=[
             jax.ShapeDtypeStruct((rows, channels), BF16),
             jax.ShapeDtypeStruct((rows, channels), F32),
             jax.ShapeDtypeStruct((spans, pairs, PAIR, PAIR), BF16),
             jax.ShapeDtypeStruct((spans, pairs, PAIR, PAIR), F32),
             jax.ShapeDtypeStruct((spans, 1, channels), F32),
-            jax.ShapeDtypeStruct((heads, MSG_ROWS, PAIR), BF16),
-        ],
+        ]
+        + [jax.ShapeDtypeStruct((MSG_ROWS, PAIR), BF16)] * GROUPS,
         scratch_shapes=[
             pltpu.VMEM((pairs, 2 * PAIR, PAIR), F32),
             pltpu.VMEM((1, channels), F32),
+            pltpu.VMEM((heads, MSG_ROWS, PAIR), BF16),
         ],
         compiler_params=pltpu.CompilerParams(dimension_semantics=("arbitrary",)),
         cost_estimate=estimate(2.0e10, 6 << 20, 2 << 20),
         name="summary",
-    )(q, k, v, di, li, base, shift)
-
-
-def group_scan(messages):
-    count = messages.shape[0]
+    )(here, q, k, v, di, li, base, shift)
+
+
+def group_scan(here, messages):
     return pl.pallas_call(
         group_kernel,
+        in_specs=[SCALARS] + [pl.BlockSpec(memory_space=pltpu.VMEM)] * GROUPS,
         out_shape=[
-            jax.ShapeDtypeStruct((count, 2 * HEAD, HEAD), F32),
-            jax.ShapeDtypeStruct((GROUPS, MSG_ROWS, PAIR), BF16),
+            jax.ShapeDtypeStruct((GROUPS, 2 * HEAD, HEAD), F32),
+            jax.ShapeDtypeStruct((MSG_ROWS, PAIR), BF16),
         ],
+        scratch_shapes=[pltpu.VMEM((GROUPS, MSG_ROWS, PAIR), BF16)],
         cost_estimate=estimate(2.0e9, 1 << 20),
         name="group_scan",
-    )(messages)
-
-
-def enter_states(here, totals, prefixes):
+    )(here, *messages)
+
+
+def enter_states(place, totals, prefixes):
     return pl.pallas_call(
         enter_kernel,
-        in_specs=[
-            pl.BlockSpec(memory_space=pltpu.SMEM),
-            pl.BlockSpec(memory_space=pltpu.VMEM),
-            pl.BlockSpec(memory_space=pltpu.VMEM),
-        ],
-        out_shape=jax.ShapeDtypeStruct((prefixes.shape[0], HEAD, PAIR), BF16),
+        in_specs=[SCALARS] + [pl.BlockSpec(memory_space=pltpu.VMEM)] * GROUPS,
+        out_shape=[jax.ShapeDtypeStruct((HEAD, PAIR), BF16)] * GROUPS,
+        scratch_shapes=[pltpu.VMEM((GROUPS, HEAD, PAIR), BF16)],
         cost_estimate=estimate(2.0e9, 1 << 20),
         name="enter_states",
-    )(here, totals, prefixes)
-
-
-def read_and_project(entering, reader, local, gather, add, fade, gain, weight):
+    )(place, *totals, prefixes)
+
+
+def read_and_project(place, entering, reader, local, gather, add, fade, gain, weight):
     rows, channels = reader.shape
     pairs = channels // PAIR
     spans = rows // SPAN
@@ -476,8 +496,9 @@
     return pl.pallas_call(
         readout_kernel,
         grid=(spans,),
-        in_specs=[
-            whole(entering.shape),
+        in_specs=[SCALARS]
+        + [whole((HEAD, PAIR))] * GROUPS
+        + [
             block,
             block,
             square,
@@ -486,13 +507,16 @@
             whole((1, channels)),
             whole(weight.shape),
         ],
-        out_specs=pl.BlockSpec((SPAN, width), lambda i: (i, 0)),
-        out_shape=jax.ShapeDtypeStruct((rows, width), BF16),
-        scratch_shapes=[pltpu.VMEM((pairs, PAIR, PAIR), F32)],
+        out_specs=[whole((SPAN, width))] * spans,
+        out_shape=[jax.ShapeDtypeStruct((SPAN, width), BF16)] * spans,
+        scratch_shapes=[
+            pltpu.VMEM((pairs, PAIR, PAIR), F32),
+            pltpu.VMEM((2 * pairs, HEAD, PAIR), BF16),
+        ],
         compiler_params=pltpu.CompilerParams(dimension_semantics=("arbitrary",)),
         cost_estimate=estimate(5.0e9, 8 << 20),
         name="readout",
-    )(entering, reader, local, gather, add, fade, gain, weight)
+    )(place, *entering, reader, local, gather, add, fade, gain, weight)
 
 
 def expert_hidden(x, gate, up):
@@ -515,21 +539,22 @@
     )(x, gate, up)
 
 
-def expert_down(hiddens, weights):
-    rows = hiddens[0].shape[0]
-    width = weights[0].shape[1]
-    tile = width // 4
+def expert_down(hiddens, own, others, part):
+    rows, units = hiddens[0].shape
+    width = others[0].shape[1]
+    tile = width // 2
     return pl.pallas_call(
         down_kernel,
-        grid=(4,),
+        grid=(2,),
         in_specs=[whole(h.shape) for h in hiddens]
-        + [pl.BlockSpec((w.shape[0], tile), lambda i: (0, i)) for w in weights],
+        + [pl.BlockSpec((units, tile), lambda i: (0, i + 2 * part))]
+        + [pl.BlockSpec((units, tile), lambda i: (0, i))] * 3,
         out_specs=pl.BlockSpec((rows, tile), lambda i: (0, i)),
         out_shape=jax.ShapeDtypeStruct((rows, width), BF16),
         compiler_params=pltpu.CompilerParams(dimension_semantics=("arbitrary",)),
-        cost_estimate=estimate(8 * rows * 256 * width, 7 << 20),
+        cost_estimate=estimate(8 * rows * units * width, 4 << 20),
         name="down",
-    )(*hiddens, *weights)
+    )(*hiddens, own, *others)
 
 
 def pack_rows(x, gain, routes, mix, places):
@@ -546,29 +571,40 @@
     )(x, gain, routes, mix)
 
 
-def combine_rows(high, rest, rows):
+def combine_rows(high, rest, rows, part, into=()):
     tokens, places = high.shape
     width = rows.shape[1]
-    tile = width // 4
+    tile = width // 2
     return pl.pallas_call(
         combine_kernel,
-        grid=(4,),
+        grid=(2,),
         in_specs=[
             whole(high.shape),
             whole(rest.shape),
             pl.BlockSpec((places, tile), lambda i: (0, i)),
-        ],
-        out_specs=pl.BlockSpec((tokens, tile), lambda i: (0, i)),
-        out_shape=jax.ShapeDtypeStruct((tokens, width), BF16),
+        ]
+        + [pl.BlockSpec(memory_space=pl.ANY)] * len(into),
+        out_specs=pl.BlockSpec((tokens, tile), lambda i: (0, i + 2 * part)),
+        out_shape=jax.ShapeDtypeStruct((tokens, 2 * width), BF16),
+        input_output_aliases={3: 0} if into else {},
         compiler_params=pltpu.CompilerParams(dimension_semantics=("arbitrary",)),
         cost_estimate=estimate(1.0e9, 3 << 20),
         name="combine",
-    )(high, rest, rows)
-
-
-def ring(x, shift):
-    count = lax.axis_size("tp")
-    return lax.ppermute(x, "tp", [(i, (i + shift) % count) for i in range(count)])
+    )(high, rest, rows, *into)
+
+
+def ring(x, shift, axis="tp"):
+    count = lax.axis_size(axis)
+    return lax.ppermute(x, axis, [(i, (i + shift) % count) for i in range(count)])
+
+
+def onward(x, shift, axis):
+    count = lax.axis_size(axis)
+    return lax.ppermute(x, axis, [(i, i + shift) for i in range(count - shift)])
+
+
+def around(parts, axis):
+    return [parts[0]] + [ring(part, n, axis) for n, part in enumerate(parts) if n]
 
 
 def exchange(x, axis):
@@ -594,21 +630,21 @@
     down_weight,
 ):
     ep_count = lax.axis_size(EP)
-    token_rows, model_width = expert_input.shape
+    _, model_width = expert_input.shape
     experts = gate_weight.shape[0] * ep_count
     places = experts * CAPACITY
 
     w_gate = gate_weight[0]
     w_up = up_weight[0]
     w_down = down_weight[0]
-    cut = w_down.shape[0] // 2
-    down_top, down_low = w_down[:cut], w_down[cut:]
+    cut = model_width // 2
+    down_0, down_1 = w_down[:, :cut], w_down[:, cut:]
     gate_r, up_l = ring(w_gate, 1), ring(w_up, -1)
     gate_l, up_r = ring(w_gate, -1), ring(w_up, 1)
-    top_r, low_l = ring(down_top, 1), ring(down_low, -1)
-    low_r, top_l = ring(down_low, 1), ring(down_top, -1)
     gate_f, up_f = ring(gate_r, 1), ring(up_l, -1)
-    top_f, low_f = ring(top_r, 1), ring(low_l, -1)
+    down_0r, down_0l = ring(down_0, 1), ring(down_0, -1)
+    down_1r, down_1l = ring(down_1, 1), ring(down_1, -1)
+    down_0f, down_1f = ring(down_0r, 1), ring(down_1l, -1)
 
     outgoing, high, rest = pack_rows(
         expert_input, expert_gain.reshape(1, -1), routes, route_weight, places
@@ -617,7 +653,11 @@
         outgoing.reshape(experts, CAPACITY, model_width), EP
     ).reshape(places, model_width)
 
-    reader, local, gather, add, fade, messages = summarize(
+    place = jnp.stack(
+        [lax.axis_index("ep_0"), lax.axis_index(GROUP), lax.axis_index("tp")]
+    ).astype(jnp.int32)
+    reader, local, gather, add, fade, *messages = summarize(
+        place[1:2],
         receptance,
         key_rows,
         value_rows,
@@ -626,14 +666,12 @@
         decay_base.reshape(1, -1),
         decay_shift,
     )
-    prefixes, totals = group_scan(exchange(messages, GROUP))
-    entered = enter_states(
-        lax.axis_index("ep_0").astype(jnp.int32).reshape(1),
-        exchange(totals, "ep_0"),
-        prefixes,
-    )
+    prefixes, total = group_scan(place[1:2], around(messages, GROUP))
+    totals = [onward(total, n, "ep_0") for n in range(1, GROUPS)]
+    entered = enter_states(place, totals, prefixes)
     partial = read_and_project(
-        exchange(entered, GROUP),
+        place,
+        around(entered, GROUP),
         reader,
         local,
         gather,
@@ -642,17 +680,22 @@
         channel_gain.reshape(1, -1),
         out_weight,
     )
-    tp_count = lax.axis_size("tp")
-    shares = exchange(partial.reshape(tp_count, token_rows, model_width), "tp")
-    mixer_out = jnp.sum(shares.astype(F32), axis=0).astype(BF16)
+    shares = around(partial, "tp")
+    mixer_out = sum(share.astype(F32) for share in shares).astype(BF16)
 
     hiddens = []
     for g, u in ((w_gate, w_up), (gate_r, up_r), (gate_l, up_l), (gate_f, up_f)):
         hiddens.append(expert_hidden(arrived, g, u))
-    returning = expert_down(hiddens, [w_down, top_r, low_r, top_l, low_l, top_f, low_f])
-    returned = exchange(returning.reshape(ep_count, CAPACITY, model_width), EP)
-    combined = combine_rows(high, rest, returned.reshape(places, model_width))
-    return (mixer_out, combined)
+    combined = ()
+    for n, others in enumerate(((down_0r, down_0l, down_0f), (down_1r, down_1l, down_1f))):
+        returning = expert_down(hiddens, w_down, others, n)
+        if n:
+            returning, returned = lax.optimization_barrier((returning, returned))
+            combined = (combine_rows(high, rest, returned, 0),)
+        returned = exchange(
+            returning.reshape(ep_count, CAPACITY, cut), EP
+        ).reshape(places, cut)
+    return (mixer_out, combine_rows(high, rest, returned, 1, combined))
 
 
 def solution(mesh):

time: 284 us -> 284 us (level)
  starting transfers between devices: 49.8 us -> 96.1 us
  waiting for transfers between devices: 144 us -> 107 us
  blocking collectives: 11.3 us -> 0 us
  Pallas kernels: 62.9 us -> 66.2 us
    all_to_all x5 -> x3, waiting for transfers between devices: 72.9 us -> 0.01 us  [exchange(): return lax.all_to_all(x, axis, 0, 0, tiled=True)]
    ppermute x12 -> x36, starting transfers between devices: 18.5 us -> 63.7 us  [the longest x29 36.9 us: ring(): lax.ppermute(x, axis, [(i, (i + shift) % count) for i in range(count)])]
    ppermute x12 -> x36, waiting for transfers between devices: 71.1 us -> 107 us  [the longest x29 99.6 us: ring(): lax.ppermute(x, axis, [(i, (i + shift) % count) for i in range(count)])]
    all_to_all x1 -> x0, blocking collectives: 11.3 us -> none  [exchange(): return lax.all_to_all(x, axis, 0, 0, tiled=True)]
    pallas_call x6 -> x8, Pallas kernels: 43.4 us -> 46.6 us  [the longest x1 19.4 us: summarize(): pl.pallas_call(summary_kernel, grid=(spans,), in_specs=[SCALARS] + [block...]
    reduce_sum x1 -> x0, other arithmetic: 2.92 us -> none  [on_device(): mixer_out = jnp.sum(shares.astype(F32), axis=0).astype(BF16)]
    all_to_all x5 -> x3, starting transfers between devices: 31.3 us -> 32.3 us  [exchange(): return lax.all_to_all(x, axis, 0, 0, tiled=True)]
    unnamed x27 -> x67, local copies, waits for them, and re-layouts: 9 us -> 8.84 us
  transfers between devices with their start and end apart: 17 -> 39, of which waited for: 8 -> 10; matrix products, arithmetic and copies ran while one was open for 2% -> 2% of each run, Pallas kernels for 12% -> 21%
where the time goes in v1:
time: 284 us; the launch traced here: 283 us
  waiting for transfers between devices  107 us (38%)
  starting transfers between devices  96.1 us (34%)
  Pallas kernels  66.2 us (23%)
  local copies, waits for them, and re-layouts  9.9 us (3%)
    ppermute x29, waiting for transfers between devices, ring(): lax.ppermute(x, axis, [(i, (i + shift) % count) for i in range(count)])  99.6 us
    ppermute x29, starting transfers between devices, ring(): lax.ppermute(x, axis, [(i, (i + shift) % count) for i in range(count)])  36.9 us
    all_to_all x3, starting transfers between devices, exchange(): return lax.all_to_all(x, axis, 0, 0, tiled=True)  32.3 us
    ppermute x7, starting transfers between devices, onward(): return lax.ppermute(x, axis, [(i, i + shift) for i in range(count - shift)])  26.9 us
    pallas_call x1, Pallas kernels, summarize(): pl.pallas_call(summary_kernel, grid=(spans,), in_specs=[SCALARS] + [block...  19.4 us
    pallas_call x4, Pallas kernels, expert_hidden(): pl.pallas_call(hidden_kernel, grid=(2,), in_specs=[pl.BlockSpec((tile, wi...  15.9 us
    pallas_call x1, Pallas kernels, read_and_project(): pl.pallas_call(readout_kernel, grid=(spans,), in_specs=[SCALARS] + [whole...  9.07 us
    unnamed x67, local copies, waits for them, and re-layouts  8.84 us
  transfers between devices with their start and end apart: 39, of which 10 were waited for; matrix products, arithmetic and copies ran while one was open for 2% of the time, Pallas kernels for 21%

profile of v1, /device:TPU:2, one launch (start us, length us, event | category | flops | bytes accessed | tf_op | source)
XLA Modules:
  0.0 282.7 jit_solution(8520132912279064772)
XLA Ops:
  3.5 3.6 %pack.1 = (bf16[512,2048]{1,0:T(8,128)(2,1)}, bf16[128,512]{1,0:T(8,128)(2,1)}, bf16[128,512]{1,0:T(8,128)(2,1)}) custom-call(bf16[128,2048]{1,0:T(8,128)(2,1)} %x_ref.1, f32[1,2048]{1,0:T(1,128)} %bitcast.33, s32[128,2]{1,0:T(8,128)} %copy.20.routes_ref, f32[128,2]{1,0:T(8,128)} %copy.21.mix_ref), custom_call_target="tpu_custom_call" | custom-call | flops 2000000000 | bytes 3145728 | tf_op jit(solution)/shard_map/pack/pallas_call | solution.py:562
  7.0 12.1 %all-to-all-start = ((bf16[64,8,2048]{2,1,0:T(8,128)(2,1)}), bf16[64,8,2048]{2,1,0:T(8,128)(2,1)S(1)}, u32[]{:S(2)}, u32[]{:S(2)}) async-start(bf16[64,8,2048]{2,1,0:T(8,128)(2,1)} %bitcast.24), calls=%async_computation | async-start | bytes 4194304 | tf_op jit(solution)/shard_map/all_to_all | solution.py:611
  22.9 2.9 %collective-permute-start.26 = (bf16[2048,256]{1,0:T(8,128)(2,1)}, bf16[2048,256]{1,0:T(8,128)(2,1)S(1)}, u32[]{:S(2)}, u32[]{:S(2)}) collective-permute-start(bf16[2048,256]{1,0:T(8,128)(2,1)} %bitcast.26), channel_id=1, source_target_pairs={{0,3},{1,0},{2,1},{3,2},{4,7},{5,4},{6,5},{7,6},{8,11},{9,8},{10,9... | collective-permute-start | bytes 3145736 | tf_op jit(solution)/shard_map/ppermute | solution.py:598
  25.7 21.1 %collective-permute-done.24.gate_ref = bf16[2048,256]{1,0:T(8,128)(2,1)} collective-permute-done((bf16[2048,256]{1,0:T(8,128)(2,1)}, bf16[2048,256]{1,0:T(8,128)(2,1)}, u32[]{:S(2)}, u32[]{:S(2)}) %collective-permute-start.24) | collective-permute-done | bytes 1048608 | tf_op jit(solution)/shard_map/ppermute | solution.py:598
  47.2 2.9 %collective-permute-start.29 = (bf16[2048,256]{1,0:T(8,128)(2,1)}, bf16[2048,256]{1,0:T(8,128)(2,1)}, u32[]{:S(2)}, u32[]{:S(2)}) collective-permute-start(bf16[2048,256]{1,0:T(8,128)(2,1)} %collective-permute-done.27.up_ref), channel_id=1, source_target_pairs={{0,3},{1,0},{2,1},{3,2},{4,7},{5,4},{6,5},{7,6},{8,11},{9,8},{10,9... | collective-permute-start | bytes 3145736 | tf_op jit(solution)/shard_map/ppermute | solution.py:598
  51.1 51.0 %collective-permute-done.33.before = bf16[256,1024]{1,0:T(8,128)(2,1)S(1)} collective-permute-done((bf16[256,1024]{1,0:T(8,128)(2,1)}, bf16[256,1024]{1,0:T(8,128)(2,1)S(1)}, u32[]{:S(2)}, u32[]{:S(2)}) %collective-permute-start.33) | collective-permute-done | bytes 524320 | tf_op jit(solution)/shard_map/ppermute | solution.py:598
  105.3 2.9 %collective-permute-start.31 = (bf16[256,1024]{1,0:T(8,128)(2,1)}, bf16[256,1024]{1,0:T(8,128)(2,1)S(1)}, u32[]{:S(2)}, u32[]{:S(2)}) collective-permute-start(bf16[256,1024]{1,0:T(8,128)(2,1)} %get-tuple-element.67), channel_id=1, source_target_pairs={{0,3},{1,0},{2,1},{3,2},{4,7},{5,4},{6,5},{7,6},{8,11},{9,8},{10,9... | collective-permute-start | bytes 1572872 | tf_op jit(solution)/shard_map/ppermute | solution.py:598
  109.5 4.0 %hidden.4.h0 = bf16[512,256]{1,0:T(8,128)(2,1)} custom-call(bf16[512,2048]{1,0:T(8,128)(2,1)} %bitcast.15, bf16[2048,256]{1,0:T(8,128)(2,1)} %bitcast.27, bf16[2048,256]{1,0:T(8,128)(2,1)} %bitcast.30), custom_call_target="tpu_custom_call" | custom-call | flops 1073741824 | bytes 5242880 | tf_op jit(solution)/shard_map/hidden/pallas_call | solution.py:526
  113.5 4.0 %hidden.5.h1 = bf16[512,256]{1,0:T(8,128)(2,1)} custom-call(bf16[512,2048]{1,0:T(8,128)(2,1)} %bitcast.16, bf16[2048,256]{1,0:T(8,128)(2,1)} %collective-permute-done.24.gate_ref, bf16[2048,256]{1,0:T(8,128)(2,1)} %copy-done.2), custom_call_target="tpu_custom_call" | custom-call | flops 1073741824 | bytes 5242880 | tf_op jit(solution)/shard_map/hidden/pallas_call | solution.py:526
  117.4 4.0 %hidden.6.h2 = bf16[512,256]{1,0:T(8,128)(2,1)} custom-call(bf16[512,2048]{1,0:T(8,128)(2,1)} %bitcast.17, bf16[2048,256]{1,0:T(8,128)(2,1)} %copy-done.3, bf16[2048,256]{1,0:T(8,128)(2,1)} %collective-permute-done.27.up_ref), custom_call_target="tpu_custom_call" | custom-call | flops 1073741824 | bytes 5242880 | tf_op jit(solution)/shard_map/hidden/pallas_call | solution.py:526
  121.4 4.0 %hidden.7.h3 = bf16[512,256]{1,0:T(8,128)(2,1)} custom-call(bf16[512,2048]{1,0:T(8,128)(2,1)} %bitcast.18, bf16[2048,256]{1,0:T(8,128)(2,1)} %collective-permute-done.28.gate_ref, bf16[2048,256]{1,0:T(8,128)(2,1)} %collective-permute-done.29.up_ref), custom_call_target="tpu_custom_call" | custom-call | flops 1073741824 | bytes 5242880 | tf_op jit(solution)/shard_map/hidden/pallas_call | solution.py:526
  125.5 4.0 %down.3 = bf16[512,1024]{1,0:T(8,128)(2,1)} custom-call(bf16[512,256]{1,0:T(8,128)(2,1)} %hidden.4.h0, bf16[512,256]{1,0:T(8,128)(2,1)} %hidden.5.h1, bf16[512,256]{1,0:T(8,128)(2,1)} %hidden.6.h2, bf16[512,256]{1,0:T(8,128)(2,1)} %hidden.7.h3, bf16[256,2048]{1,0:T(8,128)(2,1)} %bitcast.19, bf16[256,1024]{1,0:T(8,128)(2,1)} %copy-done.9, ...), custom_call_target="tpu_custom_call" | custom-call | flops 1073741824 | bytes 4194304 | tf_op jit(solution)/shard_map/down/pallas_call | solution.py:546
  129.4 10.4 %all-to-all-start.1 = ((bf16[64,8,1024]{2,1,0:T(8,128)(2,1)}), bf16[64,8,1024]{2,1,0:T(8,128)(2,1)S(1)}, u32[]{:S(2)}, u32[]{:S(2)}) async-start(bf16[64,8,1024]{2,1,0:T(8,128)(2,1)} %bitcast.23), calls=%async_computation.1 | async-start | bytes 2097152 | tf_op jit(solution)/shard_map/all_to_all | solution.py:611
  140.8 3.2 %collective-permute-start.32 = (bf16[256,1024]{1,0:T(8,128)(2,1)S(1)}, bf16[256,1024]{1,0:T(8,128)(2,1)S(1)}, u32[]{:S(2)}, u32[]{:S(2)}) collective-permute-start(bf16[256,1024]{1,0:T(8,128)(2,1)S(1)} %collective-permute-done.31.after), channel_id=1, source_target_pairs={{0,3},{1,0},{2,1},{3,2},{4,7},{5,4},{6,5},{7,6},{8,11},{9,8},{10,9... | collective-permute-start | bytes 1572872 | tf_op jit(solution)/shard_map/ppermute | solution.py:598
  144.0 19.4 %summary.1 = (bf16[512,512]{1,0:T(8,128)(2,1)}, f32[512,512]{1,0:T(8,128)}, bf16[4,4,128,128]{3,2,1,0:T(8,128)(2,1)}, f32[4,4,128,128]{3,2,1,0:T(8,128)}, f32[4,...) custom-call(s32[1]{0:T(128)} %bitcast.1.here_ref, ...), custom_call_target="tpu_custom_call" | custom-call | flops 20000000000 | bytes 6291456 | tf_op jit(solution)/shard_map/summary/pallas_call | solution.py:431
  172.1 3.9 %down.2 = bf16[512,1024]{1,0:T(8,128)(2,1)} custom-call(bf16[512,256]{1,0:T(8,128)(2,1)} %hidden.4.h0, bf16[512,256]{1,0:T(8,128)(2,1)} %hidden.5.h1, bf16[512,256]{1,0:T(8,128)(2,1)} %hidden.6.h2, bf16[512,256]{1,0:T(8,128)(2,1)} %hidden.7.h3, bf16[256,2048]{1,0:T(8,128)(2,1)} %bitcast.20, bf16[256,1024]{1,0:T(8,128)(2,1)} %copy-done.7, ...), custom_call_target="tpu_custom_call" | custom-call | flops 1073741824 | bytes 4194304 | tf_op jit(solution)/shard_map/down/pallas_call | solution.py:546
  176.1 9.8 %all-to-all-start.2 = ((bf16[64,8,1024]{2,1,0:T(8,128)(2,1)}), bf16[64,8,1024]{2,1,0:T(8,128)(2,1)S(1)}, u32[]{:S(2)}, u32[]{:S(2)}) async-start(bf16[64,8,1024]{2,1,0:T(8,128)(2,1)} %bitcast.22), calls=%async_computation.2 | async-start | bytes 2097152 | tf_op jit(solution)/shard_map/all_to_all | solution.py:611
  189.1 7.4 %collective-permute-start.10 = (bf16[80,128]{1,0:T(8,128)(2,1)}, bf16[80,128]{1,0:T(8,128)(2,1)S(1)}, u32[]{:S(2)}, u32[]{:S(2)}) collective-permute-start(bf16[80,128]{1,0:T(8,128)(2,1)} %get-tuple-element.42), channel_id=1, source_target_pairs={{0,128},{32,160},{64,192},{96,224},{1,129},{33,161},{65,193},{97,2... | collective-permute-start | bytes 61448 | tf_op jit(solution)/shard_map/ppermute | solution.py:603
  202.3 6.0 %collective-permute-done.10.refs_3_ = bf16[80,128]{1,0:T(8,128)(2,1)S(1)} collective-permute-done((bf16[80,128]{1,0:T(8,128)(2,1)}, bf16[80,128]{1,0:T(8,128)(2,1)S(1)}, u32[]{:S(2)}, u32[]{:S(2)}) %collective-permute-start.10) | collective-permute-done | bytes 20512 | tf_op jit(solution)/shard_map/ppermute | solution.py:603
  208.3 5.7 %collective-permute-start.8 = (bf16[80,128]{1,0:T(8,128)(2,1)}, bf16[80,128]{1,0:T(8,128)(2,1)S(1)}, u32[]{:S(2)}, u32[]{:S(2)}) collective-permute-start(bf16[80,128]{1,0:T(8,128)(2,1)} %get-tuple-element.42), channel_id=1, source_target_pairs={{0,64},{32,96},{64,128},{96,160},{128,192},{160,224},{1,65},{33,97... | collective-permute-start | bytes 61448 | tf_op jit(solution)/shard_map/ppermute | solution.py:603
  214.1 8.1 %collective-permute-start.9 = (bf16[80,128]{1,0:T(8,128)(2,1)}, bf16[80,128]{1,0:T(8,128)(2,1)S(1)}, u32[]{:S(2)}, u32[]{:S(2)}) collective-permute-start(bf16[80,128]{1,0:T(8,128)(2,1)} %get-tuple-element.42), channel_id=1, source_target_pairs={{0,96},{32,128},{64,160},{96,192},{128,224},{1,97},{33,129},{65,16... | collective-permute-start | bytes 61448 | tf_op jit(solution)/shard_map/ppermute | solution.py:603
  224.4 2.9 %enter_states.1 = (bf16[64,128]{1,0:T(8,128)(2,1)}, bf16[64,128]{1,0:T(8,128)(2,1)}, bf16[64,128]{1,0:T(8,128)(2,1)}, bf16[64,128]{1,0:T(8,128)(2,1)}, bf16[64,1...) custom-call(s32[3]{0:T(128)} %pad_add_fusion.place_ref, ...), custom_call_target="tpu_custom_call" | custom-call | flops 2000000000 | bytes 1048576 | tf_op jit(solution)/shard_map/enter_states/pallas_call | solution.py:479
  237.5 9.1 %readout.1 = (bf16[128,2048]{1,0:T(8,128)(2,1)}, bf16[128,2048]{1,0:T(8,128)(2,1)}, bf16[128,2048]{1,0:T(8,128)(2,1)}, bf16[128,2048]{1,0:T(8,128)(2,1)}) custom-call(s32[3]{0:T(128)} %pad_add_fusion.place_ref, bf16[64,128]{1,0:T(8,128)(2,1)} %get-tuple-element.44.refs_0_, bf16[64,128]{1,0:T(8,128)(2,1)} %copy-done.25, bf16[64,128]{1,0:T(8,128)(2,1)} %copy-done.26, ...), custom_call_target="tpu_custom_call" | custom-call | flops 5000000000 | bytes 8388608 | tf_op jit(solution)/shard_map/readout/pallas_call | solution.py:496
  249.9 24.1 %collective-permute-done.21 = bf16[128,2048]{1,0:T(8,128)(2,1)S(1)} collective-permute-done((bf16[128,2048]{1,0:T(8,128)(2,1)}, bf16[128,2048]{1,0:T(8,128)(2,1)S(1)}, u32[]{:S(2)}, u32[]{:S(2)}) %collective-permute-start.21) | collective-permute-done | bytes 524320 | tf_op jit(solution)/shard_map/ppermute | solution.py:598
  (137 shorter events, 55.2 us)
Async XLA Ops:
  7.0 101.1 %all-to-all-start = ((bf16[64,8,2048]{2,1,0:T(8,128)(2,1)}), bf16[64,8,2048]{2,1,0:T(8,128)(2,1)S(1)}, u32[]{:S(2)}, u32[]{:S(2)}) async-start(bf16[64,8,2048]{2,1,0:T(8,128)(2,1)} %bitcast.24), calls=%async_computation | async-start | bytes 4194304 | tf_op jit(solution)/shard_map/all_to_all | solution.py:611
  19.2 27.6 %collective-permute-start.24 = (bf16[2048,256]{1,0:T(8,128)(2,1)}, bf16[2048,256]{1,0:T(8,128)(2,1)}, u32[]{:S(2)}, u32[]{:S(2)}) collective-permute-start(bf16[2048,256]{1,0:T(8,128)(2,1)} %bitcast.25), channel_id=1, source_target_pairs={{0,1},{1,2},{2,3},{3,0},{4,5},{5,6},{6,7},{7,4},{8,9},{9,10},{10,1... | collective-permute-start | bytes 3145736 | tf_op jit(solution)/shard_map/ppermute | solution.py:598
  20.9 26.3 %collective-permute-start.27 = (bf16[2048,256]{1,0:T(8,128)(2,1)}, bf16[2048,256]{1,0:T(8,128)(2,1)}, u32[]{:S(2)}, u32[]{:S(2)}) collective-permute-start(bf16[2048,256]{1,0:T(8,128)(2,1)} %bitcast.28), channel_id=1, source_target_pairs={{0,3},{1,0},{2,1},{3,2},{4,7},{5,4},{6,5},{7,6},{8,11},{9,8},{10,9... | collective-permute-start | bytes 3145736 | tf_op jit(solution)/shard_map/ppermute | solution.py:598
  22.5 81.3 %collective-permute-start.25 = (bf16[2048,256]{1,0:T(8,128)(2,1)}, bf16[2048,256]{1,0:T(8,128)(2,1)S(1)}, u32[]{:S(2)}, u32[]{:S(2)}) collective-permute-start(bf16[2048,256]{1,0:T(8,128)(2,1)} %bitcast.29), channel_id=1, source_target_pairs={{0,1},{1,2},{2,3},{3,0},{4,5},{5,6},{6,7},{7,4},{8,9},{9,10},{10,1... | collective-permute-start | bytes 3145736 | tf_op jit(solution)/shard_map/ppermute | solution.py:598
  22.9 81.3 %collective-permute-start.26 = (bf16[2048,256]{1,0:T(8,128)(2,1)}, bf16[2048,256]{1,0:T(8,128)(2,1)S(1)}, u32[]{:S(2)}, u32[]{:S(2)}) collective-permute-start(bf16[2048,256]{1,0:T(8,128)(2,1)} %bitcast.26), channel_id=1, source_target_pairs={{0,3},{1,0},{2,1},{3,2},{4,7},{5,4},{6,5},{7,6},{8,11},{9,8},{10,9... | collective-permute-start | bytes 3145736 | tf_op jit(solution)/shard_map/ppermute | solution.py:598
  46.8 74.6 %collective-permute-start.28 = (bf16[2048,256]{1,0:T(8,128)(2,1)}, bf16[2048,256]{1,0:T(8,128)(2,1)}, u32[]{:S(2)}, u32[]{:S(2)}) collective-permute-start(bf16[2048,256]{1,0:T(8,128)(2,1)} %collective-permute-done.24.gate_ref), channel_id=1, source_target_pairs={{0,1},{1,2},{2,3},{3,0},{4,5},{5,6},{6,7},{7,4},{8,9},{9,10},{10,1... | collective-permute-start | bytes 3145736 | tf_op jit(solution)/shard_map/ppermute | solution.py:598
  47.2 74.2 %collective-permute-start.29 = (bf16[2048,256]{1,0:T(8,128)(2,1)}, bf16[2048,256]{1,0:T(8,128)(2,1)}, u32[]{:S(2)}, u32[]{:S(2)}) collective-permute-start(bf16[2048,256]{1,0:T(8,128)(2,1)} %collective-permute-done.27.up_ref), channel_id=1, source_target_pairs={{0,3},{1,0},{2,1},{3,2},{4,7},{5,4},{6,5},{7,6},{8,11},{9,8},{10,9... | collective-permute-start | bytes 3145736 | tf_op jit(solution)/shard_map/ppermute | solution.py:598
  51.1 51.0 %collective-permute-start.33 = (bf16[256,1024]{1,0:T(8,128)(2,1)}, bf16[256,1024]{1,0:T(8,128)(2,1)S(1)}, u32[]{:S(2)}, u32[]{:S(2)}) collective-permute-start(bf16[256,1024]{1,0:T(8,128)(2,1)} %get-tuple-element.66), channel_id=1, source_target_pairs={{0,1},{1,2},{2,3},{3,0},{4,5},{5,6},{6,7},{7,4},{8,9},{9,10},{10,1... | collective-permute-start | bytes 1572872 | tf_op jit(solution)/shard_map/ppermute | solution.py:598
  102.1 23.3 %collective-permute-start.34 = (bf16[256,1024]{1,0:T(8,128)(2,1)}, bf16[256,1024]{1,0:T(8,128)(2,1)}, u32[]{:S(2)}, u32[]{:S(2)}) collective-permute-start(bf16[256,1024]{1,0:T(8,128)(2,1)} %get-tuple-element.66), channel_id=1, source_target_pairs={{0,3},{1,0},{2,1},{3,2},{4,7},{5,4},{6,5},{7,6},{8,11},{9,8},{10,9... | collective-permute-start | bytes 1572872 | tf_op jit(solution)/shard_map/ppermute | solution.py:598
  103.9 21.6 %collective-permute-start.35 = (bf16[256,1024]{1,0:T(8,128)(2,1)S(1)}, bf16[256,1024]{1,0:T(8,128)(2,1)}, u32[]{:S(2)}, u32[]{:S(2)}) collective-permute-start(bf16[256,1024]{1,0:T(8,128)(2,1)S(1)} %collective-permute-done.33.before), channel_id=1, source_target_pairs={{0,1},{1,2},{2,3},{3,0},{4,5},{5,6},{6,7},{7,4},{8,9},{9,10},{10,1... | collective-permute-start | bytes 1572872 | tf_op jit(solution)/shard_map/ppermute | solution.py:598
  105.3 35.5 %collective-permute-start.31 = (bf16[256,1024]{1,0:T(8,128)(2,1)}, bf16[256,1024]{1,0:T(8,128)(2,1)S(1)}, u32[]{:S(2)}, u32[]{:S(2)}) collective-permute-start(bf16[256,1024]{1,0:T(8,128)(2,1)} %get-tuple-element.67), channel_id=1, source_target_pairs={{0,3},{1,0},{2,1},{3,2},{4,7},{5,4},{6,5},{7,6},{8,11},{9,8},{10,9... | collective-permute-start | bytes 1572872 | tf_op jit(solution)/shard_map/ppermute | solution.py:598
  129.4 46.6 %all-to-all-start.1 = ((bf16[64,8,1024]{2,1,0:T(8,128)(2,1)}), bf16[64,8,1024]{2,1,0:T(8,128)(2,1)S(1)}, u32[]{:S(2)}, u32[]{:S(2)}) async-start(bf16[64,8,1024]{2,1,0:T(8,128)(2,1)} %bitcast.23), calls=%async_computation.1 | async-start | bytes 2097152 | tf_op jit(solution)/shard_map/all_to_all | solution.py:611
  139.9 29.2 %collective-permute-start.30 = (bf16[256,1024]{1,0:T(8,128)(2,1)}, bf16[256,1024]{1,0:T(8,128)(2,1)S(1)}, u32[]{:S(2)}, u32[]{:S(2)}) collective-permute-start(bf16[256,1024]{1,0:T(8,128)(2,1)} %get-tuple-element.67), channel_id=1, source_target_pairs={{0,1},{1,2},{2,3},{3,0},{4,5},{5,6},{6,7},{7,4},{8,9},{9,10},{10,1... | collective-permute-start | bytes 1572872 | tf_op jit(solution)/shard_map/ppermute | solution.py:598
  140.8 30.4 %collective-permute-start.32 = (bf16[256,1024]{1,0:T(8,128)(2,1)S(1)}, bf16[256,1024]{1,0:T(8,128)(2,1)S(1)}, u32[]{:S(2)}, u32[]{:S(2)}) collective-permute-start(bf16[256,1024]{1,0:T(8,128)(2,1)S(1)} %collective-permute-done.31.after), channel_id=1, source_target_pairs={{0,3},{1,0},{2,1},{3,2},{4,7},{5,4},{6,5},{7,6},{8,11},{9,8},{10,9... | collective-permute-start | bytes 1572872 | tf_op jit(solution)/shard_map/ppermute | solution.py:598
  165.0 20.8 %collective-permute-start.2 = (bf16[80,128]{1,0:T(8,128)(2,1)}, bf16[80,128]{1,0:T(8,128)(2,1)S(1)}, u32[]{:S(2)}, u32[]{:S(2)}) collective-permute-start(bf16[80,128]{1,0:T(8,128)(2,1)} %get-tuple-element.37), channel_id=1, source_target_pairs={{0,12},{4,16},{8,20},{12,24},{16,28},{20,0},{24,4},{28,8},{1,13},{... | collective-permute-start | bytes 61448 | tf_op jit(solution)/shard_map/ppermute | solution.py:598
  166.9 19.0 %collective-permute-start.3 = (bf16[80,128]{1,0:T(8,128)(2,1)}, bf16[80,128]{1,0:T(8,128)(2,1)S(1)}, u32[]{:S(2)}, u32[]{:S(2)}) collective-permute-start(bf16[80,128]{1,0:T(8,128)(2,1)} %get-tuple-element.38), channel_id=1, source_target_pairs={{0,16},{4,20},{8,24},{12,28},{16,0},{20,4},{24,8},{28,12},{1,17},{... | collective-permute-start | bytes 61448 | tf_op jit(solution)/shard_map/ppermute | solution.py:598
  176.1 103.2 %all-to-all-start.2 = ((bf16[64,8,1024]{2,1,0:T(8,128)(2,1)}), bf16[64,8,1024]{2,1,0:T(8,128)(2,1)S(1)}, u32[]{:S(2)}, u32[]{:S(2)}) async-start(bf16[64,8,1024]{2,1,0:T(8,128)(2,1)} %bitcast.22), calls=%async_computation.2 | async-start | bytes 2097152 | tf_op jit(solution)/shard_map/all_to_all | solution.py:611
  189.1 19.2 %collective-permute-start.10 = (bf16[80,128]{1,0:T(8,128)(2,1)}, bf16[80,128]{1,0:T(8,128)(2,1)S(1)}, u32[]{:S(2)}, u32[]{:S(2)}) collective-permute-start(bf16[80,128]{1,0:T(8,128)(2,1)} %get-tuple-element.42), channel_id=1, source_target_pairs={{0,128},{32,160},{64,192},{96,224},{1,129},{33,161},{65,193},{97,2... | collective-permute-start | bytes 61448 | tf_op jit(solution)/shard_map/ppermute | solution.py:603
  197.8 25.0 %collective-permute-start.12 = (bf16[80,128]{1,0:T(8,128)(2,1)}, bf16[80,128]{1,0:T(8,128)(2,1)S(1)}, u32[]{:S(2)}, u32[]{:S(2)}) collective-permute-start(bf16[80,128]{1,0:T(8,128)(2,1)} %get-tuple-element.42), channel_id=1, source_target_pairs={{0,192},{32,224},{1,193},{33,225},{2,194},{34,226},{3,195},{35,227... | collective-permute-start | bytes 61448 | tf_op jit(solution)/shard_map/ppermute | solution.py:603
  199.1 23.7 %collective-permute-start.13 = (bf16[80,128]{1,0:T(8,128)(2,1)}, bf16[80,128]{1,0:T(8,128)(2,1)S(1)}, u32[]{:S(2)}, u32[]{:S(2)}) collective-permute-start(bf16[80,128]{1,0:T(8,128)(2,1)} %get-tuple-element.42), channel_id=1, source_target_pairs={{0,224},{1,225},{2,226},{3,227},{4,228},{5,229},{6,230},{7,231},{8... | collective-permute-start | bytes 61448 | tf_op jit(solution)/shard_map/ppermute | solution.py:603
  200.4 22.4 %collective-permute-start.7 = (bf16[80,128]{1,0:T(8,128)(2,1)}, bf16[80,128]{1,0:T(8,128)(2,1)S(1)}, u32[]{:S(2)}, u32[]{:S(2)}) collective-permute-start(bf16[80,128]{1,0:T(8,128)(2,1)} %get-tuple-element.42), channel_id=1, source_target_pairs={{0,32},{32,64},{64,96},{96,128},{128,160},{160,192},{192,224},{1,3... | collective-permute-start | bytes 61448 | tf_op jit(solution)/shard_map/ppermute | solution.py:603
  246.6 27.5 %collective-permute-start.21 = (bf16[128,2048]{1,0:T(8,128)(2,1)}, bf16[128,2048]{1,0:T(8,128)(2,1)S(1)}, u32[]{:S(2)}, u32[]{:S(2)}) collective-permute-start(bf16[128,2048]{1,0:T(8,128)(2,1)} %get-tuple-element.58), channel_id=1, source_target_pairs={{0,1},{1,2},{2,3},{3,0},{4,5},{5,6},{6,7},{7,4},{8,9},{9,10},{10,1... | collective-permute-start | bytes 1572872 | tf_op jit(solution)/shard_map/ppermute | solution.py:598
  246.7 27.4 %collective-permute-start.22 = (bf16[128,2048]{1,0:T(8,128)(2,1)}, bf16[128,2048]{1,0:T(8,128)(2,1)S(1)}, u32[]{:S(2)}, u32[]{:S(2)}) collective-permute-start(bf16[128,2048]{1,0:T(8,128)(2,1)} %get-tuple-element.59), channel_id=1, source_target_pairs={{0,2},{1,3},{2,0},{3,1},{4,6},{5,7},{6,4},{7,5},{8,10},{9,11},{10,... | collective-permute-start | bytes 1572872 | tf_op jit(solution)/shard_map/ppermute | solution.py:598
  248.3 26.4 %collective-permute-start.23 = (bf16[128,2048]{1,0:T(8,128)(2,1)}, bf16[128,2048]{1,0:T(8,128)(2,1)S(1)}, u32[]{:S(2)}, u32[]{:S(2)}) collective-permute-start(bf16[128,2048]{1,0:T(8,128)(2,1)} %get-tuple-element.60), channel_id=1, source_target_pairs={{0,3},{1,0},{2,1},{3,2},{4,7},{5,4},{6,5},{7,6},{8,11},{9,8},{10,9... | collective-permute-start | bytes 1572872 | tf_op jit(solution)/shard_map/ppermute | solution.py:598
  (47 other events, 331.3 us)

commit v2 on v1

--- a/solution.py
+++ b/solution.py
@@ -1,3 +1,5 @@
+import functools
+
 import jax
 import jax.numpy as jnp
 from jax import lax
@@ -91,7 +93,7 @@
     sent_refs, (maps_ref, total_ref, msg_ref) = rest_refs[:GROUPS], rest_refs[GROUPS:]
     step = pl.program_id(0)
     rows, channels = q_ref.shape
-    heads = shift_ref.shape[1]
+    heads = shift_ref.shape[0]
     pairs = heads // 2
     same = block_ones()
     same_f = same.astype(F32)
@@ -113,7 +115,7 @@
     pre = (
         di_ref[...].astype(F32)
         + base_ref[...]
-        + (dot(shift_high, spread) + dot(shift_low, spread))
+        + (dot_tn(shift_high, spread) + dot_tn(shift_low, spread))
     )
     log_decay = -DECAY_SCALE / (1.0 + jnp.exp(-pre))
     tri_rows, tri_cols = iota((rows, rows), 0), iota((rows, rows), 1)
@@ -295,34 +297,28 @@
     both = jnp.concatenate([eye * total - maps[:HEAD], maps[HEAD:]], axis=1).astype(BF16)
     high, rest = two_parts(jnp.broadcast_to(total, (16, HEAD)))
     ends = jnp.concatenate([high.astype(F32), rest.astype(F32)], axis=1).astype(BF16)
-    out_ref[:HEAD, :] = both
-    out_ref[HEAD:, :] = ends
-
-
-def enter_kernel(place_ref, *refs):
-    in_refs = refs[: GROUPS - 1]
-    prefix_ref = refs[GROUPS - 1]
-    sent_refs, made_ref = refs[GROUPS:-1], refs[-1]
+    for z in range(out_ref.shape[0]):
+        out_ref[z, :HEAD, :] = both
+        out_ref[z, HEAD:, :] = ends
+
+
+def enter_kernel(here_ref, in_ref, prefix_ref, out_ref):
     state = jnp.zeros((HEAD, HEAD), F32)
-    for s in range(GROUPS - 1, 0, -1):
-        lost, gained, fade = message_parts(in_refs[s - 1][...])
+    for z in range(in_ref.shape[0]):
+        lost, gained, fade = message_parts(in_ref[z])
         passed = state * fade - dot(state.astype(BF16), lost) + gained
-        state = jnp.where(s <= place_ref[0], passed, state)
+        state = jnp.where(z < here_ref[0], passed, state)
     narrow = state.astype(BF16)
-    for m in range(GROUPS):
+    for m in range(out_ref.shape[0]):
         entering = dot(narrow, prefix_ref[m, :HEAD, :].astype(BF16)) + prefix_ref[m, HEAD:, :]
-        made_ref[m] = jnp.concatenate([entering, entering], axis=1).astype(BF16)
-    for s in range(GROUPS):
-        sent_refs[s][...] = made_ref[lax.rem(place_ref[1] + s, GROUPS)]
-
-
-def readout_kernel(place_ref, *refs):
-    enter_refs = refs[:GROUPS]
-    reader_ref, local_ref, gather_ref, add_ref, fade_ref, gain_ref, weight_ref = refs[
-        GROUPS : GROUPS + 7
-    ]
-    out_refs = refs[GROUPS + 7 : -2]
-    state_ref, heads_ref = refs[-2:]
+        out_ref[m] = jnp.concatenate([entering, entering], axis=1).astype(BF16)
+
+
+def readout_kernel(
+    here_ref, enter_ref, reader_ref, local_ref, gather_ref, add_ref, fade_ref, gain_ref,
+    weight_ref, *refs,
+):
+    out_refs, state_ref = refs[:-1], refs[-1]
     step = pl.program_id(0)
     spans = len(out_refs)
     channels = reader_ref.shape[1]
@@ -332,10 +328,8 @@
 
     @pl.when(step == 0)
     def _():
-        for s in range(GROUPS):
-            heads_ref[lax.rem(place_ref[1] + GROUPS - s, GROUPS)] = enter_refs[s][...]
         for p in range(pairs):
-            entering = jnp.concatenate([heads_ref[2 * p], heads_ref[2 * p + 1]], axis=0)
+            entering = jnp.concatenate([enter_ref[2 * p], enter_ref[2 * p + 1]], axis=0)
             state_ref[p] = jnp.where(same, entering.astype(F32), 0.0)
 
     pieces = []
@@ -354,22 +348,42 @@
     result = dot(normed, weight_ref[...]).astype(BF16)
     for s in range(spans):
 
-        @pl.when(lax.rem(step + spans - place_ref[2], spans) == s)
+        @pl.when(lax.rem(step + spans - here_ref[0], spans) == s)
         def _():
             out_refs[s][...] = result
 
 
-def hidden_kernel(x_ref, gate_ref, up_ref, out_ref):
-    x = x_ref[...]
-    gates = dot(x, gate_ref[...])
-    uppers = dot(x, up_ref[...])
-    out_ref[...] = (gates / (1.0 + jnp.exp(-gates)) * uppers).astype(BF16)
-
-
-def down_kernel(h0, h1, h2, h3, own, before, after, far, out_ref):
-    units = jnp.concatenate([h0[...], h1[...], h2[...], h3[...]], axis=1)
-    weights = jnp.concatenate([own[...], before[...], after[...], far[...]], axis=0)
-    out_ref[...] = dot(units, weights).astype(BF16)
+def hidden_kernel(x_hbm, *refs):
+    weights, (out_ref, x_ref, weight_refs, sems) = refs[:8], refs[8:]
+    fetch_x = pltpu.make_async_copy(x_hbm, x_ref, sems.at[8])
+    fetch_x.start()
+    fetches = [
+        pltpu.make_async_copy(w, weight_refs.at[n], sems.at[n]) for n, w in enumerate(weights)
+    ]
+    for fetch in fetches:
+        fetch.start()
+    fetch_x.wait()
+    units = weight_refs.shape[2]
+    for q in range(4):
+        fetches[2 * q].wait()
+        gates = dot(x_ref[...], weight_refs[2 * q])
+        fetches[2 * q + 1].wait()
+        uppers = dot(x_ref[...], weight_refs[2 * q + 1])
+        out_ref[:, q * units : (q + 1) * units] = (
+            gates / (1.0 + jnp.exp(-gates)) * uppers
+        ).astype(BF16)
+
+
+def down_kernel(part, hidden_ref, own_hbm, before, after, far, out_ref, own_ref, sem):
+    units, width = before.shape
+    fetch = pltpu.make_async_copy(
+        own_hbm.at[:, part * width : (part + 1) * width], own_ref, sem
+    )
+    fetch.start()
+    others = jnp.concatenate([before[...], after[...], far[...]], axis=0)
+    result = dot(hidden_ref[:, units:], others)
+    fetch.wait()
+    out_ref[...] = (result + dot(hidden_ref[:, :units], own_ref[...])).astype(BF16)
 
 
 def pack_kernel(x_ref, gain_ref, routes_ref, mix_ref, out_ref, high_ref, rest_ref):
@@ -380,24 +394,24 @@
         x * lax.rsqrt(jnp.mean(x * x, axis=1, keepdims=True) + NORM_EPS) * gain_ref[...]
     ).astype(BF16)
     experts = places // CAPACITY
-    listed = iota((tokens, experts), 1)
-    first, second = routes_ref[:, 0:1], routes_ref[:, 1:2]
+    listed = iota((experts, tokens), 0)
+    first, second = routes_ref[0:1, :], routes_ref[1:2, :]
     first_mark = (first == listed).astype(F32)
     second_mark = (second == listed).astype(F32)
-    before = (iota((tokens, tokens), 0) > iota((tokens, tokens), 1)).astype(F32).astype(BF16)
-    earlier = dot(before, (first_mark + second_mark).astype(BF16))
-    columns = iota((tokens, places), 1)
-    table = jnp.zeros((tokens, places), F32)
-    mix = jnp.zeros((tokens, places), F32)
+    before = (iota((tokens, tokens), 0) < iota((tokens, tokens), 1)).astype(F32).astype(BF16)
+    earlier = dot((first_mark + second_mark).astype(BF16), before)
+    rows = iota((places, tokens), 0)
+    table = jnp.zeros((places, tokens), F32)
+    mix = jnp.zeros((places, tokens), F32)
     for named, mark, weight in (
-        (first, first_mark, mix_ref[:, 0:1]),
-        (second, second_mark, mix_ref[:, 1:2]),
+        (first, first_mark, mix_ref[0:1, :]),
+        (second, second_mark, mix_ref[1:2, :]),
     ):
-        slot = jnp.sum(earlier * mark, axis=1, keepdims=True).astype(jnp.int32)
-        here = columns == named * CAPACITY + slot
+        slot = jnp.sum(earlier * mark, axis=0, keepdims=True).astype(jnp.int32)
+        here = rows == named * CAPACITY + slot
         table = table + here.astype(F32)
         mix = jnp.where(here, weight, mix)
-    out_ref[...] = dot_tn(table.astype(BF16), normed).astype(BF16)
+    out_ref[...] = dot(table.astype(BF16), normed).astype(BF16)
     high, rest = two_parts(mix)
     high_ref[...] = high
     rest_ref[...] = rest
@@ -405,7 +419,7 @@
 
 def combine_kernel(high_ref, rest_ref, rows_ref, *refs):
     rows = rows_ref[...]
-    refs[-1][...] = (dot(high_ref[...], rows) + dot(rest_ref[...], rows)).astype(BF16)
+    refs[-1][...] = (dot_tn(high_ref[...], rows) + dot_tn(rest_ref[...], rows)).astype(BF16)
 
 
 def whole(shape):
@@ -423,7 +437,7 @@
 
 def summarize(here, q, k, v, di, li, base, shift):
     rows, channels = q.shape
-    heads = shift.shape[1]
+    heads = shift.shape[0]
     pairs = heads // 2
     spans = rows // SPAN
     block = pl.BlockSpec((SPAN, channels), lambda i: (i, 0))
@@ -433,7 +447,7 @@
         grid=(spans,),
         in_specs=[SCALARS]
         + [block] * 5
-        + [whole((1, channels)), pl.BlockSpec((SPAN, heads), lambda i: (i, 0))],
+        + [whole((1, channels)), pl.BlockSpec((heads, SPAN), lambda i: (0, i))],
         out_specs=[
             block,
             block,
@@ -461,32 +475,31 @@
     )(here, q, k, v, di, li, base, shift)
 
 
-def group_scan(here, messages):
+def group_scan(here, messages, copies):
     return pl.pallas_call(
         group_kernel,
         in_specs=[SCALARS] + [pl.BlockSpec(memory_space=pltpu.VMEM)] * GROUPS,
         out_shape=[
             jax.ShapeDtypeStruct((GROUPS, 2 * HEAD, HEAD), F32),
-            jax.ShapeDtypeStruct((MSG_ROWS, PAIR), BF16),
+            jax.ShapeDtypeStruct((copies, MSG_ROWS, PAIR), BF16),
         ],
         scratch_shapes=[pltpu.VMEM((GROUPS, MSG_ROWS, PAIR), BF16)],
         cost_estimate=estimate(2.0e9, 1 << 20),
         name="group_scan",
-    )(here, *messages)
-
-
-def enter_states(place, totals, prefixes):
+    )(here, *map(in_vmem, messages))
+
+
+def enter_states(here, totals, prefixes):
     return pl.pallas_call(
         enter_kernel,
-        in_specs=[SCALARS] + [pl.BlockSpec(memory_space=pltpu.VMEM)] * GROUPS,
-        out_shape=[jax.ShapeDtypeStruct((HEAD, PAIR), BF16)] * GROUPS,
-        scratch_shapes=[pltpu.VMEM((GROUPS, HEAD, PAIR), BF16)],
+        in_specs=[SCALARS] + [pl.BlockSpec(memory_space=pltpu.VMEM)] * 2,
+        out_shape=jax.ShapeDtypeStruct((prefixes.shape[0], HEAD, PAIR), BF16),
         cost_estimate=estimate(2.0e9, 1 << 20),
         name="enter_states",
-    )(place, *totals, prefixes)
-
-
-def read_and_project(place, entering, reader, local, gather, add, fade, gain, weight):
+    )(here, in_vmem(totals), prefixes)
+
+
+def read_and_project(here, entering, reader, local, gather, add, fade, gain, weight):
     rows, channels = reader.shape
     pairs = channels // PAIR
     spans = rows // SPAN
@@ -496,9 +509,9 @@
     return pl.pallas_call(
         readout_kernel,
         grid=(spans,),
-        in_specs=[SCALARS]
-        + [whole((HEAD, PAIR))] * GROUPS
-        + [
+        in_specs=[
+            SCALARS,
+            IN_VMEM,
             block,
             block,
             square,
@@ -509,52 +522,51 @@
         ],
         out_specs=[whole((SPAN, width))] * spans,
         out_shape=[jax.ShapeDtypeStruct((SPAN, width), BF16)] * spans,
-        scratch_shapes=[
-            pltpu.VMEM((pairs, PAIR, PAIR), F32),
-            pltpu.VMEM((2 * pairs, HEAD, PAIR), BF16),
-        ],
+        scratch_shapes=[pltpu.VMEM((pairs, PAIR, PAIR), F32)],
         compiler_params=pltpu.CompilerParams(dimension_semantics=("arbitrary",)),
         cost_estimate=estimate(5.0e9, 8 << 20),
         name="readout",
-    )(place, *entering, reader, local, gather, add, fade, gain, weight)
-
-
-def expert_hidden(x, gate, up):
+    )(here, in_vmem(entering), reader, local, gather, add, fade, gain, weight)
+
+
+IN_HBM = pl.BlockSpec(memory_space=pltpu.HBM)
+IN_VMEM = pl.BlockSpec(memory_space=pltpu.VMEM)
+
+
+def expert_hidden(x, weights):
     rows, width = x.shape
-    units = gate.shape[1]
-    tile = rows // 2
+    units = weights[0].shape[1]
+    count = len(weights)
     return pl.pallas_call(
         hidden_kernel,
-        grid=(2,),
-        in_specs=[
-            pl.BlockSpec((tile, width), lambda i: (i, 0)),
-            whole(gate.shape),
-            whole(up.shape),
+        in_specs=[IN_HBM] * (1 + count),
+        out_specs=IN_VMEM,
+        out_shape=jax.ShapeDtypeStruct((rows, units * count // 2), BF16),
+        scratch_shapes=[
+            pltpu.VMEM((rows, width), BF16),
+            pltpu.VMEM((count, width, units), BF16),
+            pltpu.SemaphoreType.DMA((count + 1,)),
         ],
-        out_specs=pl.BlockSpec((tile, units), lambda i: (i, 0)),
-        out_shape=jax.ShapeDtypeStruct((rows, units), BF16),
-        compiler_params=pltpu.CompilerParams(dimension_semantics=("arbitrary",)),
-        cost_estimate=estimate(4 * rows * width * units, 5 << 20, rows * units),
+        cost_estimate=estimate(2 * rows * width * units * count, 11 << 20, rows * units * 4),
         name="hidden",
-    )(x, gate, up)
-
-
-def expert_down(hiddens, own, others, part):
-    rows, units = hiddens[0].shape
-    width = others[0].shape[1]
-    tile = width // 2
+    )(pltpu.with_memory_space_constraint(x, pltpu.HBM), *weights)
+
+
+def expert_down(hidden, own, others, part):
+    rows = hidden.shape[0]
+    units, width = others[0].shape
     return pl.pallas_call(
-        down_kernel,
-        grid=(2,),
-        in_specs=[whole(h.shape) for h in hiddens]
-        + [pl.BlockSpec((units, tile), lambda i: (0, i + 2 * part))]
-        + [pl.BlockSpec((units, tile), lambda i: (0, i))] * 3,
-        out_specs=pl.BlockSpec((rows, tile), lambda i: (0, i)),
+        functools.partial(down_kernel, part),
+        in_specs=[IN_VMEM, IN_HBM] + [IN_VMEM] * 3,
+        out_specs=IN_VMEM,
         out_shape=jax.ShapeDtypeStruct((rows, width), BF16),
-        compiler_params=pltpu.CompilerParams(dimension_semantics=("arbitrary",)),
+        scratch_shapes=[
+            pltpu.VMEM((units, width), BF16),
+            pltpu.SemaphoreType.DMA,
+        ],
         cost_estimate=estimate(8 * rows * units * width, 4 << 20),
         name="down",
-    )(*hiddens, own, *others)
+    )(hidden, own, *map(in_vmem, others))
 
 
 def pack_rows(x, gain, routes, mix, places):
@@ -563,8 +575,8 @@
         pack_kernel,
         out_shape=[
             jax.ShapeDtypeStruct((places, width), BF16),
-            jax.ShapeDtypeStruct((tokens, places), BF16),
-            jax.ShapeDtypeStruct((tokens, places), BF16),
+            jax.ShapeDtypeStruct((places, tokens), BF16),
+            jax.ShapeDtypeStruct((places, tokens), BF16),
         ],
         cost_estimate=estimate(2.0e9, 3 << 20),
         name="pack",
@@ -572,25 +584,19 @@
 
 
 def combine_rows(high, rest, rows, part, into=()):
-    tokens, places = high.shape
+    _, tokens = high.shape
     width = rows.shape[1]
-    tile = width // 2
     return pl.pallas_call(
         combine_kernel,
-        grid=(2,),
-        in_specs=[
-            whole(high.shape),
-            whole(rest.shape),
-            pl.BlockSpec((places, tile), lambda i: (0, i)),
-        ]
-        + [pl.BlockSpec(memory_space=pl.ANY)] * len(into),
-        out_specs=pl.BlockSpec((tokens, tile), lambda i: (0, i + 2 * part)),
+        grid=(1,),
+        in_specs=[IN_VMEM] * 3 + [IN_HBM] * len(into),
+        out_specs=pl.BlockSpec((tokens, width), lambda i: (0, part)),
         out_shape=jax.ShapeDtypeStruct((tokens, 2 * width), BF16),
         input_output_aliases={3: 0} if into else {},
         compiler_params=pltpu.CompilerParams(dimension_semantics=("arbitrary",)),
         cost_estimate=estimate(1.0e9, 3 << 20),
         name="combine",
-    )(high, rest, rows, *into)
+    )(high, rest, in_vmem(rows), *into)
 
 
 def ring(x, shift, axis="tp"):
@@ -598,13 +604,12 @@
     return lax.ppermute(x, axis, [(i, (i + shift) % count) for i in range(count)])
 
 
-def onward(x, shift, axis):
-    count = lax.axis_size(axis)
-    return lax.ppermute(x, axis, [(i, i + shift) for i in range(count - shift)])
-
-
 def around(parts, axis):
     return [parts[0]] + [ring(part, n, axis) for n, part in enumerate(parts) if n]
+
+
+def in_vmem(x):
+    return pltpu.with_memory_space_constraint(x, pltpu.VMEM)
 
 
 def exchange(x, axis):
@@ -647,31 +652,32 @@
     down_0f, down_1f = ring(down_0r, 1), ring(down_1l, -1)
 
     outgoing, high, rest = pack_rows(
-        expert_input, expert_gain.reshape(1, -1), routes, route_weight, places
+        expert_input, expert_gain.reshape(1, -1), routes.T, route_weight.T, places
     )
     arrived = exchange(
         outgoing.reshape(experts, CAPACITY, model_width), EP
     ).reshape(places, model_width)
 
-    place = jnp.stack(
-        [lax.axis_index("ep_0"), lax.axis_index(GROUP), lax.axis_index("tp")]
-    ).astype(jnp.int32)
+    def here(axis):
+        return lax.axis_index(axis).astype(jnp.int32).reshape(1)
+
     reader, local, gather, add, fade, *messages = summarize(
-        place[1:2],
+        here(GROUP),
         receptance,
         key_rows,
         value_rows,
         decay_input,
         learn_input,
         decay_base.reshape(1, -1),
-        decay_shift,
-    )
-    prefixes, total = group_scan(place[1:2], around(messages, GROUP))
-    totals = [onward(total, n, "ep_0") for n in range(1, GROUPS)]
-    entered = enter_states(place, totals, prefixes)
+        decay_shift.T,
+    )
+    prefixes, totals = group_scan(
+        here(GROUP), around(messages, GROUP), lax.axis_size("ep_0")
+    )
+    entered = enter_states(here("ep_0"), exchange(totals, "ep_0"), prefixes)
     partial = read_and_project(
-        place,
-        around(entered, GROUP),
+        here("tp"),
+        exchange(entered, GROUP),
         reader,
         local,
         gather,
@@ -683,9 +689,9 @@
     shares = around(partial, "tp")
     mixer_out = sum(share.astype(F32) for share in shares).astype(BF16)
 
-    hiddens = []
-    for g, u in ((w_gate, w_up), (gate_r, up_r), (gate_l, up_l), (gate_f, up_f)):
-        hiddens.append(expert_hidden(arrived, g, u))
+    hiddens = expert_hidden(
+        arrived, [w_gate, w_up, gate_r, up_r, gate_l, up_l, gate_f, up_f]
+    )
     combined = ()
     for n, others in enumerate(((down_0r, down_0l, down_0f), (down_1r, down_1l, down_1f))):
         returning = expert_down(hiddens, w_down, others, n)

time: 284 us -> 231 us (0.81)
  starting transfers between devices: 96.1 us -> 65 us
  local copies, waits for them, and re-layouts: 9.9 us -> 0.91 us
  waiting for transfers between devices: 107 us -> 99 us
  Pallas kernels: 66.2 us -> 62.6 us
    ppermute x7 -> x0, starting transfers between devices: 26.9 us -> none  [onward(): return lax.ppermute(x, axis, [(i, i + shift) for i in range(count - shift)])]
    ppermute x29 -> x22, starting transfers between devices: 36.9 us -> 24.1 us  [ring(): lax.ppermute(x, axis, [(i, (i + shift) % count) for i in range(count)])]
    ppermute x29 -> x22, waiting for transfers between devices: 99.6 us -> 89.8 us  [ring(): lax.ppermute(x, axis, [(i, (i + shift) % count) for i in range(count)])]
    all_to_all x3 -> x5, waiting for transfers between devices: 0.01 us -> 9.26 us  [exchange(): return lax.all_to_all(x, axis, 0, 0, tiled=True)]
    unnamed x67 -> x6, local copies, waits for them, and re-layouts: 8.84 us -> 0.01 us
    all_to_all x3 -> x5, starting transfers between devices: 32.3 us -> 40.9 us  [exchange(): return lax.all_to_all(x, axis, 0, 0, tiled=True)]
    ppermute x7 -> x0, waiting for transfers between devices: 7.02 us -> none  [onward(): return lax.ppermute(x, axis, [(i, i + shift) for i in range(count - shift)])]
    pallas_call x9 -> x6, Pallas kernels: 37.7 us -> 35.1 us  [the longest x1 12.8 us: expert_hidden(): pl.pallas_call(hidden_kernel, in_specs=[IN_HBM] * (1 + count), out_specs=...]
  transfers between devices with their start and end apart: 39 -> 27, of which waited for: 10 -> 12; matrix products, arithmetic and copies ran while one was open for 2% -> 1% of each run, Pallas kernels for 21% -> 25%
where the time goes in v2:
time: 231 us
  waiting for transfers between devices  99 us (43%)
  starting transfers between devices  65 us (28%)
  Pallas kernels  62.6 us (27%)
    ppermute x22, waiting for transfers between devices, ring(): lax.ppermute(x, axis, [(i, (i + shift) % count) for i in range(count)])  89.8 us
    all_to_all x5, starting transfers between devices, exchange(): return lax.all_to_all(x, axis, 0, 0, tiled=True)  40.9 us
    ppermute x22, starting transfers between devices, ring(): lax.ppermute(x, axis, [(i, (i + shift) % count) for i in range(count)])  24.1 us
    pallas_call x1, Pallas kernels, summarize(): pl.pallas_call(summary_kernel, grid=(spans,), in_specs=[SCALARS] + [block...  19.6 us
    pallas_call x1, Pallas kernels, expert_hidden(): pl.pallas_call(hidden_kernel, in_specs=[IN_HBM] * (1 + count), out_specs=...  12.8 us
    all_to_all x5, waiting for transfers between devices, exchange(): return lax.all_to_all(x, axis, 0, 0, tiled=True)  9.26 us
    pallas_call x2, Pallas kernels, expert_down(): pl.pallas_call(functools.partial(down_kernel, part), in_specs=[IN_VMEM, I...  9.2 us
    pallas_call x1, Pallas kernels, read_and_project(): pl.pallas_call(readout_kernel, grid=(spans,), in_specs=[SCALARS, IN_VMEM,...  8.87 us
  transfers between devices with their start and end apart: 27, of which 12 were waited for; matrix products, arithmetic and copies ran while one was open for 1% of the time, Pallas kernels for 25%

profile of v2, /device:TPU:2, one launch (start us, length us, event | category | flops | bytes accessed | tf_op | source)
XLA Modules:
  0.0 230.6 jit_solution(17830168688078382696)
XLA Ops:
  0.6 3.3 %pack.1 = (bf16[512,2048]{1,0:T(8,128)(2,1)}, bf16[512,128]{1,0:T(8,128)(2,1)}, bf16[512,128]{1,0:T(8,128)(2,1)}) custom-call(bf16[128,2048]{1,0:T(8,128)(2,1)} %x_ref.1, f32[1,2048]{1,0:T(1,128)} %bitcast.30, s32[2,128]{1,0:T(2,128)} %bitcast.33, f32[2,128]{1,0:T(2,128)} %bitcast.34), custom_call_target="tpu_custom_call" | custom-call | flops 2000000000 | bytes 3145728 | tf_op jit(solution)/shard_map/pack/pallas_call | solution.py:574
  4.0 12.3 %all-to-all-start.2 = ((bf16[64,8,2048]{2,1,0:T(8,128)(2,1)}), bf16[64,8,2048]{2,1,0:T(8,128)(2,1)}, u32[]{:S(2)}, u32[]{:S(2)}) async-start(bf16[64,8,2048]{2,1,0:T(8,128)(2,1)} %bitcast.25), calls=%async_computation.2 | async-start | bytes 4194304 | tf_op jit(solution)/shard_map/all_to_all | solution.py:616
  16.3 3.1 %collective-permute-start.13 = (bf16[2048,256]{1,0:T(8,128)(2,1)S(1)}, bf16[2048,256]{1,0:T(8,128)(2,1)}, u32[]{:S(2)}, u32[]{:S(2)}) collective-permute-start(bf16[2048,256]{1,0:T(8,128)(2,1)S(1)} %bitcast.27), channel_id=1, source_target_pairs={{0,3},{1,0},{2,1},{3,2},{4,7},{5,4},{6,5},{7,6},{8,11},{9,8},{10,9... | collective-permute-start | bytes 3145736 | tf_op jit(solution)/shard_map/ppermute | solution.py:604
  20.0 19.6 %summary.1 = (bf16[512,512]{1,0:T(8,128)(2,1)}, f32[512,512]{1,0:T(8,128)}, bf16[4,4,128,128]{3,2,1,0:T(8,128)(2,1)}, f32[4,4,128,128]{3,2,1,0:T(8,128)}, f32[4,...) custom-call(s32[1]{0:T(128)} %bitcast.2.here_ref, ...), custom_call_target="tpu_custom_call" | custom-call | flops 20000000000 | bytes 6291456 | tf_op jit(solution)/shard_map/summary/pallas_call | solution.py:445
  43.8 2.6 %collective-permute-start.12 = (bf16[2048,256]{1,0:T(8,128)(2,1)}, bf16[2048,256]{1,0:T(8,128)(2,1)}, u32[]{:S(2)}, u32[]{:S(2)}) collective-permute-start(bf16[2048,256]{1,0:T(8,128)(2,1)} %bitcast.11.refs_0_), channel_id=1, source_target_pairs={{0,3},{1,0},{2,1},{3,2},{4,7},{5,4},{6,5},{7,6},{8,11},{9,8},{10,9... | collective-permute-start | bytes 3145736 | tf_op jit(solution)/shard_map/ppermute | solution.py:604
  46.4 21.7 %collective-permute-done.10.refs_2_ = bf16[2048,256]{1,0:T(8,128)(2,1)} collective-permute-done((bf16[2048,256]{1,0:T(8,128)(2,1)}, bf16[2048,256]{1,0:T(8,128)(2,1)}, u32[]{:S(2)}, u32[]{:S(2)}) %collective-permute-start.10) | collective-permute-done | bytes 1048608 | tf_op jit(solution)/shard_map/ppermute | solution.py:604
  68.1 3.2 %collective-permute-start.15 = (bf16[2048,256]{1,0:T(8,128)(2,1)}, bf16[2048,256]{1,0:T(8,128)(2,1)}, u32[]{:S(2)}, u32[]{:S(2)}) collective-permute-start(bf16[2048,256]{1,0:T(8,128)(2,1)} %collective-permute-done.13.refs_5_), channel_id=1, source_target_pairs={{0,3},{1,0},{2,1},{3,2},{4,7},{5,4},{6,5},{7,6},{8,11},{9,8},{10,9... | collective-permute-start | bytes 3145736 | tf_op jit(solution)/shard_map/ppermute | solution.py:604
  73.4 3.4 %collective-permute-done.3.refs_4_ = bf16[80,128]{1,0:T(8,128)(2,1)S(1)} collective-permute-done((bf16[80,128]{1,0:T(8,128)(2,1)}, bf16[80,128]{1,0:T(8,128)(2,1)S(1)}, u32[]{:S(2)}, u32[]{:S(2)}) %collective-permute-start.3) | collective-permute-done | bytes 20512 | tf_op jit(solution)/shard_map/ppermute | solution.py:604
  76.9 3.4 %collective-permute-done.4.refs_5_ = bf16[80,128]{1,0:T(8,128)(2,1)S(1)} collective-permute-done((bf16[80,128]{1,0:T(8,128)(2,1)}, bf16[80,128]{1,0:T(8,128)(2,1)S(1)}, u32[]{:S(2)}, u32[]{:S(2)}) %collective-permute-start.4) | collective-permute-done | bytes 20512 | tf_op jit(solution)/shard_map/ppermute | solution.py:604
  80.7 3.7 %collective-permute-done.5.refs_6_ = bf16[80,128]{1,0:T(8,128)(2,1)S(1)} collective-permute-done((bf16[80,128]{1,0:T(8,128)(2,1)}, bf16[80,128]{1,0:T(8,128)(2,1)S(1)}, u32[]{:S(2)}, u32[]{:S(2)}) %collective-permute-start.5) | collective-permute-done | bytes 20512 | tf_op jit(solution)/shard_map/ppermute | solution.py:604
  86.7 18.1 %collective-permute-done.19.before = bf16[256,1024]{1,0:T(8,128)(2,1)S(1)} collective-permute-done((bf16[256,1024]{1,0:T(8,128)(2,1)S(1)}, bf16[256,1024]{1,0:T(8,128)(2,1)S(1)}, u32[]{:S(2)}, u32[]{:S(2)}) %collective-permute-start.19) | collective-permute-done | bytes 524320 | tf_op jit(solution)/shard_map/ppermute | solution.py:604
  108.6 6.8 %all-to-all-start = ((bf16[8,80,128]{2,1,0:T(8,128)(2,1)}), bf16[8,80,128]{2,1,0:T(8,128)(2,1)S(1)}, u32[]{:S(2)}, u32[]{:S(2)}) async-start(bf16[8,80,128]{2,1,0:T(8,128)(2,1)} %get-tuple-element.34), calls=%async_computation | async-start | bytes 327680 | tf_op jit(solution)/shard_map/all_to_all | solution.py:616
  115.4 12.8 %hidden.1.hidden_ref = bf16[512,1024]{1,0:T(8,128)(2,1)} custom-call(bf16[512,2048]{1,0:T(8,128)(2,1)} %bitcast.10.x_hbm, bf16[2048,256]{1,0:T(8,128)(2,1)} %bitcast.11.refs_0_, bf16[2048,256]{1,0:T(8,128)(2,1)} %bitcast.26, bf16[2048,256]{1,0:T(8,128)(2,1)} %collective-permute-done.10.refs_2_, bf16[2048,256]{1,0:T(8,128)(2,1)} %collective-permute-done.11.refs_3_, ...), custom_call_target="tpu_custom_call" | custom-call | flops 4294967296 | bytes 11534336 | tf_op jit(solution)/shard_map/hidden/pallas_call | solution.py:540
  128.2 4.6 %down.3 = bf16[512,1024]{1,0:T(8,128)(2,1)} custom-call(bf16[512,1024]{1,0:T(8,128)(2,1)} %hidden.1.hidden_ref, bf16[256,2048]{1,0:T(8,128)(2,1)} %bitcast.20, bf16[256,1024]{1,0:T(8,128)(2,1)S(1)} %collective-permute-done.19.before, bf16[256,1024]{1,0:T(8,128)(2,1)S(1)} %collective-permute-done.20.after, bf16[256,1024]{1,0:T(8,128)(2,1)S(1)} %collective-permute-done.21.far), custom_call_target="tpu_custom_call" | custom-call | flops 1073741824 | bytes 4194304 | tf_op jit(solution)/shard_map/down/pallas_call | solution.py:558
  132.8 10.5 %all-to-all-start.3 = ((bf16[64,8,1024]{2,1,0:T(8,128)(2,1)}), bf16[64,8,1024]{2,1,0:T(8,128)(2,1)S(1)}, u32[]{:S(2)}, u32[]{:S(2)}) async-start(bf16[64,8,1024]{2,1,0:T(8,128)(2,1)} %bitcast.24), calls=%async_computation.3 | async-start | bytes 2097152 | tf_op jit(solution)/shard_map/all_to_all | solution.py:616
  145.4 12.1 %collective-permute-done.17.after = bf16[256,1024]{1,0:T(8,128)(2,1)S(1)} collective-permute-done((bf16[256,1024]{1,0:T(8,128)(2,1)}, bf16[256,1024]{1,0:T(8,128)(2,1)S(1)}, u32[]{:S(2)}, u32[]{:S(2)}) %collective-permute-start.17) | collective-permute-done | bytes 524320 | tf_op jit(solution)/shard_map/ppermute | solution.py:604
  159.9 2.9 %enter_states.1 = bf16[8,64,128]{2,1,0:T(8,128)(2,1)} custom-call(s32[1]{0:T(128)} %bitcast.1.here_ref, bf16[8,80,128]{2,1,0:T(8,128)(2,1)S(1)} %all-to-all-done.in_ref, f32[8,128,64]{2,1,0:T(8,128)} %get-tuple-element.35.prefix_ref), custom_call_target="tpu_custom_call" | custom-call | flops 2000000000 | bytes 1048576 | tf_op jit(solution)/shard_map/enter_states/pallas_call | solution.py:493
  162.8 9.2 %all-to-all-done.3 = bf16[64,8,1024]{2,1,0:T(8,128)(2,1)S(1)} async-done(((bf16[64,8,1024]{2,1,0:T(8,128)(2,1)}), bf16[64,8,1024]{2,1,0:T(8,128)(2,1)S(1)}, u32[]{:S(2)}, u32[]{:S(2)}) %all-to-all-start.3) | async-done | bytes 1048608 | tf_op jit(solution)/shard_map/all_to_all | solution.py:616
  172.0 4.8 %all-to-all-start.1 = ((bf16[8,64,128]{2,1,0:T(8,128)(2,1)}), bf16[8,64,128]{2,1,0:T(8,128)(2,1)S(1)}, u32[]{:S(2)}, u32[]{:S(2)}) async-start(bf16[8,64,128]{2,1,0:T(8,128)(2,1)} %enter_states.1), calls=%async_computation.1 | async-start | bytes 262144 | tf_op jit(solution)/shard_map/all_to_all | solution.py:616
  176.9 4.6 %down.2 = bf16[512,1024]{1,0:T(8,128)(2,1)} custom-call(bf16[512,1024]{1,0:T(8,128)(2,1)} %hidden.1.hidden_ref, bf16[256,2048]{1,0:T(8,128)(2,1)} %bitcast.21, bf16[256,1024]{1,0:T(8,128)(2,1)S(1)} %collective-permute-done.16.before, bf16[256,1024]{1,0:T(8,128)(2,1)S(1)} %collective-permute-done.17.after, bf16[256,1024]{1,0:T(8,128)(2,1)S(1)} %collective-permute-done.18.far), custom_call_target="tpu_custom_call" | custom-call | flops 1073741824 | bytes 4194304 | tf_op jit(solution)/shard_map/down/pallas_call | solution.py:558
  181.5 6.5 %all-to-all-start.4 = ((bf16[64,8,1024]{2,1,0:T(8,128)(2,1)}), bf16[64,8,1024]{2,1,0:T(8,128)(2,1)S(1)}, u32[]{:S(2)}, u32[]{:S(2)}) async-start(bf16[64,8,1024]{2,1,0:T(8,128)(2,1)} %bitcast.23), calls=%async_computation.4 | async-start | bytes 2097152 | tf_op jit(solution)/shard_map/all_to_all | solution.py:616
  188.0 8.9 %readout.1 = (bf16[128,2048]{1,0:T(8,128)(2,1)}, bf16[128,2048]{1,0:T(8,128)(2,1)}, bf16[128,2048]{1,0:T(8,128)(2,1)}, bf16[128,2048]{1,0:T(8,128)(2,1)}) custom-call(s32[1]{0:T(128)} %bitcast.here_ref, bf16[8,64,128]{2,1,0:T(8,128)(2,1)S(1)} %all-to-all-done.1.enter_ref, bf16[512,512]{1,0:T(8,128)(2,1)} %get-tuple-element.36.reader_ref, ...), custom_call_target="tpu_custom_call" | custom-call | flops 5000000000 | bytes 8388608 | tf_op jit(solution)/shard_map/readout/pallas_call | solution.py:509
  196.9 2.7 %collective-permute-start.8 = (bf16[128,2048]{1,0:T(8,128)(2,1)}, bf16[128,2048]{1,0:T(8,128)(2,1)S(1)}, u32[]{:S(2)}, u32[]{:S(2)}) collective-permute-start(bf16[128,2048]{1,0:T(8,128)(2,1)} %get-tuple-element.43), channel_id=1, source_target_pairs={{0,2},{1,3},{2,0},{3,1},{4,6},{5,7},{6,4},{7,5},{8,10},{9,11},{10,... | collective-permute-start | bytes 1572872 | tf_op jit(solution)/shard_map/ppermute | solution.py:604
  200.1 23.4 %collective-permute-done.7 = bf16[128,2048]{1,0:T(8,128)(2,1)S(1)} collective-permute-done((bf16[128,2048]{1,0:T(8,128)(2,1)}, bf16[128,2048]{1,0:T(8,128)(2,1)S(1)}, u32[]{:S(2)}, u32[]{:S(2)}) %collective-permute-start.7) | collective-permute-done | bytes 524320 | tf_op jit(solution)/shard_map/ppermute | solution.py:604
  (48 shorter events, 25.6 us)
Async XLA Ops:
  4.0 104.6 %all-to-all-start.2 = ((bf16[64,8,2048]{2,1,0:T(8,128)(2,1)}), bf16[64,8,2048]{2,1,0:T(8,128)(2,1)}, u32[]{:S(2)}, u32[]{:S(2)}) async-start(bf16[64,8,2048]{2,1,0:T(8,128)(2,1)} %bitcast.25), calls=%async_computation.2 | async-start | bytes 4194304 | tf_op jit(solution)/shard_map/all_to_all | solution.py:616
  16.3 51.8 %collective-permute-start.13 = (bf16[2048,256]{1,0:T(8,128)(2,1)S(1)}, bf16[2048,256]{1,0:T(8,128)(2,1)}, u32[]{:S(2)}, u32[]{:S(2)}) collective-permute-start(bf16[2048,256]{1,0:T(8,128)(2,1)S(1)} %bitcast.27), channel_id=1, source_target_pairs={{0,3},{1,0},{2,1},{3,2},{4,7},{5,4},{6,5},{7,6},{8,11},{9,8},{10,9... | collective-permute-start | bytes 3145736 | tf_op jit(solution)/shard_map/ppermute | solution.py:604
  19.4 85.4 %collective-permute-start.11 = (bf16[2048,256]{1,0:T(8,128)(2,1)S(1)}, bf16[2048,256]{1,0:T(8,128)(2,1)}, u32[]{:S(2)}, u32[]{:S(2)}) collective-permute-start(bf16[2048,256]{1,0:T(8,128)(2,1)S(1)} %bitcast.28), channel_id=1, source_target_pairs={{0,1},{1,2},{2,3},{3,0},{4,5},{5,6},{6,7},{7,4},{8,9},{9,10},{10,1... | collective-permute-start | bytes 3145736 | tf_op jit(solution)/shard_map/ppermute | solution.py:604
  19.4 48.7 %collective-permute-start.10 = (bf16[2048,256]{1,0:T(8,128)(2,1)}, bf16[2048,256]{1,0:T(8,128)(2,1)}, u32[]{:S(2)}, u32[]{:S(2)}) collective-permute-start(bf16[2048,256]{1,0:T(8,128)(2,1)} %bitcast.11.refs_0_), channel_id=1, source_target_pairs={{0,1},{1,2},{2,3},{3,0},{4,5},{5,6},{6,7},{7,4},{8,9},{9,10},{10,1... | collective-permute-start | bytes 3145736 | tf_op jit(solution)/shard_map/ppermute | solution.py:604
  39.6 4.1 %collective-permute-start.1 = (bf16[80,128]{1,0:T(8,128)(2,1)}, bf16[80,128]{1,0:T(8,128)(2,1)S(1)}, u32[]{:S(2)}, u32[]{:S(2)}) collective-permute-start(bf16[80,128]{1,0:T(8,128)(2,1)} %get-tuple-element.28), channel_id=1, source_target_pairs={{0,8},{4,12},{8,16},{12,20},{16,24},{20,28},{24,0},{28,4},{1,9},{5... | collective-permute-start | bytes 61448 | tf_op jit(solution)/shard_map/ppermute | solution.py:604
  43.0 28.3 %collective-permute-start.2 = (bf16[80,128]{1,0:T(8,128)(2,1)}, bf16[80,128]{1,0:T(8,128)(2,1)S(1)}, u32[]{:S(2)}, u32[]{:S(2)}) collective-permute-start(bf16[80,128]{1,0:T(8,128)(2,1)} %get-tuple-element.29), channel_id=1, source_target_pairs={{0,12},{4,16},{8,20},{12,24},{16,28},{20,0},{24,4},{28,8},{1,13},{... | collective-permute-start | bytes 61448 | tf_op jit(solution)/shard_map/ppermute | solution.py:604
  43.8 71.6 %collective-permute-start.12 = (bf16[2048,256]{1,0:T(8,128)(2,1)}, bf16[2048,256]{1,0:T(8,128)(2,1)}, u32[]{:S(2)}, u32[]{:S(2)}) collective-permute-start(bf16[2048,256]{1,0:T(8,128)(2,1)} %bitcast.11.refs_0_), channel_id=1, source_target_pairs={{0,3},{1,0},{2,1},{3,2},{4,7},{5,4},{6,5},{7,6},{8,11},{9,8},{10,9... | collective-permute-start | bytes 3145736 | tf_op jit(solution)/shard_map/ppermute | solution.py:604
  68.1 47.3 %collective-permute-start.14 = (bf16[2048,256]{1,0:T(8,128)(2,1)}, bf16[2048,256]{1,0:T(8,128)(2,1)}, u32[]{:S(2)}, u32[]{:S(2)}) collective-permute-start(bf16[2048,256]{1,0:T(8,128)(2,1)} %collective-permute-done.10.refs_2_), channel_id=1, source_target_pairs={{0,1},{1,2},{2,3},{3,0},{4,5},{5,6},{6,7},{7,4},{8,9},{9,10},{10,1... | collective-permute-start | bytes 3145736 | tf_op jit(solution)/shard_map/ppermute | solution.py:604
  68.1 47.3 %collective-permute-start.15 = (bf16[2048,256]{1,0:T(8,128)(2,1)}, bf16[2048,256]{1,0:T(8,128)(2,1)}, u32[]{:S(2)}, u32[]{:S(2)}) collective-permute-start(bf16[2048,256]{1,0:T(8,128)(2,1)} %collective-permute-done.13.refs_5_), channel_id=1, source_target_pairs={{0,3},{1,0},{2,1},{3,2},{4,7},{5,4},{6,5},{7,6},{8,11},{9,8},{10,9... | collective-permute-start | bytes 3145736 | tf_op jit(solution)/shard_map/ppermute | solution.py:604
  71.4 5.5 %collective-permute-start.3 = (bf16[80,128]{1,0:T(8,128)(2,1)}, bf16[80,128]{1,0:T(8,128)(2,1)S(1)}, u32[]{:S(2)}, u32[]{:S(2)}) collective-permute-start(bf16[80,128]{1,0:T(8,128)(2,1)} %get-tuple-element.30), channel_id=1, source_target_pairs={{0,16},{4,20},{8,24},{12,28},{16,0},{20,4},{24,8},{28,12},{1,17},{... | collective-permute-start | bytes 61448 | tf_op jit(solution)/shard_map/ppermute | solution.py:604
  80.3 4.1 %collective-permute-start.5 = (bf16[80,128]{1,0:T(8,128)(2,1)}, bf16[80,128]{1,0:T(8,128)(2,1)S(1)}, u32[]{:S(2)}, u32[]{:S(2)}) collective-permute-start(bf16[80,128]{1,0:T(8,128)(2,1)} %get-tuple-element.32), channel_id=1, source_target_pairs={{0,24},{4,28},{8,0},{12,4},{16,8},{20,12},{24,16},{28,20},{1,25},{... | collective-permute-start | bytes 61448 | tf_op jit(solution)/shard_map/ppermute | solution.py:604
  86.7 18.1 %collective-permute-start.19 = (bf16[256,1024]{1,0:T(8,128)(2,1)S(1)}, bf16[256,1024]{1,0:T(8,128)(2,1)S(1)}, u32[]{:S(2)}, u32[]{:S(2)}) collective-permute-start(bf16[256,1024]{1,0:T(8,128)(2,1)S(1)} %get-tuple-element.50), channel_id=1, source_target_pairs={{0,1},{1,2},{2,3},{3,0},{4,5},{5,6},{6,7},{7,4},{8,9},{9,10},{10,1... | collective-permute-start | bytes 1572872 | tf_op jit(solution)/shard_map/ppermute | solution.py:604
  104.8 23.3 %collective-permute-start.20 = (bf16[256,1024]{1,0:T(8,128)(2,1)S(1)}, bf16[256,1024]{1,0:T(8,128)(2,1)S(1)}, u32[]{:S(2)}, u32[]{:S(2)}) collective-permute-start(bf16[256,1024]{1,0:T(8,128)(2,1)S(1)} %get-tuple-element.50), channel_id=1, source_target_pairs={{0,3},{1,0},{2,1},{3,2},{4,7},{5,4},{6,5},{7,6},{8,11},{9,8},{10,9... | collective-permute-start | bytes 1572872 | tf_op jit(solution)/shard_map/ppermute | solution.py:604
  104.8 23.4 %collective-permute-start.21 = (bf16[256,1024]{1,0:T(8,128)(2,1)S(1)}, bf16[256,1024]{1,0:T(8,128)(2,1)S(1)}, u32[]{:S(2)}, u32[]{:S(2)}) collective-permute-start(bf16[256,1024]{1,0:T(8,128)(2,1)S(1)} %collective-permute-done.19.before), channel_id=1, source_target_pairs={{0,1},{1,2},{2,3},{3,0},{4,5},{5,6},{6,7},{7,4},{8,9},{9,10},{10,1... | collective-permute-start | bytes 1572872 | tf_op jit(solution)/shard_map/ppermute | solution.py:604
  108.6 24.2 %all-to-all-start = ((bf16[8,80,128]{2,1,0:T(8,128)(2,1)}), bf16[8,80,128]{2,1,0:T(8,128)(2,1)S(1)}, u32[]{:S(2)}, u32[]{:S(2)}) async-start(bf16[8,80,128]{2,1,0:T(8,128)(2,1)} %get-tuple-element.34), calls=%async_computation | async-start | bytes 327680 | tf_op jit(solution)/shard_map/all_to_all | solution.py:616
  132.8 39.2 %all-to-all-start.3 = ((bf16[64,8,1024]{2,1,0:T(8,128)(2,1)}), bf16[64,8,1024]{2,1,0:T(8,128)(2,1)S(1)}, u32[]{:S(2)}, u32[]{:S(2)}) async-start(bf16[64,8,1024]{2,1,0:T(8,128)(2,1)} %bitcast.24), calls=%async_computation.3 | async-start | bytes 2097152 | tf_op jit(solution)/shard_map/all_to_all | solution.py:616
  143.3 14.2 %collective-permute-start.17 = (bf16[256,1024]{1,0:T(8,128)(2,1)}, bf16[256,1024]{1,0:T(8,128)(2,1)S(1)}, u32[]{:S(2)}, u32[]{:S(2)}) collective-permute-start(bf16[256,1024]{1,0:T(8,128)(2,1)} %get-tuple-element.51), channel_id=1, source_target_pairs={{0,3},{1,0},{2,1},{3,2},{4,7},{5,4},{6,5},{7,6},{8,11},{9,8},{10,9... | collective-permute-start | bytes 1572872 | tf_op jit(solution)/shard_map/ppermute | solution.py:604
  144.6 32.3 %collective-permute-start.16 = (bf16[256,1024]{1,0:T(8,128)(2,1)}, bf16[256,1024]{1,0:T(8,128)(2,1)S(1)}, u32[]{:S(2)}, u32[]{:S(2)}) collective-permute-start(bf16[256,1024]{1,0:T(8,128)(2,1)} %get-tuple-element.51), channel_id=1, source_target_pairs={{0,1},{1,2},{2,3},{3,0},{4,5},{5,6},{6,7},{7,4},{8,9},{9,10},{10,1... | collective-permute-start | bytes 1572872 | tf_op jit(solution)/shard_map/ppermute | solution.py:604
  157.5 19.4 %collective-permute-start.18 = (bf16[256,1024]{1,0:T(8,128)(2,1)S(1)}, bf16[256,1024]{1,0:T(8,128)(2,1)S(1)}, u32[]{:S(2)}, u32[]{:S(2)}) collective-permute-start(bf16[256,1024]{1,0:T(8,128)(2,1)S(1)} %collective-permute-done.17.after), channel_id=1, source_target_pairs={{0,3},{1,0},{2,1},{3,2},{4,7},{5,4},{6,5},{7,6},{8,11},{9,8},{10,9... | collective-permute-start | bytes 1572872 | tf_op jit(solution)/shard_map/ppermute | solution.py:604
  172.0 9.5 %all-to-all-start.1 = ((bf16[8,64,128]{2,1,0:T(8,128)(2,1)}), bf16[8,64,128]{2,1,0:T(8,128)(2,1)S(1)}, u32[]{:S(2)}, u32[]{:S(2)}) async-start(bf16[8,64,128]{2,1,0:T(8,128)(2,1)} %enter_states.1), calls=%async_computation.1 | async-start | bytes 262144 | tf_op jit(solution)/shard_map/all_to_all | solution.py:616
  181.5 46.9 %all-to-all-start.4 = ((bf16[64,8,1024]{2,1,0:T(8,128)(2,1)}), bf16[64,8,1024]{2,1,0:T(8,128)(2,1)S(1)}, u32[]{:S(2)}, u32[]{:S(2)}) async-start(bf16[64,8,1024]{2,1,0:T(8,128)(2,1)} %bitcast.23), calls=%async_computation.4 | async-start | bytes 2097152 | tf_op jit(solution)/shard_map/all_to_all | solution.py:616
  196.9 26.6 %collective-permute-start.7 = (bf16[128,2048]{1,0:T(8,128)(2,1)}, bf16[128,2048]{1,0:T(8,128)(2,1)S(1)}, u32[]{:S(2)}, u32[]{:S(2)}) collective-permute-start(bf16[128,2048]{1,0:T(8,128)(2,1)} %get-tuple-element.42), channel_id=1, source_target_pairs={{0,1},{1,2},{2,3},{3,0},{4,5},{5,6},{6,7},{7,4},{8,9},{9,10},{10,1... | collective-permute-start | bytes 1572872 | tf_op jit(solution)/shard_map/ppermute | solution.py:604
  196.9 26.6 %collective-permute-start.8 = (bf16[128,2048]{1,0:T(8,128)(2,1)}, bf16[128,2048]{1,0:T(8,128)(2,1)S(1)}, u32[]{:S(2)}, u32[]{:S(2)}) collective-permute-start(bf16[128,2048]{1,0:T(8,128)(2,1)} %get-tuple-element.43), channel_id=1, source_target_pairs={{0,2},{1,3},{2,0},{3,1},{4,6},{5,7},{6,4},{7,5},{8,10},{9,11},{10,... | collective-permute-start | bytes 1572872 | tf_op jit(solution)/shard_map/ppermute | solution.py:604
  199.6 24.5 %collective-permute-start.9 = (bf16[128,2048]{1,0:T(8,128)(2,1)}, bf16[128,2048]{1,0:T(8,128)(2,1)S(1)}, u32[]{:S(2)}, u32[]{:S(2)}) collective-permute-start(bf16[128,2048]{1,0:T(8,128)(2,1)} %get-tuple-element.44), channel_id=1, source_target_pairs={{0,3},{1,0},{2,1},{3,2},{4,7},{5,4},{6,5},{7,6},{8,11},{9,8},{10,9... | collective-permute-start | bytes 1572872 | tf_op jit(solution)/shard_map/ppermute | solution.py:604
  (6 other events, 153.8 us)

commit v3 on v2

--- a/solution.py
+++ b/solution.py
@@ -1,5 +1,3 @@
-import functools
-
 import jax
 import jax.numpy as jnp
 from jax import lax
@@ -366,27 +364,39 @@
     units = weight_refs.shape[2]
     for q in range(4):
         fetches[2 * q].wait()
+        fetches[2 * q + 1].wait()
         gates = dot(x_ref[...], weight_refs[2 * q])
-        fetches[2 * q + 1].wait()
         uppers = dot(x_ref[...], weight_refs[2 * q + 1])
         out_ref[:, q * units : (q + 1) * units] = (
             gates / (1.0 + jnp.exp(-gates)) * uppers
         ).astype(BF16)
 
 
-def down_kernel(part, hidden_ref, own_hbm, before, after, far, out_ref, own_ref, sem):
-    units, width = before.shape
-    fetch = pltpu.make_async_copy(
-        own_hbm.at[:, part * width : (part + 1) * width], own_ref, sem
-    )
-    fetch.start()
-    others = jnp.concatenate([before[...], after[...], far[...]], axis=0)
-    result = dot(hidden_ref[:, units:], others)
-    fetch.wait()
-    out_ref[...] = (result + dot(hidden_ref[:, :units], own_ref[...])).astype(BF16)
-
-
-def pack_kernel(x_ref, gain_ref, routes_ref, mix_ref, out_ref, high_ref, rest_ref):
+def down_early_kernel(hidden_ref, own, before_0, before_1, after_0, after_1, out_ref):
+    count = 3 * own.shape[0]
+    halves = pl.num_programs(0) // 2
+    for half, before, after in ((0, before_0, after_0), (1, before_1, after_1)):
+
+        @pl.when(pl.program_id(0) // halves == half)
+        def _():
+            weights = jnp.concatenate([own[...], before[...], after[...]], axis=0)
+            out_ref[...] = dot(hidden_ref[:, :count], weights).astype(BF16)
+
+
+def down_late_kernel(early_ref, hidden_ref, far_0, far_1, out_ref):
+    tile = out_ref.shape[1]
+    for part in range(4):
+        far = (far_0, far_1)[part // 2]
+
+        @pl.when(pl.program_id(0) == part)
+        def _():
+            low = (part % 2) * tile
+            out_ref[...] = (
+                early_ref[...].astype(F32) + dot(hidden_ref[...], far[:, low : low + tile])
+            ).astype(BF16)
+
+
+def pack_kernel(x_ref, gain_ref, routes_ref, mix_ref, out_ref, mix_out_ref):
     tokens = x_ref.shape[0]
     places = out_ref.shape[0]
     x = x_ref[...].astype(F32)
@@ -412,14 +422,15 @@
         table = table + here.astype(F32)
         mix = jnp.where(here, weight, mix)
     out_ref[...] = dot(table.astype(BF16), normed).astype(BF16)
-    high, rest = two_parts(mix)
-    high_ref[...] = high
-    rest_ref[...] = rest
-
-
-def combine_kernel(high_ref, rest_ref, rows_ref, *refs):
-    rows = rows_ref[...]
-    refs[-1][...] = (dot_tn(high_ref[...], rows) + dot_tn(rest_ref[...], rows)).astype(BF16)
+    high, rest = two_parts(jnp.transpose(mix))
+    mix_out_ref[:tokens, :] = high
+    mix_out_ref[tokens:, :] = rest
+
+
+def combine_kernel(mix_ref, rows_ref, out_ref):
+    tokens = out_ref.shape[0]
+    both = dot(mix_ref[...], rows_ref[...])
+    out_ref[...] = (both[:tokens] + both[tokens:]).astype(BF16)
 
 
 def whole(shape):
@@ -552,21 +563,50 @@
     )(pltpu.with_memory_space_constraint(x, pltpu.HBM), *weights)
 
 
-def expert_down(hidden, own, others, part):
+def first_half(units, tile):
+    return pl.BlockSpec((units, tile), lambda i: (0, jnp.minimum(i, 1)))
+
+
+def last_half(units, tile):
+    return pl.BlockSpec((units, tile), lambda i: (0, jnp.maximum(i - 2, 0)))
+
+
+def expert_down_early(hidden, own, before, after):
     rows = hidden.shape[0]
-    units, width = others[0].shape
-    return pl.pallas_call(
-        functools.partial(down_kernel, part),
-        in_specs=[IN_VMEM, IN_HBM] + [IN_VMEM] * 3,
-        out_specs=IN_VMEM,
+    units, width = own.shape
+    tile = width // 4
+    halves = [first_half(units, tile), last_half(units, tile)]
+    return pl.pallas_call(
+        down_early_kernel,
+        grid=(4,),
+        in_specs=[whole(hidden.shape), pl.BlockSpec((units, tile), lambda i: (0, i))]
+        + 2 * halves,
+        out_specs=pl.BlockSpec((rows, tile), lambda i: (0, i)),
         out_shape=jax.ShapeDtypeStruct((rows, width), BF16),
-        scratch_shapes=[
-            pltpu.VMEM((units, width), BF16),
-            pltpu.SemaphoreType.DMA,
+        cost_estimate=estimate(6 * rows * units * width, 6 << 20),
+        name="down_early",
+    )(hidden, own, *before, *after)
+
+
+def expert_down_late(early, hidden, far):
+    rows, width = early.shape
+    units = far[0].shape[0]
+    tile = width // 4
+    column = pl.BlockSpec((rows, tile), lambda i: (0, i))
+    return pl.pallas_call(
+        down_late_kernel,
+        grid=(4,),
+        in_specs=[
+            column,
+            pl.BlockSpec((rows, units), lambda i: (0, 3)),
+            IN_VMEM,
+            IN_VMEM,
         ],
-        cost_estimate=estimate(8 * rows * units * width, 4 << 20),
-        name="down",
-    )(hidden, own, *map(in_vmem, others))
+        out_specs=column,
+        out_shape=jax.ShapeDtypeStruct((rows, width), BF16),
+        cost_estimate=estimate(2 * rows * units * width, 5 << 20),
+        name="down_late",
+    )(early, hidden, *map(in_vmem, far))
 
 
 def pack_rows(x, gain, routes, mix, places):
@@ -575,28 +615,23 @@
         pack_kernel,
         out_shape=[
             jax.ShapeDtypeStruct((places, width), BF16),
-            jax.ShapeDtypeStruct((places, tokens), BF16),
-            jax.ShapeDtypeStruct((places, tokens), BF16),
+            jax.ShapeDtypeStruct((2 * tokens, places), BF16),
         ],
         cost_estimate=estimate(2.0e9, 3 << 20),
         name="pack",
     )(x, gain, routes, mix)
 
 
-def combine_rows(high, rest, rows, part, into=()):
-    _, tokens = high.shape
-    width = rows.shape[1]
+def combine_rows(mix, rows):
+    tokens = mix.shape[0] // 2
     return pl.pallas_call(
         combine_kernel,
-        grid=(1,),
-        in_specs=[IN_VMEM] * 3 + [IN_HBM] * len(into),
-        out_specs=pl.BlockSpec((tokens, width), lambda i: (0, part)),
-        out_shape=jax.ShapeDtypeStruct((tokens, 2 * width), BF16),
-        input_output_aliases={3: 0} if into else {},
-        compiler_params=pltpu.CompilerParams(dimension_semantics=("arbitrary",)),
+        in_specs=[IN_VMEM, IN_VMEM],
+        out_specs=IN_VMEM,
+        out_shape=jax.ShapeDtypeStruct((tokens, rows.shape[1]), BF16),
         cost_estimate=estimate(1.0e9, 3 << 20),
         name="combine",
-    )(high, rest, in_vmem(rows), *into)
+    )(mix, in_vmem(rows))
 
 
 def ring(x, shift, axis="tp"):
@@ -645,13 +680,13 @@
     cut = model_width // 2
     down_0, down_1 = w_down[:, :cut], w_down[:, cut:]
     gate_r, up_l = ring(w_gate, 1), ring(w_up, -1)
-    gate_l, up_r = ring(w_gate, -1), ring(w_up, 1)
+    up_r, gate_l = ring(w_up, 1), ring(w_gate, -1)
     gate_f, up_f = ring(gate_r, 1), ring(up_l, -1)
-    down_0r, down_0l = ring(down_0, 1), ring(down_0, -1)
-    down_1r, down_1l = ring(down_1, 1), ring(down_1, -1)
+    down_0r, down_1l = ring(down_0, 1), ring(down_1, -1)
+    down_1r, down_0l = ring(down_1, 1), ring(down_0, -1)
     down_0f, down_1f = ring(down_0r, 1), ring(down_1l, -1)
 
-    outgoing, high, rest = pack_rows(
+    outgoing, mix = pack_rows(
         expert_input, expert_gain.reshape(1, -1), routes.T, route_weight.T, places
     )
     arrived = exchange(
@@ -692,16 +727,10 @@
     hiddens = expert_hidden(
         arrived, [w_gate, w_up, gate_r, up_r, gate_l, up_l, gate_f, up_f]
     )
-    combined = ()
-    for n, others in enumerate(((down_0r, down_0l, down_0f), (down_1r, down_1l, down_1f))):
-        returning = expert_down(hiddens, w_down, others, n)
-        if n:
-            returning, returned = lax.optimization_barrier((returning, returned))
-            combined = (combine_rows(high, rest, returned, 0),)
-        returned = exchange(
-            returning.reshape(ep_count, CAPACITY, cut), EP
-        ).reshape(places, cut)
-    return (mixer_out, combine_rows(high, rest, returned, 1, combined))
+    early = expert_down_early(hiddens, w_down, (down_0r, down_1r), (down_0l, down_1l))
+    returning = expert_down_late(early, hiddens, (down_0f, down_1f))
+    returned = exchange(returning.reshape(ep_count, CAPACITY, model_width), EP)
+    return (mixer_out, combine_rows(mix, returned.reshape(places, model_width)))
 
 
 def solution(mesh):

time: 231 us -> 241 us (1.043)
  waiting for transfers between devices: 99 us -> 118 us
  starting transfers between devices: 65 us -> 57.9 us
  Pallas kernels: 62.6 us -> 57.5 us
  local copies, waits for them, and re-layouts: 0.91 us -> 3.37 us
    all_to_all x5 -> x4, starting transfers between devices: 40.9 us -> 28.6 us  [exchange(): return lax.all_to_all(x, axis, 0, 0, tiled=True)]
    all_to_all x5 -> x4, waiting for transfers between devices: 9.26 us -> 20.4 us  [exchange(): return lax.all_to_all(x, axis, 0, 0, tiled=True)]
    ppermute x22, waiting for transfers between devices: 89.8 us -> 97.7 us  [ring(): lax.ppermute(x, axis, [(i, (i + shift) % count) for i in range(count)])]
    ppermute x22, starting transfers between devices: 24.1 us -> 29.3 us  [ring(): lax.ppermute(x, axis, [(i, (i + shift) % count) for i in range(count)])]
    pallas_call x1, Pallas kernels: 12.8 us -> 8.33 us  [expert_hidden(): pl.pallas_call(hidden_kernel, in_specs=[IN_HBM] * (1 + count), out_specs=...]
    pallas_call x4 -> x3, Pallas kernels: 13.5 us -> 12.7 us  [the longest x1 5.76 us: expert_down_early(): pl.pallas_call(down_early_kernel, grid=(4,), in_specs=[whole(hidden.shape...]
  transfers between devices with their start and end apart: 27 -> 26, of which waited for: 12 -> 11; matrix products, arithmetic and copies ran while one was open for 1% -> 1% of each run, Pallas kernels for 25% -> 14%
where the time goes in v3:
time: 241 us; the launch traced here: 240 us
  waiting for transfers between devices  118 us (49%)
  starting transfers between devices  57.9 us (24%)
  Pallas kernels  57.5 us (24%)
  local copies, waits for them, and re-layouts  3.37 us (1%)
    ppermute x22, waiting for transfers between devices, ring(): lax.ppermute(x, axis, [(i, (i + shift) % count) for i in range(count)])  97.7 us
    ppermute x22, starting transfers between devices, ring(): lax.ppermute(x, axis, [(i, (i + shift) % count) for i in range(count)])  29.3 us
    all_to_all x4, starting transfers between devices, exchange(): return lax.all_to_all(x, axis, 0, 0, tiled=True)  28.6 us
    all_to_all x4, waiting for transfers between devices, exchange(): return lax.all_to_all(x, axis, 0, 0, tiled=True)  20.4 us
    pallas_call x1, Pallas kernels, summarize(): pl.pallas_call(summary_kernel, grid=(spans,), in_specs=[SCALARS] + [block...  19.5 us
    pallas_call x1, Pallas kernels, read_and_project(): pl.pallas_call(readout_kernel, grid=(spans,), in_specs=[SCALARS, IN_VMEM,...  8.87 us
    pallas_call x1, Pallas kernels, expert_hidden(): pl.pallas_call(hidden_kernel, in_specs=[IN_HBM] * (1 + count), out_specs=...  8.33 us
    pallas_call x1, Pallas kernels, expert_down_early(): pl.pallas_call(down_early_kernel, grid=(4,), in_specs=[whole(hidden.shape...  5.76 us
  transfers between devices with their start and end apart: 26, of which 11 were waited for; matrix products, arithmetic and copies ran while one was open for 1% of the time, Pallas kernels for 14%

profile of v3, /device:TPU:2, one launch (start us, length us, event | category | flops | bytes accessed | tf_op | source)
XLA Modules:
  0.0 239.8 jit_solution(2700155952786535814)
XLA Ops:
  0.6 19.5 %summary.1 = (bf16[512,512]{1,0:T(8,128)(2,1)}, f32[512,512]{1,0:T(8,128)}, bf16[4,4,128,128]{3,2,1,0:T(8,128)(2,1)}, f32[4,4,128,128]{3,2,1,0:T(8,128)}, f32[4,...) custom-call(s32[1]{0:T(128)} %bitcast.2.here_ref, ...), custom_call_target="tpu_custom_call" | custom-call | flops 20000000000 | bytes 6291456 | tf_op jit(solution)/shard_map/summary/pallas_call | solution.py:456
  21.7 2.7 %collective-permute-start.2 = (bf16[80,128]{1,0:T(8,128)(2,1)}, bf16[80,128]{1,0:T(8,128)(2,1)S(1)}, u32[]{:S(2)}, u32[]{:S(2)}) collective-permute-start(bf16[80,128]{1,0:T(8,128)(2,1)} %get-tuple-element.26), channel_id=1, source_target_pairs={{0,12},{4,16},{8,20},{12,24},{16,28},{20,0},{24,4},{28,8},{1,13},{... | collective-permute-start | bytes 61448 | tf_op jit(solution)/shard_map/ppermute | solution.py:639
  25.2 2.4 collective-permute-start.4
  34.0 6.8 %all-to-all-start = ((bf16[8,80,128]{2,1,0:T(8,128)(2,1)}), bf16[8,80,128]{2,1,0:T(8,128)(2,1)S(1)}, u32[]{:S(2)}, u32[]{:S(2)}) async-start(bf16[8,80,128]{2,1,0:T(8,128)(2,1)} %get-tuple-element.31), calls=%async_computation | async-start | bytes 327680 | tf_op jit(solution)/shard_map/all_to_all | solution.py:651
  40.8 3.4 %pack.1 = (bf16[512,2048]{1,0:T(8,128)(2,1)}, bf16[256,512]{1,0:T(8,128)(2,1)}) custom-call(bf16[128,2048]{1,0:T(8,128)(2,1)} %x_ref.1, f32[1,2048]{1,0:T(1,128)} %bitcast.25, s32[2,128]{1,0:T(2,128)} %bitcast.28, f32[2,128]{1,0:T(2,128)} %bitcast.29), custom_call_target="tpu_custom_call" | custom-call | flops 2000000000 | bytes 3145728 | tf_op jit(solution)/shard_map/pack/pallas_call | solution.py:614
  44.2 7.4 %all-to-all-done.in_ref = bf16[8,80,128]{2,1,0:T(8,128)(2,1)S(1)} async-done(((bf16[8,80,128]{2,1,0:T(8,128)(2,1)}), bf16[8,80,128]{2,1,0:T(8,128)(2,1)S(1)}, u32[]{:S(2)}, u32[]{:S(2)}) %all-to-all-start) | async-done | bytes 163872 | tf_op jit(solution)/shard_map/all_to_all | solution.py:651
  51.6 6.4 %all-to-all-start.2 = ((bf16[64,8,2048]{2,1,0:T(8,128)(2,1)}), bf16[64,8,2048]{2,1,0:T(8,128)(2,1)}, u32[]{:S(2)}, u32[]{:S(2)}) async-start(bf16[64,8,2048]{2,1,0:T(8,128)(2,1)} %bitcast.20), calls=%async_computation.2 | async-start | bytes 4194304 | tf_op jit(solution)/shard_map/all_to_all | solution.py:651
  66.0 19.4 %collective-permute-done.10.refs_2_ = bf16[2048,256]{1,0:T(8,128)(2,1)} collective-permute-done((bf16[2048,256]{1,0:T(8,128)(2,1)S(1)}, bf16[2048,256]{1,0:T(8,128)(2,1)}, u32[]{:S(2)}, u32[]{:S(2)}) %collective-permute-start.10) | collective-permute-done | bytes 1048608 | tf_op jit(solution)/shard_map/ppermute | solution.py:639
  86.1 2.9 %collective-permute-start.15 = (bf16[2048,256]{1,0:T(8,128)(2,1)}, bf16[2048,256]{1,0:T(8,128)(2,1)}, u32[]{:S(2)}, u32[]{:S(2)}) collective-permute-start(bf16[2048,256]{1,0:T(8,128)(2,1)} %collective-permute-done.13.refs_5_), channel_id=1, source_target_pairs={{0,3},{1,0},{2,1},{3,2},{4,7},{5,4},{6,5},{7,6},{8,11},{9,8},{10,9... | collective-permute-start | bytes 3145736 | tf_op jit(solution)/shard_map/ppermute | solution.py:639
  88.9 7.7 %collective-permute-done.16.before_0 = bf16[256,1024]{1,0:T(8,128)(2,1)S(1)} collective-permute-done((bf16[256,1024]{1,0:T(8,128)(2,1)}, bf16[256,1024]{1,0:T(8,128)(2,1)S(1)}, u32[]{:S(2)}, u32[]{:S(2)}) %collective-permute-start.16) | collective-permute-done | bytes 524320 | tf_op jit(solution)/shard_map/ppermute | solution.py:639
  98.4 42.6 %collective-permute-done.19.after_1 = bf16[256,1024]{1,0:T(8,128)(2,1)S(1)} collective-permute-done((bf16[256,1024]{1,0:T(8,128)(2,1)}, bf16[256,1024]{1,0:T(8,128)(2,1)S(1)}, u32[]{:S(2)}, u32[]{:S(2)}) %collective-permute-start.19) | collective-permute-done | bytes 524320 | tf_op jit(solution)/shard_map/ppermute | solution.py:639
  144.3 2.9 %enter_states.1 = bf16[8,64,128]{2,1,0:T(8,128)(2,1)} custom-call(s32[1]{0:T(128)} %bitcast.1.here_ref, bf16[8,80,128]{2,1,0:T(8,128)(2,1)S(1)} %all-to-all-done.in_ref, f32[8,128,64]{2,1,0:T(8,128)} %get-tuple-element.32.prefix_ref), custom_call_target="tpu_custom_call" | custom-call | flops 2000000000 | bytes 1048576 | tf_op jit(solution)/shard_map/enter_states/pallas_call | solution.py:504
  147.1 4.8 %all-to-all-start.1 = ((bf16[8,64,128]{2,1,0:T(8,128)(2,1)}), bf16[8,64,128]{2,1,0:T(8,128)(2,1)S(1)}, u32[]{:S(2)}, u32[]{:S(2)}) async-start(bf16[8,64,128]{2,1,0:T(8,128)(2,1)} %enter_states.1), calls=%async_computation.1 | async-start | bytes 262144 | tf_op jit(solution)/shard_map/all_to_all | solution.py:651
  152.4 2.9 %collective-permute-start.21 = (bf16[256,1024]{1,0:T(8,128)(2,1)S(1)}, bf16[256,1024]{1,0:T(8,128)(2,1)S(1)}, u32[]{:S(2)}, u32[]{:S(2)}) collective-permute-start(bf16[256,1024]{1,0:T(8,128)(2,1)S(1)} %collective-permute-done.19.after_1), channel_id=1, source_target_pairs={{0,3},{1,0},{2,1},{3,2},{4,7},{5,4},{6,5},{7,6},{8,11},{9,8},{10,9... | collective-permute-start | bytes 1572872 | tf_op jit(solution)/shard_map/ppermute | solution.py:639
  155.3 8.3 %hidden.1.hidden_ref = bf16[512,1024]{1,0:T(8,128)(2,1)} custom-call(bf16[512,2048]{1,0:T(8,128)(2,1)} %bitcast.10.x_hbm, bf16[2048,256]{1,0:T(8,128)(2,1)} %bitcast.21, bf16[2048,256]{1,0:T(8,128)(2,1)} %bitcast.12.refs_1_, bf16[2048,256]{1,0:T(8,128)(2,1)} %collective-permute-done.10.refs_2_, bf16[2048,256]{1,0:T(8,128)(2,1)} %collective-permute-done.11.refs_3_, ...), custom_call_target="tpu_custom_call" | custom-call | flops 4294967296 | bytes 11534336 | tf_op jit(solution)/shard_map/hidden/pallas_call | solution.py:551
  165.2 5.8 %down_early.1.early_ref = bf16[512,2048]{1,0:T(8,128)(2,1)} custom-call(bf16[512,1024]{1,0:T(8,128)(2,1)} %hidden.1.hidden_ref, bf16[256,2048]{1,0:T(8,128)(2,1)} %bitcast.18, bf16[256,1024]{1,0:T(8,128)(2,1)} %copy-done.2, bf16[256,1024]{1,0:T(8,128)(2,1)} %copy-done.4, bf16[256,1024]{1,0:T(8,128)(2,1)} %copy-done.5, bf16[256,1024]{1,0:T(8,128)(2,1)} %copy-done.3), custom_call_target="tpu_custom_call" | custom-call | flops 1610612736 | bytes 6291456 | tf_op jit(solution)/shard_map/down_early/pallas_call | solution.py:579
  171.0 4.5 %down_late.1 = bf16[512,2048]{1,0:T(8,128)(2,1)} custom-call(bf16[512,2048]{1,0:T(8,128)(2,1)} %down_early.1.early_ref, bf16[512,1024]{1,0:T(8,128)(2,1)} %hidden.1.hidden_ref, bf16[256,1024]{1,0:T(8,128)(2,1)S(1)} %collective-permute-done.20.far_0, bf16[256,1024]{1,0:T(8,128)(2,1)S(1)} %collective-permute-done.21.far_1), custom_call_target="tpu_custom_call" | custom-call | flops 536870912 | bytes 5242880 | tf_op jit(solution)/shard_map/down_late/pallas_call | solution.py:596
  175.5 10.6 %all-to-all-start.3 = ((bf16[64,8,2048]{2,1,0:T(8,128)(2,1)}), bf16[64,8,2048]{2,1,0:T(8,128)(2,1)S(1)}, u32[]{:S(2)}, u32[]{:S(2)}) async-start(bf16[64,8,2048]{2,1,0:T(8,128)(2,1)} %bitcast.17), calls=%async_computation.3 | async-start | bytes 4194304 | tf_op jit(solution)/shard_map/all_to_all | solution.py:651
  186.1 8.9 %readout.1 = (bf16[128,2048]{1,0:T(8,128)(2,1)}, bf16[128,2048]{1,0:T(8,128)(2,1)}, bf16[128,2048]{1,0:T(8,128)(2,1)}, bf16[128,2048]{1,0:T(8,128)(2,1)}) custom-call(s32[1]{0:T(128)} %bitcast.here_ref, bf16[8,64,128]{2,1,0:T(8,128)(2,1)S(1)} %all-to-all-done.1.enter_ref, bf16[512,512]{1,0:T(8,128)(2,1)} %get-tuple-element.33.reader_ref, ...), custom_call_target="tpu_custom_call" | custom-call | flops 5000000000 | bytes 8388608 | tf_op jit(solution)/shard_map/readout/pallas_call | solution.py:520
  197.0 13.0 %collective-permute-done.9 = bf16[128,2048]{1,0:T(8,128)(2,1)S(1)} collective-permute-done((bf16[128,2048]{1,0:T(8,128)(2,1)}, bf16[128,2048]{1,0:T(8,128)(2,1)S(1)}, u32[]{:S(2)}, u32[]{:S(2)}) %collective-permute-start.9) | collective-permute-done | bytes 524320 | tf_op jit(solution)/shard_map/ppermute | solution.py:639
  212.2 10.1 %collective-permute-done.7 = bf16[128,2048]{1,0:T(8,128)(2,1)S(1)} collective-permute-done((bf16[128,2048]{1,0:T(8,128)(2,1)}, bf16[128,2048]{1,0:T(8,128)(2,1)S(1)}, u32[]{:S(2)}, u32[]{:S(2)}) %collective-permute-start.7) | collective-permute-done | bytes 524320 | tf_op jit(solution)/shard_map/ppermute | solution.py:639
  222.2 2.2 add_convert_fusion
  224.4 13.0 %all-to-all-done.3 = bf16[64,8,2048]{2,1,0:T(8,128)(2,1)S(1)} async-done(((bf16[64,8,2048]{2,1,0:T(8,128)(2,1)}), bf16[64,8,2048]{2,1,0:T(8,128)(2,1)S(1)}, u32[]{:S(2)}, u32[]{:S(2)}) %all-to-all-start.3) | async-done | bytes 2097184 | tf_op jit(solution)/shard_map/all_to_all | solution.py:651
  237.4 2.5 %combine.1 = bf16[128,2048]{1,0:T(8,128)(2,1)} custom-call(bf16[256,512]{1,0:T(8,128)(2,1)} %get-tuple-element.42.mix_ref, bf16[512,2048]{1,0:T(8,128)(2,1)S(1)} %bitcast.16), custom_call_target="tpu_custom_call" | custom-call | flops 1000000000 | bytes 3145728 | tf_op jit(solution)/shard_map/combine/pallas_call | solution.py:627
  (53 shorter events, 28.6 us)
Async XLA Ops:
  20.2 7.4 %collective-permute-start = (bf16[80,128]{1,0:T(8,128)(2,1)}, bf16[80,128]{1,0:T(8,128)(2,1)S(1)}, u32[]{:S(2)}, u32[]{:S(2)}) collective-permute-start(bf16[80,128]{1,0:T(8,128)(2,1)} %get-tuple-element.24), channel_id=1, source_target_pairs={{0,4},{4,8},{8,12},{12,16},{16,20},{20,24},{24,28},{28,0},{1,5},{5... | collective-permute-start | bytes 61448 | tf_op jit(solution)/shard_map/ppermute | solution.py:639
  20.2 7.8 %collective-permute-start.1 = (bf16[80,128]{1,0:T(8,128)(2,1)}, bf16[80,128]{1,0:T(8,128)(2,1)S(1)}, u32[]{:S(2)}, u32[]{:S(2)}) collective-permute-start(bf16[80,128]{1,0:T(8,128)(2,1)} %get-tuple-element.25), channel_id=1, source_target_pairs={{0,8},{4,12},{8,16},{12,20},{16,24},{20,28},{24,0},{28,4},{1,9},{5... | collective-permute-start | bytes 61448 | tf_op jit(solution)/shard_map/ppermute | solution.py:639
  21.7 7.2 %collective-permute-start.2 = (bf16[80,128]{1,0:T(8,128)(2,1)}, bf16[80,128]{1,0:T(8,128)(2,1)S(1)}, u32[]{:S(2)}, u32[]{:S(2)}) collective-permute-start(bf16[80,128]{1,0:T(8,128)(2,1)} %get-tuple-element.26), channel_id=1, source_target_pairs={{0,12},{4,16},{8,20},{12,24},{16,28},{20,0},{24,4},{28,8},{1,13},{... | collective-permute-start | bytes 61448 | tf_op jit(solution)/shard_map/ppermute | solution.py:639
  24.5 5.6 %collective-permute-start.3 = (bf16[80,128]{1,0:T(8,128)(2,1)}, bf16[80,128]{1,0:T(8,128)(2,1)S(1)}, u32[]{:S(2)}, u32[]{:S(2)}) collective-permute-start(bf16[80,128]{1,0:T(8,128)(2,1)} %get-tuple-element.27), channel_id=1, source_target_pairs={{0,16},{4,20},{8,24},{12,28},{16,0},{20,4},{24,8},{28,12},{1,17},{... | collective-permute-start | bytes 61448 | tf_op jit(solution)/shard_map/ppermute | solution.py:639
  25.2 4.9 %collective-permute-start.4 = (bf16[80,128]{1,0:T(8,128)(2,1)}, bf16[80,128]{1,0:T(8,128)(2,1)S(1)}, u32[]{:S(2)}, u32[]{:S(2)}) collective-permute-start(bf16[80,128]{1,0:T(8,128)(2,1)} %get-tuple-element.28), channel_id=1, source_target_pairs={{0,20},{4,24},{8,28},{12,0},{16,4},{20,8},{24,12},{28,16},{1,21},{... | collective-permute-start | bytes 61448 | tf_op jit(solution)/shard_map/ppermute | solution.py:639
  34.0 17.6 %all-to-all-start = ((bf16[8,80,128]{2,1,0:T(8,128)(2,1)}), bf16[8,80,128]{2,1,0:T(8,128)(2,1)S(1)}, u32[]{:S(2)}, u32[]{:S(2)}) async-start(bf16[8,80,128]{2,1,0:T(8,128)(2,1)} %get-tuple-element.31), calls=%async_computation | async-start | bytes 327680 | tf_op jit(solution)/shard_map/all_to_all | solution.py:651
  51.6 95.5 %all-to-all-start.2 = ((bf16[64,8,2048]{2,1,0:T(8,128)(2,1)}), bf16[64,8,2048]{2,1,0:T(8,128)(2,1)}, u32[]{:S(2)}, u32[]{:S(2)}) async-start(bf16[64,8,2048]{2,1,0:T(8,128)(2,1)} %bitcast.20), calls=%async_computation.2 | async-start | bytes 4194304 | tf_op jit(solution)/shard_map/all_to_all | solution.py:651
  58.1 27.4 %collective-permute-start.10 = (bf16[2048,256]{1,0:T(8,128)(2,1)S(1)}, bf16[2048,256]{1,0:T(8,128)(2,1)}, u32[]{:S(2)}, u32[]{:S(2)}) collective-permute-start(bf16[2048,256]{1,0:T(8,128)(2,1)S(1)} %bitcast.22), channel_id=1, source_target_pairs={{0,1},{1,2},{2,3},{3,0},{4,5},{5,6},{6,7},{7,4},{8,9},{9,10},{10,1... | collective-permute-start | bytes 3145736 | tf_op jit(solution)/shard_map/ppermute | solution.py:639
  59.7 26.3 %collective-permute-start.13 = (bf16[2048,256]{1,0:T(8,128)(2,1)}, bf16[2048,256]{1,0:T(8,128)(2,1)}, u32[]{:S(2)}, u32[]{:S(2)}) collective-permute-start(bf16[2048,256]{1,0:T(8,128)(2,1)} %bitcast.12.refs_1_), channel_id=1, source_target_pairs={{0,3},{1,0},{2,1},{3,2},{4,7},{5,4},{6,5},{7,6},{8,11},{9,8},{10,9... | collective-permute-start | bytes 3145736 | tf_op jit(solution)/shard_map/ppermute | solution.py:639
  62.4 34.2 %collective-permute-start.16 = (bf16[256,1024]{1,0:T(8,128)(2,1)}, bf16[256,1024]{1,0:T(8,128)(2,1)S(1)}, u32[]{:S(2)}, u32[]{:S(2)}) collective-permute-start(bf16[256,1024]{1,0:T(8,128)(2,1)} %get-tuple-element.45), channel_id=1, source_target_pairs={{0,1},{1,2},{2,3},{3,0},{4,5},{5,6},{6,7},{7,4},{8,9},{9,10},{10,1... | collective-permute-start | bytes 1572872 | tf_op jit(solution)/shard_map/ppermute | solution.py:639
  62.8 79.8 %collective-permute-start.11 = (bf16[2048,256]{1,0:T(8,128)(2,1)}, bf16[2048,256]{1,0:T(8,128)(2,1)}, u32[]{:S(2)}, u32[]{:S(2)}) collective-permute-start(bf16[2048,256]{1,0:T(8,128)(2,1)} %bitcast.12.refs_1_), channel_id=1, source_target_pairs={{0,1},{1,2},{2,3},{3,0},{4,5},{5,6},{6,7},{7,4},{8,9},{9,10},{10,1... | collective-permute-start | bytes 3145736 | tf_op jit(solution)/shard_map/ppermute | solution.py:639
  64.4 87.6 %collective-permute-start.12 = (bf16[2048,256]{1,0:T(8,128)(2,1)S(1)}, bf16[2048,256]{1,0:T(8,128)(2,1)}, u32[]{:S(2)}, u32[]{:S(2)}) collective-permute-start(bf16[2048,256]{1,0:T(8,128)(2,1)S(1)} %bitcast.23), channel_id=1, source_target_pairs={{0,3},{1,0},{2,1},{3,2},{4,7},{5,4},{6,5},{7,6},{8,11},{9,8},{10,9... | collective-permute-start | bytes 3145736 | tf_op jit(solution)/shard_map/ppermute | solution.py:639
  85.5 66.9 %collective-permute-start.14 = (bf16[2048,256]{1,0:T(8,128)(2,1)}, bf16[2048,256]{1,0:T(8,128)(2,1)}, u32[]{:S(2)}, u32[]{:S(2)}) collective-permute-start(bf16[2048,256]{1,0:T(8,128)(2,1)} %collective-permute-done.10.refs_2_), channel_id=1, source_target_pairs={{0,1},{1,2},{2,3},{3,0},{4,5},{5,6},{6,7},{7,4},{8,9},{9,10},{10,1... | collective-permute-start | bytes 3145736 | tf_op jit(solution)/shard_map/ppermute | solution.py:639
  86.1 69.2 %collective-permute-start.15 = (bf16[2048,256]{1,0:T(8,128)(2,1)}, bf16[2048,256]{1,0:T(8,128)(2,1)}, u32[]{:S(2)}, u32[]{:S(2)}) collective-permute-start(bf16[2048,256]{1,0:T(8,128)(2,1)} %collective-permute-done.13.refs_5_), channel_id=1, source_target_pairs={{0,3},{1,0},{2,1},{3,2},{4,7},{5,4},{6,5},{7,6},{8,11},{9,8},{10,9... | collective-permute-start | bytes 3145736 | tf_op jit(solution)/shard_map/ppermute | solution.py:639
  96.6 44.4 %collective-permute-start.19 = (bf16[256,1024]{1,0:T(8,128)(2,1)}, bf16[256,1024]{1,0:T(8,128)(2,1)S(1)}, u32[]{:S(2)}, u32[]{:S(2)}) collective-permute-start(bf16[256,1024]{1,0:T(8,128)(2,1)} %get-tuple-element.44), channel_id=1, source_target_pairs={{0,3},{1,0},{2,1},{3,2},{4,7},{5,4},{6,5},{7,6},{8,11},{9,8},{10,9... | collective-permute-start | bytes 1572872 | tf_op jit(solution)/shard_map/ppermute | solution.py:639
  141.0 22.6 %collective-permute-start.17 = (bf16[256,1024]{1,0:T(8,128)(2,1)}, bf16[256,1024]{1,0:T(8,128)(2,1)S(1)}, u32[]{:S(2)}, u32[]{:S(2)}) collective-permute-start(bf16[256,1024]{1,0:T(8,128)(2,1)} %get-tuple-element.44), channel_id=1, source_target_pairs={{0,1},{1,2},{2,3},{3,0},{4,5},{5,6},{6,7},{7,4},{8,9},{9,10},{10,1... | collective-permute-start | bytes 1572872 | tf_op jit(solution)/shard_map/ppermute | solution.py:639
  142.6 21.1 %collective-permute-start.18 = (bf16[256,1024]{1,0:T(8,128)(2,1)}, bf16[256,1024]{1,0:T(8,128)(2,1)S(1)}, u32[]{:S(2)}, u32[]{:S(2)}) collective-permute-start(bf16[256,1024]{1,0:T(8,128)(2,1)} %get-tuple-element.45), channel_id=1, source_target_pairs={{0,3},{1,0},{2,1},{3,2},{4,7},{5,4},{6,5},{7,6},{8,11},{9,8},{10,9... | collective-permute-start | bytes 1572872 | tf_op jit(solution)/shard_map/ppermute | solution.py:639
  147.1 28.4 %all-to-all-start.1 = ((bf16[8,64,128]{2,1,0:T(8,128)(2,1)}), bf16[8,64,128]{2,1,0:T(8,128)(2,1)S(1)}, u32[]{:S(2)}, u32[]{:S(2)}) async-start(bf16[8,64,128]{2,1,0:T(8,128)(2,1)} %enter_states.1), calls=%async_computation.1 | async-start | bytes 262144 | tf_op jit(solution)/shard_map/all_to_all | solution.py:651
  152.0 19.0 %collective-permute-start.20 = (bf16[256,1024]{1,0:T(8,128)(2,1)S(1)}, bf16[256,1024]{1,0:T(8,128)(2,1)S(1)}, u32[]{:S(2)}, u32[]{:S(2)}) collective-permute-start(bf16[256,1024]{1,0:T(8,128)(2,1)S(1)} %collective-permute-done.16.before_0), channel_id=1, source_target_pairs={{0,1},{1,2},{2,3},{3,0},{4,5},{5,6},{6,7},{7,4},{8,9},{9,10},{10,1... | collective-permute-start | bytes 1572872 | tf_op jit(solution)/shard_map/ppermute | solution.py:639
  152.4 18.6 %collective-permute-start.21 = (bf16[256,1024]{1,0:T(8,128)(2,1)S(1)}, bf16[256,1024]{1,0:T(8,128)(2,1)S(1)}, u32[]{:S(2)}, u32[]{:S(2)}) collective-permute-start(bf16[256,1024]{1,0:T(8,128)(2,1)S(1)} %collective-permute-done.19.after_1), channel_id=1, source_target_pairs={{0,3},{1,0},{2,1},{3,2},{4,7},{5,4},{6,5},{7,6},{8,11},{9,8},{10,9... | collective-permute-start | bytes 1572872 | tf_op jit(solution)/shard_map/ppermute | solution.py:639
  175.5 61.8 %all-to-all-start.3 = ((bf16[64,8,2048]{2,1,0:T(8,128)(2,1)}), bf16[64,8,2048]{2,1,0:T(8,128)(2,1)S(1)}, u32[]{:S(2)}, u32[]{:S(2)}) async-start(bf16[64,8,2048]{2,1,0:T(8,128)(2,1)} %bitcast.17), calls=%async_computation.3 | async-start | bytes 4194304 | tf_op jit(solution)/shard_map/all_to_all | solution.py:651
  195.0 15.0 %collective-permute-start.9 = (bf16[128,2048]{1,0:T(8,128)(2,1)}, bf16[128,2048]{1,0:T(8,128)(2,1)S(1)}, u32[]{:S(2)}, u32[]{:S(2)}) collective-permute-start(bf16[128,2048]{1,0:T(8,128)(2,1)} %get-tuple-element.41), channel_id=1, source_target_pairs={{0,3},{1,0},{2,1},{3,2},{4,7},{5,4},{6,5},{7,6},{8,11},{9,8},{10,9... | collective-permute-start | bytes 1572872 | tf_op jit(solution)/shard_map/ppermute | solution.py:639
  195.6 16.6 %collective-permute-start.8 = (bf16[128,2048]{1,0:T(8,128)(2,1)}, bf16[128,2048]{1,0:T(8,128)(2,1)S(1)}, u32[]{:S(2)}, u32[]{:S(2)}) collective-permute-start(bf16[128,2048]{1,0:T(8,128)(2,1)} %get-tuple-element.40), channel_id=1, source_target_pairs={{0,2},{1,3},{2,0},{3,1},{4,6},{5,7},{6,4},{7,5},{8,10},{9,11},{10,... | collective-permute-start | bytes 1572872 | tf_op jit(solution)/shard_map/ppermute | solution.py:639
  196.2 26.0 %collective-permute-start.7 = (bf16[128,2048]{1,0:T(8,128)(2,1)}, bf16[128,2048]{1,0:T(8,128)(2,1)S(1)}, u32[]{:S(2)}, u32[]{:S(2)}) collective-permute-start(bf16[128,2048]{1,0:T(8,128)(2,1)} %get-tuple-element.39), channel_id=1, source_target_pairs={{0,1},{1,2},{2,3},{3,0},{4,5},{5,6},{6,7},{7,4},{8,9},{9,10},{10,1... | collective-permute-start | bytes 1572872 | tf_op jit(solution)/shard_map/ppermute | solution.py:639
  (9 other events, 92.8 us)

commit v4 on v3

--- a/solution.py
+++ b/solution.py
@@ -372,28 +372,58 @@
         ).astype(BF16)
 
 
-def down_early_kernel(hidden_ref, own, before_0, before_1, after_0, after_1, out_ref):
-    count = 3 * own.shape[0]
-    halves = pl.num_programs(0) // 2
-    for half, before, after in ((0, before_0, after_0), (1, before_1, after_1)):
-
-        @pl.when(pl.program_id(0) // halves == half)
-        def _():
-            weights = jnp.concatenate([own[...], before[...], after[...]], axis=0)
-            out_ref[...] = dot(hidden_ref[:, :count], weights).astype(BF16)
-
-
-def down_late_kernel(early_ref, hidden_ref, far_0, far_1, out_ref):
-    tile = out_ref.shape[1]
-    for part in range(4):
+def down_early_kernel(
+    hidden_ref, own, before_0, before_1, after_0, after_1, out_ref, weight_ref, sems
+):
+    units, width = own.shape
+    half = width // 2
+    places = (
+        (own, 0, 0, width),
+        (before_0, 1, 0, half),
+        (after_0, 2, 0, half),
+        (before_1, 1, half, half),
+        (after_1, 2, half, half),
+    )
+    fetches = [
+        pltpu.make_async_copy(
+            w, weight_ref.at[row * units : (row + 1) * units, low : low + size], sems.at[n]
+        )
+        for n, (w, row, low, size) in enumerate(places)
+    ]
+    for fetch in fetches:
+        fetch.start()
+    for part, waits in ((0, fetches[:3]), (1, fetches[3:])):
+        for fetch in waits:
+            fetch.wait()
+        lanes = slice(part * half, (part + 1) * half)
+        out_ref[:, lanes] = dot(hidden_ref[:, : 3 * units], weight_ref[:, lanes]).astype(BF16)
+
+
+def down_late_kernel(
+    early_ref, hidden_hbm, far_0, far_1, out_hbm, hidden_ref, made_ref, hidden_sem, sems
+):
+    units = hidden_ref.shape[1]
+    width = made_ref.shape[1]
+    parts = 4
+    tile = width // parts
+    fetch = pltpu.make_async_copy(
+        hidden_hbm.at[:, hidden_hbm.shape[1] - units :], hidden_ref, hidden_sem
+    )
+    fetch.start()
+    fetch.wait()
+    stores = []
+    for part in range(parts):
         far = (far_0, far_1)[part // 2]
-
-        @pl.when(pl.program_id(0) == part)
-        def _():
-            low = (part % 2) * tile
-            out_ref[...] = (
-                early_ref[...].astype(F32) + dot(hidden_ref[...], far[:, low : low + tile])
-            ).astype(BF16)
+        low = (part % 2) * tile
+        lanes = slice(part * tile, (part + 1) * tile)
+        made_ref[:, lanes] = (
+            early_ref[:, lanes].astype(F32) + dot(hidden_ref[...], far[:, low : low + tile])
+        ).astype(BF16)
+        store = pltpu.make_async_copy(made_ref.at[:, lanes], out_hbm.at[:, lanes], sems.at[part])
+        store.start()
+        stores.append(store)
+    for store in stores:
+        store.wait()
 
 
 def pack_kernel(x_ref, gain_ref, routes_ref, mix_ref, out_ref, mix_out_ref):
@@ -563,26 +593,18 @@
     )(pltpu.with_memory_space_constraint(x, pltpu.HBM), *weights)
 
 
-def first_half(units, tile):
-    return pl.BlockSpec((units, tile), lambda i: (0, jnp.minimum(i, 1)))
-
-
-def last_half(units, tile):
-    return pl.BlockSpec((units, tile), lambda i: (0, jnp.maximum(i - 2, 0)))
-
-
 def expert_down_early(hidden, own, before, after):
     rows = hidden.shape[0]
     units, width = own.shape
-    tile = width // 4
-    halves = [first_half(units, tile), last_half(units, tile)]
     return pl.pallas_call(
         down_early_kernel,
-        grid=(4,),
-        in_specs=[whole(hidden.shape), pl.BlockSpec((units, tile), lambda i: (0, i))]
-        + 2 * halves,
-        out_specs=pl.BlockSpec((rows, tile), lambda i: (0, i)),
-        out_shape=jax.ShapeDtypeStruct((rows, width), BF16),
+        in_specs=[IN_VMEM] + [IN_HBM] * 5,
+        out_specs=IN_VMEM,
+        out_shape=pltpu.VMEM((rows, width), BF16),
+        scratch_shapes=[
+            pltpu.VMEM((3 * units, width), BF16),
+            pltpu.SemaphoreType.DMA((5,)),
+        ],
         cost_estimate=estimate(6 * rows * units * width, 6 << 20),
         name="down_early",
     )(hidden, own, *before, *after)
@@ -591,22 +613,20 @@
 def expert_down_late(early, hidden, far):
     rows, width = early.shape
     units = far[0].shape[0]
-    tile = width // 4
-    column = pl.BlockSpec((rows, tile), lambda i: (0, i))
     return pl.pallas_call(
         down_late_kernel,
-        grid=(4,),
-        in_specs=[
-            column,
-            pl.BlockSpec((rows, units), lambda i: (0, 3)),
-            IN_VMEM,
-            IN_VMEM,
+        in_specs=[IN_VMEM, IN_HBM, IN_VMEM, IN_VMEM],
+        out_specs=IN_HBM,
+        out_shape=jax.ShapeDtypeStruct((rows, width), BF16),
+        scratch_shapes=[
+            pltpu.VMEM((rows, units), BF16),
+            pltpu.VMEM((rows, width), BF16),
+            pltpu.SemaphoreType.DMA,
+            pltpu.SemaphoreType.DMA((4,)),
         ],
-        out_specs=column,
-        out_shape=jax.ShapeDtypeStruct((rows, width), BF16),
         cost_estimate=estimate(2 * rows * units * width, 5 << 20),
         name="down_late",
-    )(early, hidden, *map(in_vmem, far))
+    )(in_vmem(early), hidden, *map(in_vmem, far))
 
 
 def pack_rows(x, gain, routes, mix, places):

time: 241 us -> 236 us (0.979)
  Pallas kernels: 57.5 us -> 54.6 us
    pallas_call x2, Pallas kernels: 10.3 us -> 7.45 us  [the longest x1 4.75 us: expert_down_early(): pl.pallas_call(down_early_kernel, in_specs=[IN_VMEM] + [IN_HBM] * 5, out_...]
  transfers between devices with their start and end apart: 26 -> 26, of which waited for: 11 -> 9; matrix products, arithmetic and copies ran while one was open for 1% -> 1% of each run, Pallas kernels for 14% -> 13%
where the time goes in v4:
time: 236 us; the launch traced here: 235 us
  waiting for transfers between devices  117 us (50%)
  starting transfers between devices  58.2 us (25%)
  Pallas kernels  54.6 us (23%)
    ppermute x22, waiting for transfers between devices, ring(): lax.ppermute(x, axis, [(i, (i + shift) % count) for i in range(count)])  98.1 us
    ppermute x22, starting transfers between devices, ring(): lax.ppermute(x, axis, [(i, (i + shift) % count) for i in range(count)])  30.1 us
    all_to_all x4, starting transfers between devices, exchange(): return lax.all_to_all(x, axis, 0, 0, tiled=True)  28.1 us
    pallas_call x1, Pallas kernels, summarize(): pl.pallas_call(summary_kernel, grid=(spans,), in_specs=[SCALARS] + [block...  19.5 us
    all_to_all x4, waiting for transfers between devices, exchange(): return lax.all_to_all(x, axis, 0, 0, tiled=True)  19.3 us
    pallas_call x1, Pallas kernels, read_and_project(): pl.pallas_call(readout_kernel, grid=(spans,), in_specs=[SCALARS, IN_VMEM,...  8.9 us
    pallas_call x1, Pallas kernels, expert_hidden(): pl.pallas_call(hidden_kernel, in_specs=[IN_HBM] * (1 + count), out_specs=...  8.3 us
    pallas_call x1, Pallas kernels, expert_down_early(): pl.pallas_call(down_early_kernel, in_specs=[IN_VMEM] + [IN_HBM] * 5, out_...  4.75 us
  transfers between devices with their start and end apart: 26, of which 9 were waited for; matrix products, arithmetic and copies ran while one was open for 1% of the time, Pallas kernels for 13%

profile of v4, /device:TPU:2, one launch (start us, length us, event | category | flops | bytes accessed | tf_op | source)
XLA Modules:
  0.0 234.8 jit_solution(577278086505695230)
XLA Ops:
  0.6 19.5 %summary.1 = (bf16[512,512]{1,0:T(8,128)(2,1)}, f32[512,512]{1,0:T(8,128)}, bf16[4,4,128,128]{3,2,1,0:T(8,128)(2,1)}, f32[4,4,128,128]{3,2,1,0:T(8,128)}, f32[4,...) custom-call(s32[1]{0:T(128)} %bitcast.2.here_ref, ...), custom_call_target="tpu_custom_call" | custom-call | flops 20000000000 | bytes 6291456 | tf_op jit(solution)/shard_map/summary/pallas_call | solution.py:486
  21.7 2.7 %collective-permute-start.2 = (bf16[80,128]{1,0:T(8,128)(2,1)}, bf16[80,128]{1,0:T(8,128)(2,1)S(1)}, u32[]{:S(2)}, u32[]{:S(2)}) collective-permute-start(bf16[80,128]{1,0:T(8,128)(2,1)} %get-tuple-element.26), channel_id=1, source_target_pairs={{0,12},{4,16},{8,20},{12,24},{16,28},{20,0},{24,4},{28,8},{1,13},{... | collective-permute-start | bytes 61448 | tf_op jit(solution)/shard_map/ppermute | solution.py:659
  25.2 2.4 %collective-permute-start.4 = (bf16[80,128]{1,0:T(8,128)(2,1)}, bf16[80,128]{1,0:T(8,128)(2,1)S(1)}, u32[]{:S(2)}, u32[]{:S(2)}) collective-permute-start(bf16[80,128]{1,0:T(8,128)(2,1)} %get-tuple-element.28), channel_id=1, source_target_pairs={{0,20},{4,24},{8,28},{12,0},{16,4},{20,8},{24,12},{28,16},{1,21},{... | collective-permute-start | bytes 61448 | tf_op jit(solution)/shard_map/ppermute | solution.py:659
  34.0 6.8 %all-to-all-start = ((bf16[8,80,128]{2,1,0:T(8,128)(2,1)}), bf16[8,80,128]{2,1,0:T(8,128)(2,1)S(1)}, u32[]{:S(2)}, u32[]{:S(2)}) async-start(bf16[8,80,128]{2,1,0:T(8,128)(2,1)} %get-tuple-element.31), calls=%async_computation | async-start | bytes 327680 | tf_op jit(solution)/shard_map/all_to_all | solution.py:671
  40.8 3.4 %pack.1 = (bf16[512,2048]{1,0:T(8,128)(2,1)}, bf16[256,512]{1,0:T(8,128)(2,1)}) custom-call(bf16[128,2048]{1,0:T(8,128)(2,1)} %x_ref.1, f32[1,2048]{1,0:T(1,128)} %bitcast.23, s32[2,128]{1,0:T(2,128)} %bitcast.26, f32[2,128]{1,0:T(2,128)} %bitcast.27), custom_call_target="tpu_custom_call" | custom-call | flops 2000000000 | bytes 3145728 | tf_op jit(solution)/shard_map/pack/pallas_call | solution.py:634
  44.2 7.4 %all-to-all-done.in_ref = bf16[8,80,128]{2,1,0:T(8,128)(2,1)S(1)} async-done(((bf16[8,80,128]{2,1,0:T(8,128)(2,1)}), bf16[8,80,128]{2,1,0:T(8,128)(2,1)S(1)}, u32[]{:S(2)}, u32[]{:S(2)}) %all-to-all-start) | async-done | bytes 163872 | tf_op jit(solution)/shard_map/all_to_all | solution.py:671
  51.6 6.0 %all-to-all-start.2 = ((bf16[64,8,2048]{2,1,0:T(8,128)(2,1)}), bf16[64,8,2048]{2,1,0:T(8,128)(2,1)S(1)}, u32[]{:S(2)}, u32[]{:S(2)}) async-start(bf16[64,8,2048]{2,1,0:T(8,128)(2,1)} %bitcast.21), calls=%async_computation.2 | async-start | bytes 4194304 | tf_op jit(solution)/shard_map/all_to_all | solution.py:671
  65.4 19.8 %collective-permute-done.10.refs_2_ = bf16[2048,256]{1,0:T(8,128)(2,1)} collective-permute-done((bf16[2048,256]{1,0:T(8,128)(2,1)}, bf16[2048,256]{1,0:T(8,128)(2,1)}, u32[]{:S(2)}, u32[]{:S(2)}) %collective-permute-start.10) | collective-permute-done | bytes 1048608 | tf_op jit(solution)/shard_map/ppermute | solution.py:659
  85.6 2.9 %collective-permute-start.15 = (bf16[2048,256]{1,0:T(8,128)(2,1)}, bf16[2048,256]{1,0:T(8,128)(2,1)}, u32[]{:S(2)}, u32[]{:S(2)}) collective-permute-start(bf16[2048,256]{1,0:T(8,128)(2,1)} %collective-permute-done.13.refs_5_), channel_id=1, source_target_pairs={{0,3},{1,0},{2,1},{3,2},{4,7},{5,4},{6,5},{7,6},{8,11},{9,8},{10,9... | collective-permute-start | bytes 3145736 | tf_op jit(solution)/shard_map/ppermute | solution.py:659
  88.5 8.0 %collective-permute-done.16.before_0 = bf16[256,1024]{1,0:T(8,128)(2,1)} collective-permute-done((bf16[256,1024]{1,0:T(8,128)(2,1)S(1)}, bf16[256,1024]{1,0:T(8,128)(2,1)}, u32[]{:S(2)}, u32[]{:S(2)}) %collective-permute-start.16) | collective-permute-done | bytes 524320 | tf_op jit(solution)/shard_map/ppermute | solution.py:659
  98.3 42.3 %collective-permute-done.19.after_1 = bf16[256,1024]{1,0:T(8,128)(2,1)S(1)} collective-permute-done((bf16[256,1024]{1,0:T(8,128)(2,1)}, bf16[256,1024]{1,0:T(8,128)(2,1)S(1)}, u32[]{:S(2)}, u32[]{:S(2)}) %collective-permute-start.19) | collective-permute-done | bytes 524320 | tf_op jit(solution)/shard_map/ppermute | solution.py:659
  143.8 2.9 %enter_states.1 = bf16[8,64,128]{2,1,0:T(8,128)(2,1)} custom-call(s32[1]{0:T(128)} %bitcast.1.here_ref, bf16[8,80,128]{2,1,0:T(8,128)(2,1)S(1)} %all-to-all-done.in_ref, f32[8,128,64]{2,1,0:T(8,128)} %get-tuple-element.32.prefix_ref), custom_call_target="tpu_custom_call" | custom-call | flops 2000000000 | bytes 1048576 | tf_op jit(solution)/shard_map/enter_states/pallas_call | solution.py:534
  146.7 4.8 %all-to-all-start.1 = ((bf16[8,64,128]{2,1,0:T(8,128)(2,1)}), bf16[8,64,128]{2,1,0:T(8,128)(2,1)S(1)}, u32[]{:S(2)}, u32[]{:S(2)}) async-start(bf16[8,64,128]{2,1,0:T(8,128)(2,1)} %enter_states.1), calls=%async_computation.1 | async-start | bytes 262144 | tf_op jit(solution)/shard_map/all_to_all | solution.py:671
  151.9 2.9 %collective-permute-start.21 = (bf16[256,1024]{1,0:T(8,128)(2,1)}, bf16[256,1024]{1,0:T(8,128)(2,1)S(1)}, u32[]{:S(2)}, u32[]{:S(2)}) collective-permute-start(bf16[256,1024]{1,0:T(8,128)(2,1)} %copy-done.3), channel_id=1, source_target_pairs={{0,3},{1,0},{2,1},{3,2},{4,7},{5,4},{6,5},{7,6},{8,11},{9,8},{10,9... | collective-permute-start | bytes 1572872 | tf_op jit(solution)/shard_map/ppermute | solution.py:659
  154.7 8.3 %hidden.1.hidden_ref.hidden_hbm = bf16[512,1024]{1,0:T(8,128)(2,1)} custom-call(bf16[512,2048]{1,0:T(8,128)(2,1)} %bitcast.20, bf16[2048,256]{1,0:T(8,128)(2,1)} %bitcast.11.refs_0_, bf16[2048,256]{1,0:T(8,128)(2,1)} %bitcast.12.refs_1_, bf16[2048,256]{1,0:T(8,128)(2,1)} %collective-permute-done.10.refs_2_, ...), custom_call_target="tpu_custom_call" | custom-call | flops 4294967296 | bytes 11534336 | tf_op jit(solution)/shard_map/hidden/pallas_call | solution.py:581
  163.1 4.8 %down_early.1.early_ref = bf16[512,2048]{1,0:T(8,128)(2,1)S(1)} custom-call(bf16[512,1024]{1,0:T(8,128)(2,1)} %hidden.1.hidden_ref.hidden_hbm, bf16[256,2048]{1,0:T(8,128)(2,1)} %bitcast.18, bf16[256,1024]{1,0:T(8,128)(2,1)} %collective-permute-done.16.before_0, bf16[256,1024]{1,0:T(8,128)(2,1)} %collective-permute-done.17.before_1, ...), custom_call_target="tpu_custom_call" | custom-call | flops 1610612736 | bytes 6291456 | tf_op jit(solution)/shard_map/down_early/pallas_call | solution.py:599
  167.8 2.7 %down_late.1 = bf16[512,2048]{1,0:T(8,128)(2,1)} custom-call(bf16[512,2048]{1,0:T(8,128)(2,1)S(1)} %down_early.1.early_ref, bf16[512,1024]{1,0:T(8,128)(2,1)} %hidden.1.hidden_ref.hidden_hbm, bf16[256,1024]{1,0:T(8,128)(2,1)S(1)} %collective-permute-done.20.far_0, bf16[256,1024]{1,0:T(8,128)(2,1)S(1)} %collective-permute-done.21.far_1), custom_call_target="tpu_custom_call" | custom-call | flops 536870912 | bytes 5242880 | tf_op jit(solution)/shard_map/down_late/pallas_call | solution.py:616
  170.6 10.5 %all-to-all-start.3 = ((bf16[64,8,2048]{2,1,0:T(8,128)(2,1)}), bf16[64,8,2048]{2,1,0:T(8,128)(2,1)S(1)}, u32[]{:S(2)}, u32[]{:S(2)}) async-start(bf16[64,8,2048]{2,1,0:T(8,128)(2,1)} %bitcast.17), calls=%async_computation.3 | async-start | bytes 4194304 | tf_op jit(solution)/shard_map/all_to_all | solution.py:671
  181.1 8.9 %readout.1 = (bf16[128,2048]{1,0:T(8,128)(2,1)}, bf16[128,2048]{1,0:T(8,128)(2,1)}, bf16[128,2048]{1,0:T(8,128)(2,1)}, bf16[128,2048]{1,0:T(8,128)(2,1)}) custom-call(s32[1]{0:T(128)} %bitcast.here_ref, bf16[8,64,128]{2,1,0:T(8,128)(2,1)S(1)} %all-to-all-done.1.enter_ref, bf16[512,512]{1,0:T(8,128)(2,1)} %get-tuple-element.33.reader_ref, ...), custom_call_target="tpu_custom_call" | custom-call | flops 5000000000 | bytes 8388608 | tf_op jit(solution)/shard_map/readout/pallas_call | solution.py:550
  192.9 22.1 %collective-permute-done.9 = bf16[128,2048]{1,0:T(8,128)(2,1)S(1)} collective-permute-done((bf16[128,2048]{1,0:T(8,128)(2,1)}, bf16[128,2048]{1,0:T(8,128)(2,1)S(1)}, u32[]{:S(2)}, u32[]{:S(2)}) %collective-permute-start.9) | collective-permute-done | bytes 524320 | tf_op jit(solution)/shard_map/ppermute | solution.py:659
  215.0 3.3 %collective-permute-done.7 = bf16[128,2048]{1,0:T(8,128)(2,1)S(1)} collective-permute-done((bf16[128,2048]{1,0:T(8,128)(2,1)}, bf16[128,2048]{1,0:T(8,128)(2,1)S(1)}, u32[]{:S(2)}, u32[]{:S(2)}) %collective-permute-start.7) | collective-permute-done | bytes 524320 | tf_op jit(solution)/shard_map/ppermute | solution.py:659
  218.3 2.2 add_convert_fusion
  220.4 11.9 %all-to-all-done.3 = bf16[64,8,2048]{2,1,0:T(8,128)(2,1)S(1)} async-done(((bf16[64,8,2048]{2,1,0:T(8,128)(2,1)}), bf16[64,8,2048]{2,1,0:T(8,128)(2,1)S(1)}, u32[]{:S(2)}, u32[]{:S(2)}) %all-to-all-start.3) | async-done | bytes 2097184 | tf_op jit(solution)/shard_map/all_to_all | solution.py:671
  232.3 2.5 %combine.1 = bf16[128,2048]{1,0:T(8,128)(2,1)} custom-call(bf16[256,512]{1,0:T(8,128)(2,1)} %get-tuple-element.42.mix_ref, bf16[512,2048]{1,0:T(8,128)(2,1)S(1)} %bitcast.16), custom_call_target="tpu_custom_call" | custom-call | flops 1000000000 | bytes 3145728 | tf_op jit(solution)/shard_map/combine/pallas_call | solution.py:647
  (49 shorter events, 25.3 us)
Async XLA Ops:
  20.2 7.4 %collective-permute-start = (bf16[80,128]{1,0:T(8,128)(2,1)}, bf16[80,128]{1,0:T(8,128)(2,1)S(1)}, u32[]{:S(2)}, u32[]{:S(2)}) collective-permute-start(bf16[80,128]{1,0:T(8,128)(2,1)} %get-tuple-element.24), channel_id=1, source_target_pairs={{0,4},{4,8},{8,12},{12,16},{16,20},{20,24},{24,28},{28,0},{1,5},{5... | collective-permute-start | bytes 61448 | tf_op jit(solution)/shard_map/ppermute | solution.py:659
  20.2 7.8 %collective-permute-start.1 = (bf16[80,128]{1,0:T(8,128)(2,1)}, bf16[80,128]{1,0:T(8,128)(2,1)S(1)}, u32[]{:S(2)}, u32[]{:S(2)}) collective-permute-start(bf16[80,128]{1,0:T(8,128)(2,1)} %get-tuple-element.25), channel_id=1, source_target_pairs={{0,8},{4,12},{8,16},{12,20},{16,24},{20,28},{24,0},{28,4},{1,9},{5... | collective-permute-start | bytes 61448 | tf_op jit(solution)/shard_map/ppermute | solution.py:659
  21.7 7.2 %collective-permute-start.2 = (bf16[80,128]{1,0:T(8,128)(2,1)}, bf16[80,128]{1,0:T(8,128)(2,1)S(1)}, u32[]{:S(2)}, u32[]{:S(2)}) collective-permute-start(bf16[80,128]{1,0:T(8,128)(2,1)} %get-tuple-element.26), channel_id=1, source_target_pairs={{0,12},{4,16},{8,20},{12,24},{16,28},{20,0},{24,4},{28,8},{1,13},{... | collective-permute-start | bytes 61448 | tf_op jit(solution)/shard_map/ppermute | solution.py:659
  24.5 5.6 %collective-permute-start.3 = (bf16[80,128]{1,0:T(8,128)(2,1)}, bf16[80,128]{1,0:T(8,128)(2,1)S(1)}, u32[]{:S(2)}, u32[]{:S(2)}) collective-permute-start(bf16[80,128]{1,0:T(8,128)(2,1)} %get-tuple-element.27), channel_id=1, source_target_pairs={{0,16},{4,20},{8,24},{12,28},{16,0},{20,4},{24,8},{28,12},{1,17},{... | collective-permute-start | bytes 61448 | tf_op jit(solution)/shard_map/ppermute | solution.py:659
  25.2 4.9 %collective-permute-start.4 = (bf16[80,128]{1,0:T(8,128)(2,1)}, bf16[80,128]{1,0:T(8,128)(2,1)S(1)}, u32[]{:S(2)}, u32[]{:S(2)}) collective-permute-start(bf16[80,128]{1,0:T(8,128)(2,1)} %get-tuple-element.28), channel_id=1, source_target_pairs={{0,20},{4,24},{8,28},{12,0},{16,4},{20,8},{24,12},{28,16},{1,21},{... | collective-permute-start | bytes 61448 | tf_op jit(solution)/shard_map/ppermute | solution.py:659
  34.0 17.6 %all-to-all-start = ((bf16[8,80,128]{2,1,0:T(8,128)(2,1)}), bf16[8,80,128]{2,1,0:T(8,128)(2,1)S(1)}, u32[]{:S(2)}, u32[]{:S(2)}) async-start(bf16[8,80,128]{2,1,0:T(8,128)(2,1)} %get-tuple-element.31), calls=%async_computation | async-start | bytes 327680 | tf_op jit(solution)/shard_map/all_to_all | solution.py:671
  51.6 95.1 %all-to-all-start.2 = ((bf16[64,8,2048]{2,1,0:T(8,128)(2,1)}), bf16[64,8,2048]{2,1,0:T(8,128)(2,1)S(1)}, u32[]{:S(2)}, u32[]{:S(2)}) async-start(bf16[64,8,2048]{2,1,0:T(8,128)(2,1)} %bitcast.21), calls=%async_computation.2 | async-start | bytes 4194304 | tf_op jit(solution)/shard_map/all_to_all | solution.py:671
  57.6 27.6 %collective-permute-start.10 = (bf16[2048,256]{1,0:T(8,128)(2,1)}, bf16[2048,256]{1,0:T(8,128)(2,1)}, u32[]{:S(2)}, u32[]{:S(2)}) collective-permute-start(bf16[2048,256]{1,0:T(8,128)(2,1)} %bitcast.11.refs_0_), channel_id=1, source_target_pairs={{0,1},{1,2},{2,3},{3,0},{4,5},{5,6},{6,7},{7,4},{8,9},{9,10},{10,1... | collective-permute-start | bytes 3145736 | tf_op jit(solution)/shard_map/ppermute | solution.py:659
  59.2 26.3 %collective-permute-start.13 = (bf16[2048,256]{1,0:T(8,128)(2,1)}, bf16[2048,256]{1,0:T(8,128)(2,1)}, u32[]{:S(2)}, u32[]{:S(2)}) collective-permute-start(bf16[2048,256]{1,0:T(8,128)(2,1)} %bitcast.12.refs_1_), channel_id=1, source_target_pairs={{0,3},{1,0},{2,1},{3,2},{4,7},{5,4},{6,5},{7,6},{8,11},{9,8},{10,9... | collective-permute-start | bytes 3145736 | tf_op jit(solution)/shard_map/ppermute | solution.py:659
  61.8 34.6 %collective-permute-start.16 = (bf16[256,1024]{1,0:T(8,128)(2,1)S(1)}, bf16[256,1024]{1,0:T(8,128)(2,1)}, u32[]{:S(2)}, u32[]{:S(2)}) collective-permute-start(bf16[256,1024]{1,0:T(8,128)(2,1)S(1)} %get-tuple-element.45), channel_id=1, source_target_pairs={{0,1},{1,2},{2,3},{3,0},{4,5},{5,6},{6,7},{7,4},{8,9},{9,10},{10,1... | collective-permute-start | bytes 1572872 | tf_op jit(solution)/shard_map/ppermute | solution.py:659
  62.2 79.9 %collective-permute-start.11 = (bf16[2048,256]{1,0:T(8,128)(2,1)}, bf16[2048,256]{1,0:T(8,128)(2,1)}, u32[]{:S(2)}, u32[]{:S(2)}) collective-permute-start(bf16[2048,256]{1,0:T(8,128)(2,1)} %bitcast.12.refs_1_), channel_id=1, source_target_pairs={{0,1},{1,2},{2,3},{3,0},{4,5},{5,6},{6,7},{7,4},{8,9},{9,10},{10,1... | collective-permute-start | bytes 3145736 | tf_op jit(solution)/shard_map/ppermute | solution.py:659
  63.8 87.7 %collective-permute-start.12 = (bf16[2048,256]{1,0:T(8,128)(2,1)}, bf16[2048,256]{1,0:T(8,128)(2,1)}, u32[]{:S(2)}, u32[]{:S(2)}) collective-permute-start(bf16[2048,256]{1,0:T(8,128)(2,1)} %bitcast.11.refs_0_), channel_id=1, source_target_pairs={{0,3},{1,0},{2,1},{3,2},{4,7},{5,4},{6,5},{7,6},{8,11},{9,8},{10,9... | collective-permute-start | bytes 3145736 | tf_op jit(solution)/shard_map/ppermute | solution.py:659
  85.2 66.6 %collective-permute-start.14 = (bf16[2048,256]{1,0:T(8,128)(2,1)}, bf16[2048,256]{1,0:T(8,128)(2,1)}, u32[]{:S(2)}, u32[]{:S(2)}) collective-permute-start(bf16[2048,256]{1,0:T(8,128)(2,1)} %collective-permute-done.10.refs_2_), channel_id=1, source_target_pairs={{0,1},{1,2},{2,3},{3,0},{4,5},{5,6},{6,7},{7,4},{8,9},{9,10},{10,1... | collective-permute-start | bytes 3145736 | tf_op jit(solution)/shard_map/ppermute | solution.py:659
  85.6 69.1 %collective-permute-start.15 = (bf16[2048,256]{1,0:T(8,128)(2,1)}, bf16[2048,256]{1,0:T(8,128)(2,1)}, u32[]{:S(2)}, u32[]{:S(2)}) collective-permute-start(bf16[2048,256]{1,0:T(8,128)(2,1)} %collective-permute-done.13.refs_5_), channel_id=1, source_target_pairs={{0,3},{1,0},{2,1},{3,2},{4,7},{5,4},{6,5},{7,6},{8,11},{9,8},{10,9... | collective-permute-start | bytes 3145736 | tf_op jit(solution)/shard_map/ppermute | solution.py:659
  96.5 44.1 %collective-permute-start.19 = (bf16[256,1024]{1,0:T(8,128)(2,1)}, bf16[256,1024]{1,0:T(8,128)(2,1)S(1)}, u32[]{:S(2)}, u32[]{:S(2)}) collective-permute-start(bf16[256,1024]{1,0:T(8,128)(2,1)} %get-tuple-element.44), channel_id=1, source_target_pairs={{0,3},{1,0},{2,1},{3,2},{4,7},{5,4},{6,5},{7,6},{8,11},{9,8},{10,9... | collective-permute-start | bytes 1572872 | tf_op jit(solution)/shard_map/ppermute | solution.py:659
  140.5 22.5 %collective-permute-start.17 = (bf16[256,1024]{1,0:T(8,128)(2,1)}, bf16[256,1024]{1,0:T(8,128)(2,1)}, u32[]{:S(2)}, u32[]{:S(2)}) collective-permute-start(bf16[256,1024]{1,0:T(8,128)(2,1)} %get-tuple-element.44), channel_id=1, source_target_pairs={{0,1},{1,2},{2,3},{3,0},{4,5},{5,6},{6,7},{7,4},{8,9},{9,10},{10,1... | collective-permute-start | bytes 1572872 | tf_op jit(solution)/shard_map/ppermute | solution.py:659
  142.1 20.9 %collective-permute-start.18 = (bf16[256,1024]{1,0:T(8,128)(2,1)}, bf16[256,1024]{1,0:T(8,128)(2,1)}, u32[]{:S(2)}, u32[]{:S(2)}) collective-permute-start(bf16[256,1024]{1,0:T(8,128)(2,1)} %copy-done.4), channel_id=1, source_target_pairs={{0,3},{1,0},{2,1},{3,2},{4,7},{5,4},{6,5},{7,6},{8,11},{9,8},{10,9... | collective-permute-start | bytes 1572872 | tf_op jit(solution)/shard_map/ppermute | solution.py:659
  146.7 23.9 %all-to-all-start.1 = ((bf16[8,64,128]{2,1,0:T(8,128)(2,1)}), bf16[8,64,128]{2,1,0:T(8,128)(2,1)S(1)}, u32[]{:S(2)}, u32[]{:S(2)}) async-start(bf16[8,64,128]{2,1,0:T(8,128)(2,1)} %enter_states.1), calls=%async_computation.1 | async-start | bytes 262144 | tf_op jit(solution)/shard_map/all_to_all | solution.py:671
  151.5 16.3 %collective-permute-start.20 = (bf16[256,1024]{1,0:T(8,128)(2,1)}, bf16[256,1024]{1,0:T(8,128)(2,1)S(1)}, u32[]{:S(2)}, u32[]{:S(2)}) collective-permute-start(bf16[256,1024]{1,0:T(8,128)(2,1)} %collective-permute-done.16.before_0), channel_id=1, source_target_pairs={{0,1},{1,2},{2,3},{3,0},{4,5},{5,6},{6,7},{7,4},{8,9},{9,10},{10,1... | collective-permute-start | bytes 1572872 | tf_op jit(solution)/shard_map/ppermute | solution.py:659
  151.9 16.0 %collective-permute-start.21 = (bf16[256,1024]{1,0:T(8,128)(2,1)}, bf16[256,1024]{1,0:T(8,128)(2,1)S(1)}, u32[]{:S(2)}, u32[]{:S(2)}) collective-permute-start(bf16[256,1024]{1,0:T(8,128)(2,1)} %copy-done.3), channel_id=1, source_target_pairs={{0,3},{1,0},{2,1},{3,2},{4,7},{5,4},{6,5},{7,6},{8,11},{9,8},{10,9... | collective-permute-start | bytes 1572872 | tf_op jit(solution)/shard_map/ppermute | solution.py:659
  170.6 61.8 %all-to-all-start.3 = ((bf16[64,8,2048]{2,1,0:T(8,128)(2,1)}), bf16[64,8,2048]{2,1,0:T(8,128)(2,1)S(1)}, u32[]{:S(2)}, u32[]{:S(2)}) async-start(bf16[64,8,2048]{2,1,0:T(8,128)(2,1)} %bitcast.17), calls=%async_computation.3 | async-start | bytes 4194304 | tf_op jit(solution)/shard_map/all_to_all | solution.py:671
  190.0 25.0 %collective-permute-start.9 = (bf16[128,2048]{1,0:T(8,128)(2,1)}, bf16[128,2048]{1,0:T(8,128)(2,1)S(1)}, u32[]{:S(2)}, u32[]{:S(2)}) collective-permute-start(bf16[128,2048]{1,0:T(8,128)(2,1)} %get-tuple-element.41), channel_id=1, source_target_pairs={{0,3},{1,0},{2,1},{3,2},{4,7},{5,4},{6,5},{7,6},{8,11},{9,8},{10,9... | collective-permute-start | bytes 1572872 | tf_op jit(solution)/shard_map/ppermute | solution.py:659
  192.0 23.1 %collective-permute-start.8 = (bf16[128,2048]{1,0:T(8,128)(2,1)}, bf16[128,2048]{1,0:T(8,128)(2,1)S(1)}, u32[]{:S(2)}, u32[]{:S(2)}) collective-permute-start(bf16[128,2048]{1,0:T(8,128)(2,1)} %get-tuple-element.40), channel_id=1, source_target_pairs={{0,2},{1,3},{2,0},{3,1},{4,6},{5,7},{6,4},{7,5},{8,10},{9,11},{10,... | collective-permute-start | bytes 1572872 | tf_op jit(solution)/shard_map/ppermute | solution.py:659
  192.0 26.3 %collective-permute-start.7 = (bf16[128,2048]{1,0:T(8,128)(2,1)}, bf16[128,2048]{1,0:T(8,128)(2,1)S(1)}, u32[]{:S(2)}, u32[]{:S(2)}) collective-permute-start(bf16[128,2048]{1,0:T(8,128)(2,1)} %get-tuple-element.39), channel_id=1, source_target_pairs={{0,1},{1,2},{2,3},{3,0},{4,5},{5,6},{6,7},{7,4},{8,9},{9,10},{10,1... | collective-permute-start | bytes 1572872 | tf_op jit(solution)/shard_map/ppermute | solution.py:659
  (7 other events, 66.4 us)

commit v5 on v4

--- a/solution.py
+++ b/solution.py
@@ -373,7 +373,7 @@
 
 
 def down_early_kernel(
-    hidden_ref, own, before_0, before_1, after_0, after_1, out_ref, weight_ref, sems
+    hidden_ref, own, before_0, before_1, after_0, after_1, out_ref, last_ref, weight_ref, sems
 ):
     units, width = own.shape
     half = width // 2
@@ -392,6 +392,7 @@
     ]
     for fetch in fetches:
         fetch.start()
+    last_ref[...] = hidden_ref[:, 3 * units :]
     for part, waits in ((0, fetches[:3]), (1, fetches[3:])):
         for fetch in waits:
             fetch.wait()
@@ -399,18 +400,10 @@
         out_ref[:, lanes] = dot(hidden_ref[:, : 3 * units], weight_ref[:, lanes]).astype(BF16)
 
 
-def down_late_kernel(
-    early_ref, hidden_hbm, far_0, far_1, out_hbm, hidden_ref, made_ref, hidden_sem, sems
-):
-    units = hidden_ref.shape[1]
+def down_late_kernel(early_ref, hidden_ref, far_0, far_1, out_hbm, made_ref, sems):
     width = made_ref.shape[1]
     parts = 4
     tile = width // parts
-    fetch = pltpu.make_async_copy(
-        hidden_hbm.at[:, hidden_hbm.shape[1] - units :], hidden_ref, hidden_sem
-    )
-    fetch.start()
-    fetch.wait()
     stores = []
     for part in range(parts):
         far = (far_0, far_1)[part // 2]
@@ -457,10 +450,20 @@
     mix_out_ref[tokens:, :] = rest
 
 
-def combine_kernel(mix_ref, rows_ref, out_ref):
-    tokens = out_ref.shape[0]
-    both = dot(mix_ref[...], rows_ref[...])
-    out_ref[...] = (both[:tokens] + both[tokens:]).astype(BF16)
+def combine_kernel(mix_ref, rows_ref, out_hbm, made_ref, sems):
+    tokens, width = made_ref.shape
+    parts = 4
+    tile = width // parts
+    stores = []
+    for part in range(parts):
+        lanes = slice(part * tile, (part + 1) * tile)
+        both = dot(mix_ref[...], rows_ref[:, lanes])
+        made_ref[:, lanes] = (both[:tokens] + both[tokens:]).astype(BF16)
+        store = pltpu.make_async_copy(made_ref.at[:, lanes], out_hbm.at[:, lanes], sems.at[part])
+        store.start()
+        stores.append(store)
+    for store in stores:
+        store.wait()
 
 
 def whole(shape):
@@ -599,8 +602,8 @@
     return pl.pallas_call(
         down_early_kernel,
         in_specs=[IN_VMEM] + [IN_HBM] * 5,
-        out_specs=IN_VMEM,
-        out_shape=pltpu.VMEM((rows, width), BF16),
+        out_specs=[IN_VMEM, IN_VMEM],
+        out_shape=[pltpu.VMEM((rows, width), BF16), pltpu.VMEM((rows, units), BF16)],
         scratch_shapes=[
             pltpu.VMEM((3 * units, width), BF16),
             pltpu.SemaphoreType.DMA((5,)),
@@ -615,18 +618,16 @@
     units = far[0].shape[0]
     return pl.pallas_call(
         down_late_kernel,
-        in_specs=[IN_VMEM, IN_HBM, IN_VMEM, IN_VMEM],
+        in_specs=[IN_VMEM] * 4,
         out_specs=IN_HBM,
         out_shape=jax.ShapeDtypeStruct((rows, width), BF16),
         scratch_shapes=[
-            pltpu.VMEM((rows, units), BF16),
             pltpu.VMEM((rows, width), BF16),
-            pltpu.SemaphoreType.DMA,
             pltpu.SemaphoreType.DMA((4,)),
         ],
         cost_estimate=estimate(2 * rows * units * width, 5 << 20),
         name="down_late",
-    )(in_vmem(early), hidden, *map(in_vmem, far))
+    )(in_vmem(early), in_vmem(hidden), *map(in_vmem, far))
 
 
 def pack_rows(x, gain, routes, mix, places):
@@ -644,11 +645,13 @@
 
 def combine_rows(mix, rows):
     tokens = mix.shape[0] // 2
+    width = rows.shape[1]
     return pl.pallas_call(
         combine_kernel,
         in_specs=[IN_VMEM, IN_VMEM],
-        out_specs=IN_VMEM,
-        out_shape=jax.ShapeDtypeStruct((tokens, rows.shape[1]), BF16),
+        out_specs=IN_HBM,
+        out_shape=jax.ShapeDtypeStruct((tokens, width), BF16),
+        scratch_shapes=[pltpu.VMEM((tokens, width), BF16), pltpu.SemaphoreType.DMA((4,))],
         cost_estimate=estimate(1.0e9, 3 << 20),
         name="combine",
     )(mix, in_vmem(rows))
@@ -726,9 +729,7 @@
         decay_base.reshape(1, -1),
         decay_shift.T,
     )
-    prefixes, totals = group_scan(
-        here(GROUP), around(messages, GROUP), lax.axis_size("ep_0")
-    )
+    prefixes, totals = group_scan(here(GROUP), around(messages, GROUP), lax.axis_size("ep_0"))
     entered = enter_states(here("ep_0"), exchange(totals, "ep_0"), prefixes)
     partial = read_and_project(
         here("tp"),
@@ -747,8 +748,8 @@
     hiddens = expert_hidden(
         arrived, [w_gate, w_up, gate_r, up_r, gate_l, up_l, gate_f, up_f]
     )
-    early = expert_down_early(hiddens, w_down, (down_0r, down_1r), (down_0l, down_1l))
-    returning = expert_down_late(early, hiddens, (down_0f, down_1f))
+    early, last = expert_down_early(hiddens, w_down, (down_0r, down_1r), (down_0l, down_1l))
+    returning = expert_down_late(early, last, (down_0f, down_1f))
     returned = exchange(returning.reshape(ep_count, CAPACITY, model_width), EP)
     return (mixer_out, combine_rows(mix, returned.reshape(places, model_width)))
 

time: 236 us -> 235 us (level)
  no operation moved by 1% of the time
where the time goes in v5:
time: 235 us; the launch traced here: 234 us
  waiting for transfers between devices  117 us (50%)
  starting transfers between devices  58.3 us (25%)
  Pallas kernels  53.6 us (23%)
    ppermute x22, waiting for transfers between devices, ring(): lax.ppermute(x, axis, [(i, (i + shift) % count) for i in range(count)])  98 us
    ppermute x22, starting transfers between devices, ring(): lax.ppermute(x, axis, [(i, (i + shift) % count) for i in range(count)])  30.2 us
    all_to_all x4, starting transfers between devices, exchange(): return lax.all_to_all(x, axis, 0, 0, tiled=True)  28.1 us
    pallas_call x1, Pallas kernels, summarize(): pl.pallas_call(summary_kernel, grid=(spans,), in_specs=[SCALARS] + [block...  19.5 us
    all_to_all x4, waiting for transfers between devices, exchange(): return lax.all_to_all(x, axis, 0, 0, tiled=True)  19.3 us
    pallas_call x1, Pallas kernels, read_and_project(): pl.pallas_call(readout_kernel, grid=(spans,), in_specs=[SCALARS, IN_VMEM,...  8.9 us
    pallas_call x1, Pallas kernels, expert_hidden(): pl.pallas_call(hidden_kernel, in_specs=[IN_HBM] * (1 + count), out_specs=...  8.3 us
    pallas_call x1, Pallas kernels, expert_down_early(): pl.pallas_call(down_early_kernel, in_specs=[IN_VMEM] + [IN_HBM] * 5, out_...  4.75 us
  transfers between devices with their start and end apart: 26, of which 9 were waited for; matrix products, arithmetic and copies ran while one was open for 1% of the time, Pallas kernels for 13%

profile of v5, /device:TPU:2, one launch (start us, length us, event | category | flops | bytes accessed | tf_op | source)
XLA Modules:
  0.0 234.1 jit_solution(7392582792481200374)
XLA Ops:
  0.6 19.5 %summary.1 = (bf16[512,512]{1,0:T(8,128)(2,1)}, f32[512,512]{1,0:T(8,128)}, bf16[4,4,128,128]{3,2,1,0:T(8,128)(2,1)}, f32[4,4,128,128]{3,2,1,0:T(8,128)}, f32[4,...) custom-call(s32[1]{0:T(128)} %bitcast.2.here_ref, ...), custom_call_target="tpu_custom_call" | custom-call | flops 20000000000 | bytes 6291456 | tf_op jit(solution)/shard_map/summary/pallas_call | solution.py:489
  21.7 2.7 %collective-permute-start.2 = (bf16[80,128]{1,0:T(8,128)(2,1)}, bf16[80,128]{1,0:T(8,128)(2,1)S(1)}, u32[]{:S(2)}, u32[]{:S(2)}) collective-permute-start(bf16[80,128]{1,0:T(8,128)(2,1)} %get-tuple-element.28), channel_id=1, source_target_pairs={{0,12},{4,16},{8,20},{12,24},{16,28},{20,0},{24,4},{28,8},{1,13},{... | collective-permute-start | bytes 61448 | tf_op jit(solution)/shard_map/ppermute | solution.py:662
  25.2 2.4 %collective-permute-start.4 = (bf16[80,128]{1,0:T(8,128)(2,1)}, bf16[80,128]{1,0:T(8,128)(2,1)S(1)}, u32[]{:S(2)}, u32[]{:S(2)}) collective-permute-start(bf16[80,128]{1,0:T(8,128)(2,1)} %get-tuple-element.30), channel_id=1, source_target_pairs={{0,20},{4,24},{8,28},{12,0},{16,4},{20,8},{24,12},{28,16},{1,21},{... | collective-permute-start | bytes 61448 | tf_op jit(solution)/shard_map/ppermute | solution.py:662
  34.0 6.8 %all-to-all-start = ((bf16[8,80,128]{2,1,0:T(8,128)(2,1)}), bf16[8,80,128]{2,1,0:T(8,128)(2,1)S(1)}, u32[]{:S(2)}, u32[]{:S(2)}) async-start(bf16[8,80,128]{2,1,0:T(8,128)(2,1)} %get-tuple-element.33), calls=%async_computation | async-start | bytes 327680 | tf_op jit(solution)/shard_map/all_to_all | solution.py:674
  40.8 3.4 %pack.1 = (bf16[512,2048]{1,0:T(8,128)(2,1)}, bf16[256,512]{1,0:T(8,128)(2,1)}) custom-call(bf16[128,2048]{1,0:T(8,128)(2,1)} %x_ref.1, f32[1,2048]{1,0:T(1,128)} %bitcast.23, s32[2,128]{1,0:T(2,128)} %bitcast.26, f32[2,128]{1,0:T(2,128)} %bitcast.27), custom_call_target="tpu_custom_call" | custom-call | flops 2000000000 | bytes 3145728 | tf_op jit(solution)/shard_map/pack/pallas_call | solution.py:635
  44.2 7.4 %all-to-all-done.in_ref = bf16[8,80,128]{2,1,0:T(8,128)(2,1)S(1)} async-done(((bf16[8,80,128]{2,1,0:T(8,128)(2,1)}), bf16[8,80,128]{2,1,0:T(8,128)(2,1)S(1)}, u32[]{:S(2)}, u32[]{:S(2)}) %all-to-all-start) | async-done | bytes 163872 | tf_op jit(solution)/shard_map/all_to_all | solution.py:674
  51.6 6.0 %all-to-all-start.2 = ((bf16[64,8,2048]{2,1,0:T(8,128)(2,1)}), bf16[64,8,2048]{2,1,0:T(8,128)(2,1)S(1)}, u32[]{:S(2)}, u32[]{:S(2)}) async-start(bf16[64,8,2048]{2,1,0:T(8,128)(2,1)} %bitcast.19), calls=%async_computation.2 | async-start | bytes 4194304 | tf_op jit(solution)/shard_map/all_to_all | solution.py:674
  65.6 19.6 %collective-permute-done.10.refs_2_ = bf16[2048,256]{1,0:T(8,128)(2,1)} collective-permute-done((bf16[2048,256]{1,0:T(8,128)(2,1)}, bf16[2048,256]{1,0:T(8,128)(2,1)}, u32[]{:S(2)}, u32[]{:S(2)}) %collective-permute-start.10) | collective-permute-done | bytes 1048608 | tf_op jit(solution)/shard_map/ppermute | solution.py:662
  85.6 2.9 %collective-permute-start.15 = (bf16[2048,256]{1,0:T(8,128)(2,1)}, bf16[2048,256]{1,0:T(8,128)(2,1)}, u32[]{:S(2)}, u32[]{:S(2)}) collective-permute-start(bf16[2048,256]{1,0:T(8,128)(2,1)} %collective-permute-done.13.refs_5_), channel_id=1, source_target_pairs={{0,3},{1,0},{2,1},{3,2},{4,7},{5,4},{6,5},{7,6},{8,11},{9,8},{10,9... | collective-permute-start | bytes 3145736 | tf_op jit(solution)/shard_map/ppermute | solution.py:662
  88.5 8.0 %collective-permute-done.16.before_0 = bf16[256,1024]{1,0:T(8,128)(2,1)} collective-permute-done((bf16[256,1024]{1,0:T(8,128)(2,1)}, bf16[256,1024]{1,0:T(8,128)(2,1)}, u32[]{:S(2)}, u32[]{:S(2)}) %collective-permute-start.16) | collective-permute-done | bytes 524320 | tf_op jit(solution)/shard_map/ppermute | solution.py:662
  98.3 42.4 %collective-permute-done.19.after_1 = bf16[256,1024]{1,0:T(8,128)(2,1)} collective-permute-done((bf16[256,1024]{1,0:T(8,128)(2,1)}, bf16[256,1024]{1,0:T(8,128)(2,1)}, u32[]{:S(2)}, u32[]{:S(2)}) %collective-permute-start.19) | collective-permute-done | bytes 524320 | tf_op jit(solution)/shard_map/ppermute | solution.py:662
  143.9 2.9 %enter_states.1 = bf16[8,64,128]{2,1,0:T(8,128)(2,1)} custom-call(s32[1]{0:T(128)} %bitcast.1.here_ref, bf16[8,80,128]{2,1,0:T(8,128)(2,1)S(1)} %all-to-all-done.in_ref, f32[8,128,64]{2,1,0:T(8,128)} %get-tuple-element.34.prefix_ref), custom_call_target="tpu_custom_call" | custom-call | flops 2000000000 | bytes 1048576 | tf_op jit(solution)/shard_map/enter_states/pallas_call | solution.py:537
  146.8 4.8 %all-to-all-start.1 = ((bf16[8,64,128]{2,1,0:T(8,128)(2,1)}), bf16[8,64,128]{2,1,0:T(8,128)(2,1)S(1)}, u32[]{:S(2)}, u32[]{:S(2)}) async-start(bf16[8,64,128]{2,1,0:T(8,128)(2,1)} %enter_states.1), calls=%async_computation.1 | async-start | bytes 262144 | tf_op jit(solution)/shard_map/all_to_all | solution.py:674
  152.0 2.9 %collective-permute-start.21 = (bf16[256,1024]{1,0:T(8,128)(2,1)}, bf16[256,1024]{1,0:T(8,128)(2,1)S(1)}, u32[]{:S(2)}, u32[]{:S(2)}) collective-permute-start(bf16[256,1024]{1,0:T(8,128)(2,1)} %collective-permute-done.19.after_1), channel_id=1, source_target_pairs={{0,3},{1,0},{2,1},{3,2},{4,7},{5,4},{6,5},{7,6},{8,11},{9,8},{10,9... | collective-permute-start | bytes 1572872 | tf_op jit(solution)/shard_map/ppermute | solution.py:662
  154.9 8.3 %hidden.1.hidden_ref = bf16[512,1024]{1,0:T(8,128)(2,1)} custom-call(bf16[512,2048]{1,0:T(8,128)(2,1)} %bitcast.18, bf16[2048,256]{1,0:T(8,128)(2,1)} %bitcast.11.refs_0_, bf16[2048,256]{1,0:T(8,128)(2,1)} %bitcast.12.refs_1_, bf16[2048,256]{1,0:T(8,128)(2,1)} %collective-permute-done.10.refs_2_, bf16[2048,256]{1,0:T(8,128)(2,1)} %copy-done.3, ...), custom_call_target="tpu_custom_call" | custom-call | flops 4294967296 | bytes 11534336 | tf_op jit(solution)/shard_map/hidden/pallas_call | solution.py:584
  163.2 4.8 %down_early.1 = (bf16[512,2048]{1,0:T(8,128)(2,1)S(1)}, bf16[512,256]{1,0:T(8,128)(2,1)S(1)}) custom-call(bf16[512,1024]{1,0:T(8,128)(2,1)} %hidden.1.hidden_ref, bf16[256,2048]{1,0:T(8,128)(2,1)} %bitcast.20, bf16[256,1024]{1,0:T(8,128)(2,1)} %collective-permute-done.16.before_0, bf16[256,1024]{1,0:T(8,128)(2,1)} %collective-permute-done.17.before_1, ...), custom_call_target="tpu_custom_call" | custom-call | flops 1610612736 | bytes 6291456 | tf_op jit(solution)/shard_map/down_early/pallas_call | solution.py:602
  169.8 10.5 %all-to-all-start.3 = ((bf16[64,8,2048]{2,1,0:T(8,128)(2,1)}), bf16[64,8,2048]{2,1,0:T(8,128)(2,1)S(1)}, u32[]{:S(2)}, u32[]{:S(2)}) async-start(bf16[64,8,2048]{2,1,0:T(8,128)(2,1)} %bitcast.17), calls=%async_computation.3 | async-start | bytes 4194304 | tf_op jit(solution)/shard_map/all_to_all | solution.py:674
  180.3 8.9 %readout.1 = (bf16[128,2048]{1,0:T(8,128)(2,1)}, bf16[128,2048]{1,0:T(8,128)(2,1)}, bf16[128,2048]{1,0:T(8,128)(2,1)}, bf16[128,2048]{1,0:T(8,128)(2,1)}) custom-call(s32[1]{0:T(128)} %bitcast.here_ref, bf16[8,64,128]{2,1,0:T(8,128)(2,1)S(1)} %all-to-all-done.1.enter_ref, bf16[512,512]{1,0:T(8,128)(2,1)} %get-tuple-element.35.reader_ref, ...), custom_call_target="tpu_custom_call" | custom-call | flops 5000000000 | bytes 8388608 | tf_op jit(solution)/shard_map/readout/pallas_call | solution.py:553
  189.2 2.0 collective-permute-start.9
  192.1 22.1 %collective-permute-done.9 = bf16[128,2048]{1,0:T(8,128)(2,1)S(1)} collective-permute-done((bf16[128,2048]{1,0:T(8,128)(2,1)}, bf16[128,2048]{1,0:T(8,128)(2,1)S(1)}, u32[]{:S(2)}, u32[]{:S(2)}) %collective-permute-start.9) | collective-permute-done | bytes 524320 | tf_op jit(solution)/shard_map/ppermute | solution.py:662
  214.2 3.3 %collective-permute-done.7 = bf16[128,2048]{1,0:T(8,128)(2,1)S(1)} collective-permute-done((bf16[128,2048]{1,0:T(8,128)(2,1)}, bf16[128,2048]{1,0:T(8,128)(2,1)S(1)}, u32[]{:S(2)}, u32[]{:S(2)}) %collective-permute-start.7) | collective-permute-done | bytes 524320 | tf_op jit(solution)/shard_map/ppermute | solution.py:662
  217.5 2.2 add_convert_fusion
  219.7 11.9 %all-to-all-done.3 = bf16[64,8,2048]{2,1,0:T(8,128)(2,1)S(1)} async-done(((bf16[64,8,2048]{2,1,0:T(8,128)(2,1)}), bf16[64,8,2048]{2,1,0:T(8,128)(2,1)S(1)}, u32[]{:S(2)}, u32[]{:S(2)}) %all-to-all-start.3) | async-done | bytes 2097184 | tf_op jit(solution)/shard_map/all_to_all | solution.py:674
  231.6 2.4 %combine.1 = bf16[128,2048]{1,0:T(8,128)(2,1)} custom-call(bf16[256,512]{1,0:T(8,128)(2,1)} %get-tuple-element.44.mix_ref, bf16[512,2048]{1,0:T(8,128)(2,1)S(1)} %bitcast.16), custom_call_target="tpu_custom_call" | custom-call | flops 1000000000 | bytes 3145728 | tf_op jit(solution)/shard_map/combine/pallas_call | solution.py:649
  (47 shorter events, 25.3 us)
Async XLA Ops:
  20.2 7.4 %collective-permute-start = (bf16[80,128]{1,0:T(8,128)(2,1)}, bf16[80,128]{1,0:T(8,128)(2,1)S(1)}, u32[]{:S(2)}, u32[]{:S(2)}) collective-permute-start(bf16[80,128]{1,0:T(8,128)(2,1)} %get-tuple-element.26), channel_id=1, source_target_pairs={{0,4},{4,8},{8,12},{12,16},{16,20},{20,24},{24,28},{28,0},{1,5},{5... | collective-permute-start | bytes 61448 | tf_op jit(solution)/shard_map/ppermute | solution.py:662
  20.2 7.8 %collective-permute-start.1 = (bf16[80,128]{1,0:T(8,128)(2,1)}, bf16[80,128]{1,0:T(8,128)(2,1)S(1)}, u32[]{:S(2)}, u32[]{:S(2)}) collective-permute-start(bf16[80,128]{1,0:T(8,128)(2,1)} %get-tuple-element.27), channel_id=1, source_target_pairs={{0,8},{4,12},{8,16},{12,20},{16,24},{20,28},{24,0},{28,4},{1,9},{5... | collective-permute-start | bytes 61448 | tf_op jit(solution)/shard_map/ppermute | solution.py:662
  21.7 7.2 %collective-permute-start.2 = (bf16[80,128]{1,0:T(8,128)(2,1)}, bf16[80,128]{1,0:T(8,128)(2,1)S(1)}, u32[]{:S(2)}, u32[]{:S(2)}) collective-permute-start(bf16[80,128]{1,0:T(8,128)(2,1)} %get-tuple-element.28), channel_id=1, source_target_pairs={{0,12},{4,16},{8,20},{12,24},{16,28},{20,0},{24,4},{28,8},{1,13},{... | collective-permute-start | bytes 61448 | tf_op jit(solution)/shard_map/ppermute | solution.py:662
  24.5 5.6 %collective-permute-start.3 = (bf16[80,128]{1,0:T(8,128)(2,1)}, bf16[80,128]{1,0:T(8,128)(2,1)S(1)}, u32[]{:S(2)}, u32[]{:S(2)}) collective-permute-start(bf16[80,128]{1,0:T(8,128)(2,1)} %get-tuple-element.29), channel_id=1, source_target_pairs={{0,16},{4,20},{8,24},{12,28},{16,0},{20,4},{24,8},{28,12},{1,17},{... | collective-permute-start | bytes 61448 | tf_op jit(solution)/shard_map/ppermute | solution.py:662
  25.2 4.9 %collective-permute-start.4 = (bf16[80,128]{1,0:T(8,128)(2,1)}, bf16[80,128]{1,0:T(8,128)(2,1)S(1)}, u32[]{:S(2)}, u32[]{:S(2)}) collective-permute-start(bf16[80,128]{1,0:T(8,128)(2,1)} %get-tuple-element.30), channel_id=1, source_target_pairs={{0,20},{4,24},{8,28},{12,0},{16,4},{20,8},{24,12},{28,16},{1,21},{... | collective-permute-start | bytes 61448 | tf_op jit(solution)/shard_map/ppermute | solution.py:662
  34.0 17.6 %all-to-all-start = ((bf16[8,80,128]{2,1,0:T(8,128)(2,1)}), bf16[8,80,128]{2,1,0:T(8,128)(2,1)S(1)}, u32[]{:S(2)}, u32[]{:S(2)}) async-start(bf16[8,80,128]{2,1,0:T(8,128)(2,1)} %get-tuple-element.33), calls=%async_computation | async-start | bytes 327680 | tf_op jit(solution)/shard_map/all_to_all | solution.py:674
  51.6 95.2 %all-to-all-start.2 = ((bf16[64,8,2048]{2,1,0:T(8,128)(2,1)}), bf16[64,8,2048]{2,1,0:T(8,128)(2,1)S(1)}, u32[]{:S(2)}, u32[]{:S(2)}) async-start(bf16[64,8,2048]{2,1,0:T(8,128)(2,1)} %bitcast.19), calls=%async_computation.2 | async-start | bytes 4194304 | tf_op jit(solution)/shard_map/all_to_all | solution.py:674
  57.6 27.6 %collective-permute-start.10 = (bf16[2048,256]{1,0:T(8,128)(2,1)}, bf16[2048,256]{1,0:T(8,128)(2,1)}, u32[]{:S(2)}, u32[]{:S(2)}) collective-permute-start(bf16[2048,256]{1,0:T(8,128)(2,1)} %bitcast.11.refs_0_), channel_id=1, source_target_pairs={{0,1},{1,2},{2,3},{3,0},{4,5},{5,6},{6,7},{7,4},{8,9},{9,10},{10,1... | collective-permute-start | bytes 3145736 | tf_op jit(solution)/shard_map/ppermute | solution.py:662
  59.2 26.3 %collective-permute-start.13 = (bf16[2048,256]{1,0:T(8,128)(2,1)}, bf16[2048,256]{1,0:T(8,128)(2,1)}, u32[]{:S(2)}, u32[]{:S(2)}) collective-permute-start(bf16[2048,256]{1,0:T(8,128)(2,1)} %bitcast.12.refs_1_), channel_id=1, source_target_pairs={{0,3},{1,0},{2,1},{3,2},{4,7},{5,4},{6,5},{7,6},{8,11},{9,8},{10,9... | collective-permute-start | bytes 3145736 | tf_op jit(solution)/shard_map/ppermute | solution.py:662
  62.0 34.4 %collective-permute-start.16 = (bf16[256,1024]{1,0:T(8,128)(2,1)}, bf16[256,1024]{1,0:T(8,128)(2,1)}, u32[]{:S(2)}, u32[]{:S(2)}) collective-permute-start(bf16[256,1024]{1,0:T(8,128)(2,1)} %get-tuple-element.49), channel_id=1, source_target_pairs={{0,1},{1,2},{2,3},{3,0},{4,5},{5,6},{6,7},{7,4},{8,9},{9,10},{10,1... | collective-permute-start | bytes 1572872 | tf_op jit(solution)/shard_map/ppermute | solution.py:662
  62.4 79.8 %collective-permute-start.11 = (bf16[2048,256]{1,0:T(8,128)(2,1)}, bf16[2048,256]{1,0:T(8,128)(2,1)S(1)}, u32[]{:S(2)}, u32[]{:S(2)}) collective-permute-start(bf16[2048,256]{1,0:T(8,128)(2,1)} %bitcast.12.refs_1_), channel_id=1, source_target_pairs={{0,1},{1,2},{2,3},{3,0},{4,5},{5,6},{6,7},{7,4},{8,9},{9,10},{10,1... | collective-permute-start | bytes 3145736 | tf_op jit(solution)/shard_map/ppermute | solution.py:662
  64.0 87.6 %collective-permute-start.12 = (bf16[2048,256]{1,0:T(8,128)(2,1)}, bf16[2048,256]{1,0:T(8,128)(2,1)}, u32[]{:S(2)}, u32[]{:S(2)}) collective-permute-start(bf16[2048,256]{1,0:T(8,128)(2,1)} %bitcast.11.refs_0_), channel_id=1, source_target_pairs={{0,3},{1,0},{2,1},{3,2},{4,7},{5,4},{6,5},{7,6},{8,11},{9,8},{10,9... | collective-permute-start | bytes 3145736 | tf_op jit(solution)/shard_map/ppermute | solution.py:662
  85.2 66.8 %collective-permute-start.14 = (bf16[2048,256]{1,0:T(8,128)(2,1)}, bf16[2048,256]{1,0:T(8,128)(2,1)}, u32[]{:S(2)}, u32[]{:S(2)}) collective-permute-start(bf16[2048,256]{1,0:T(8,128)(2,1)} %collective-permute-done.10.refs_2_), channel_id=1, source_target_pairs={{0,1},{1,2},{2,3},{3,0},{4,5},{5,6},{6,7},{7,4},{8,9},{9,10},{10,1... | collective-permute-start | bytes 3145736 | tf_op jit(solution)/shard_map/ppermute | solution.py:662
  85.6 69.3 %collective-permute-start.15 = (bf16[2048,256]{1,0:T(8,128)(2,1)}, bf16[2048,256]{1,0:T(8,128)(2,1)}, u32[]{:S(2)}, u32[]{:S(2)}) collective-permute-start(bf16[2048,256]{1,0:T(8,128)(2,1)} %collective-permute-done.13.refs_5_), channel_id=1, source_target_pairs={{0,3},{1,0},{2,1},{3,2},{4,7},{5,4},{6,5},{7,6},{8,11},{9,8},{10,9... | collective-permute-start | bytes 3145736 | tf_op jit(solution)/shard_map/ppermute | solution.py:662
  96.5 44.2 %collective-permute-start.19 = (bf16[256,1024]{1,0:T(8,128)(2,1)}, bf16[256,1024]{1,0:T(8,128)(2,1)}, u32[]{:S(2)}, u32[]{:S(2)}) collective-permute-start(bf16[256,1024]{1,0:T(8,128)(2,1)} %get-tuple-element.48), channel_id=1, source_target_pairs={{0,3},{1,0},{2,1},{3,2},{4,7},{5,4},{6,5},{7,6},{8,11},{9,8},{10,9... | collective-permute-start | bytes 1572872 | tf_op jit(solution)/shard_map/ppermute | solution.py:662
  140.6 22.6 %collective-permute-start.17 = (bf16[256,1024]{1,0:T(8,128)(2,1)}, bf16[256,1024]{1,0:T(8,128)(2,1)}, u32[]{:S(2)}, u32[]{:S(2)}) collective-permute-start(bf16[256,1024]{1,0:T(8,128)(2,1)} %get-tuple-element.48), channel_id=1, source_target_pairs={{0,1},{1,2},{2,3},{3,0},{4,5},{5,6},{6,7},{7,4},{8,9},{9,10},{10,1... | collective-permute-start | bytes 1572872 | tf_op jit(solution)/shard_map/ppermute | solution.py:662
  142.2 21.0 %collective-permute-start.18 = (bf16[256,1024]{1,0:T(8,128)(2,1)}, bf16[256,1024]{1,0:T(8,128)(2,1)}, u32[]{:S(2)}, u32[]{:S(2)}) collective-permute-start(bf16[256,1024]{1,0:T(8,128)(2,1)} %get-tuple-element.49), channel_id=1, source_target_pairs={{0,3},{1,0},{2,1},{3,2},{4,7},{5,4},{6,5},{7,6},{8,11},{9,8},{10,9... | collective-permute-start | bytes 1572872 | tf_op jit(solution)/shard_map/ppermute | solution.py:662
  146.8 23.0 %all-to-all-start.1 = ((bf16[8,64,128]{2,1,0:T(8,128)(2,1)}), bf16[8,64,128]{2,1,0:T(8,128)(2,1)S(1)}, u32[]{:S(2)}, u32[]{:S(2)}) async-start(bf16[8,64,128]{2,1,0:T(8,128)(2,1)} %enter_states.1), calls=%async_computation.1 | async-start | bytes 262144 | tf_op jit(solution)/shard_map/all_to_all | solution.py:674
  151.6 16.4 %collective-permute-start.20 = (bf16[256,1024]{1,0:T(8,128)(2,1)}, bf16[256,1024]{1,0:T(8,128)(2,1)S(1)}, u32[]{:S(2)}, u32[]{:S(2)}) collective-permute-start(bf16[256,1024]{1,0:T(8,128)(2,1)} %collective-permute-done.16.before_0), channel_id=1, source_target_pairs={{0,1},{1,2},{2,3},{3,0},{4,5},{5,6},{6,7},{7,4},{8,9},{9,10},{10,1... | collective-permute-start | bytes 1572872 | tf_op jit(solution)/shard_map/ppermute | solution.py:662
  152.0 16.0 %collective-permute-start.21 = (bf16[256,1024]{1,0:T(8,128)(2,1)}, bf16[256,1024]{1,0:T(8,128)(2,1)S(1)}, u32[]{:S(2)}, u32[]{:S(2)}) collective-permute-start(bf16[256,1024]{1,0:T(8,128)(2,1)} %collective-permute-done.19.after_1), channel_id=1, source_target_pairs={{0,3},{1,0},{2,1},{3,2},{4,7},{5,4},{6,5},{7,6},{8,11},{9,8},{10,9... | collective-permute-start | bytes 1572872 | tf_op jit(solution)/shard_map/ppermute | solution.py:662
  169.8 61.8 %all-to-all-start.3 = ((bf16[64,8,2048]{2,1,0:T(8,128)(2,1)}), bf16[64,8,2048]{2,1,0:T(8,128)(2,1)S(1)}, u32[]{:S(2)}, u32[]{:S(2)}) async-start(bf16[64,8,2048]{2,1,0:T(8,128)(2,1)} %bitcast.17), calls=%async_computation.3 | async-start | bytes 4194304 | tf_op jit(solution)/shard_map/all_to_all | solution.py:674
  189.2 25.0 %collective-permute-start.9 = (bf16[128,2048]{1,0:T(8,128)(2,1)}, bf16[128,2048]{1,0:T(8,128)(2,1)S(1)}, u32[]{:S(2)}, u32[]{:S(2)}) collective-permute-start(bf16[128,2048]{1,0:T(8,128)(2,1)} %get-tuple-element.43), channel_id=1, source_target_pairs={{0,3},{1,0},{2,1},{3,2},{4,7},{5,4},{6,5},{7,6},{8,11},{9,8},{10,9... | collective-permute-start | bytes 1572872 | tf_op jit(solution)/shard_map/ppermute | solution.py:662
  191.2 23.1 %collective-permute-start.8 = (bf16[128,2048]{1,0:T(8,128)(2,1)}, bf16[128,2048]{1,0:T(8,128)(2,1)S(1)}, u32[]{:S(2)}, u32[]{:S(2)}) collective-permute-start(bf16[128,2048]{1,0:T(8,128)(2,1)} %get-tuple-element.42), channel_id=1, source_target_pairs={{0,2},{1,3},{2,0},{3,1},{4,6},{5,7},{6,4},{7,5},{8,10},{9,11},{10,... | collective-permute-start | bytes 1572872 | tf_op jit(solution)/shard_map/ppermute | solution.py:662
  191.2 26.3 %collective-permute-start.7 = (bf16[128,2048]{1,0:T(8,128)(2,1)}, bf16[128,2048]{1,0:T(8,128)(2,1)S(1)}, u32[]{:S(2)}, u32[]{:S(2)}) collective-permute-start(bf16[128,2048]{1,0:T(8,128)(2,1)} %get-tuple-element.41), channel_id=1, source_target_pairs={{0,1},{1,2},{2,3},{3,0},{4,5},{5,6},{6,7},{7,4},{8,9},{9,10},{10,1... | collective-permute-start | bytes 1572872 | tf_op jit(solution)/shard_map/ppermute | solution.py:662
  (6 other events, 26.9 us)

commit v6 on v5

--- a/solution.py
+++ b/solution.py
@@ -445,20 +445,17 @@
         table = table + here.astype(F32)
         mix = jnp.where(here, weight, mix)
     out_ref[...] = dot(table.astype(BF16), normed).astype(BF16)
-    high, rest = two_parts(jnp.transpose(mix))
-    mix_out_ref[:tokens, :] = high
-    mix_out_ref[tokens:, :] = rest
+    mix_out_ref[...] = jnp.transpose(mix).astype(BF16)
 
 
 def combine_kernel(mix_ref, rows_ref, out_hbm, made_ref, sems):
-    tokens, width = made_ref.shape
+    width = made_ref.shape[1]
     parts = 4
     tile = width // parts
     stores = []
     for part in range(parts):
         lanes = slice(part * tile, (part + 1) * tile)
-        both = dot(mix_ref[...], rows_ref[:, lanes])
-        made_ref[:, lanes] = (both[:tokens] + both[tokens:]).astype(BF16)
+        made_ref[:, lanes] = dot(mix_ref[...], rows_ref[:, lanes]).astype(BF16)
         store = pltpu.make_async_copy(made_ref.at[:, lanes], out_hbm.at[:, lanes], sems.at[part])
         store.start()
         stores.append(store)
@@ -636,7 +633,7 @@
         pack_kernel,
         out_shape=[
             jax.ShapeDtypeStruct((places, width), BF16),
-            jax.ShapeDtypeStruct((2 * tokens, places), BF16),
+            jax.ShapeDtypeStruct((tokens, places), BF16),
         ],
         cost_estimate=estimate(2.0e9, 3 << 20),
         name="pack",
@@ -644,7 +641,7 @@
 
 
 def combine_rows(mix, rows):
-    tokens = mix.shape[0] // 2
+    tokens = mix.shape[0]
     width = rows.shape[1]
     return pl.pallas_call(
         combine_kernel,

time: 235 us -> 235 us (level)
  no operation moved by 1% of the time
where the time goes in v6:
time: 235 us; the launch traced here: 234 us
  waiting for transfers between devices  117 us (50%)
  starting transfers between devices  58.3 us (25%)
  Pallas kernels  53.2 us (23%)
    ppermute x22, waiting for transfers between devices, ring(): lax.ppermute(x, axis, [(i, (i + shift) % count) for i in range(count)])  98 us
    ppermute x22, starting transfers between devices, ring(): lax.ppermute(x, axis, [(i, (i + shift) % count) for i in range(count)])  30.2 us
    all_to_all x4, starting transfers between devices, exchange(): return lax.all_to_all(x, axis, 0, 0, tiled=True)  28.1 us
    pallas_call x1, Pallas kernels, summarize(): pl.pallas_call(summary_kernel, grid=(spans,), in_specs=[SCALARS] + [block...  19.5 us
    all_to_all x4, waiting for transfers between devices, exchange(): return lax.all_to_all(x, axis, 0, 0, tiled=True)  19.3 us
    pallas_call x1, Pallas kernels, read_and_project(): pl.pallas_call(readout_kernel, grid=(spans,), in_specs=[SCALARS, IN_VMEM,...  8.89 us
    pallas_call x1, Pallas kernels, expert_hidden(): pl.pallas_call(hidden_kernel, in_specs=[IN_HBM] * (1 + count), out_specs=...  8.3 us
    pallas_call x1, Pallas kernels, expert_down_early(): pl.pallas_call(down_early_kernel, in_specs=[IN_VMEM] + [IN_HBM] * 5, out_...  4.75 us
  transfers between devices with their start and end apart: 26, of which 9 were waited for; matrix products, arithmetic and copies ran while one was open for 1% of the time, Pallas kernels for 13%

profile of v6, /device:TPU:2, one launch (start us, length us, event | category | flops | bytes accessed | tf_op | source)
XLA Modules:
  0.0 233.8 jit_solution(4234198757293404560)
XLA Ops:
  0.6 19.5 %summary.1 = (bf16[512,512]{1,0:T(8,128)(2,1)}, f32[512,512]{1,0:T(8,128)}, bf16[4,4,128,128]{3,2,1,0:T(8,128)(2,1)}, f32[4,4,128,128]{3,2,1,0:T(8,128)}, f32[4,...) custom-call(s32[1]{0:T(128)} %bitcast.2.here_ref, ...), custom_call_target="tpu_custom_call" | custom-call | flops 20000000000 | bytes 6291456 | tf_op jit(solution)/shard_map/summary/pallas_call | solution.py:486
  21.7 2.7 %collective-permute-start.2 = (bf16[80,128]{1,0:T(8,128)(2,1)}, bf16[80,128]{1,0:T(8,128)(2,1)S(1)}, u32[]{:S(2)}, u32[]{:S(2)}) collective-permute-start(bf16[80,128]{1,0:T(8,128)(2,1)} %get-tuple-element.28), channel_id=1, source_target_pairs={{0,12},{4,16},{8,20},{12,24},{16,28},{20,0},{24,4},{28,8},{1,13},{... | collective-permute-start | bytes 61448 | tf_op jit(solution)/shard_map/ppermute | solution.py:659
  25.2 2.4 %collective-permute-start.4 = (bf16[80,128]{1,0:T(8,128)(2,1)}, bf16[80,128]{1,0:T(8,128)(2,1)S(1)}, u32[]{:S(2)}, u32[]{:S(2)}) collective-permute-start(bf16[80,128]{1,0:T(8,128)(2,1)} %get-tuple-element.30), channel_id=1, source_target_pairs={{0,20},{4,24},{8,28},{12,0},{16,4},{20,8},{24,12},{28,16},{1,21},{... | collective-permute-start | bytes 61448 | tf_op jit(solution)/shard_map/ppermute | solution.py:659
  34.0 6.8 %all-to-all-start = ((bf16[8,80,128]{2,1,0:T(8,128)(2,1)}), bf16[8,80,128]{2,1,0:T(8,128)(2,1)S(1)}, u32[]{:S(2)}, u32[]{:S(2)}) async-start(bf16[8,80,128]{2,1,0:T(8,128)(2,1)} %get-tuple-element.33), calls=%async_computation | async-start | bytes 327680 | tf_op jit(solution)/shard_map/all_to_all | solution.py:671
  40.8 3.3 %pack.1 = (bf16[512,2048]{1,0:T(8,128)(2,1)}, bf16[128,512]{1,0:T(8,128)(2,1)}) custom-call(bf16[128,2048]{1,0:T(8,128)(2,1)} %x_ref.1, f32[1,2048]{1,0:T(1,128)} %bitcast.23, s32[2,128]{1,0:T(2,128)} %bitcast.26, f32[2,128]{1,0:T(2,128)} %bitcast.27), custom_call_target="tpu_custom_call" | custom-call | flops 2000000000 | bytes 3145728 | tf_op jit(solution)/shard_map/pack/pallas_call | solution.py:632
  44.2 7.4 %all-to-all-done.in_ref = bf16[8,80,128]{2,1,0:T(8,128)(2,1)S(1)} async-done(((bf16[8,80,128]{2,1,0:T(8,128)(2,1)}), bf16[8,80,128]{2,1,0:T(8,128)(2,1)S(1)}, u32[]{:S(2)}, u32[]{:S(2)}) %all-to-all-start) | async-done | bytes 163872 | tf_op jit(solution)/shard_map/all_to_all | solution.py:671
  51.6 6.0 %all-to-all-start.2 = ((bf16[64,8,2048]{2,1,0:T(8,128)(2,1)}), bf16[64,8,2048]{2,1,0:T(8,128)(2,1)S(1)}, u32[]{:S(2)}, u32[]{:S(2)}) async-start(bf16[64,8,2048]{2,1,0:T(8,128)(2,1)} %bitcast.19), calls=%async_computation.2 | async-start | bytes 4194304 | tf_op jit(solution)/shard_map/all_to_all | solution.py:671
  65.6 19.6 %collective-permute-done.10.refs_2_ = bf16[2048,256]{1,0:T(8,128)(2,1)} collective-permute-done((bf16[2048,256]{1,0:T(8,128)(2,1)}, bf16[2048,256]{1,0:T(8,128)(2,1)}, u32[]{:S(2)}, u32[]{:S(2)}) %collective-permute-start.10) | collective-permute-done | bytes 1048608 | tf_op jit(solution)/shard_map/ppermute | solution.py:659
  85.6 2.9 %collective-permute-start.15 = (bf16[2048,256]{1,0:T(8,128)(2,1)}, bf16[2048,256]{1,0:T(8,128)(2,1)}, u32[]{:S(2)}, u32[]{:S(2)}) collective-permute-start(bf16[2048,256]{1,0:T(8,128)(2,1)} %collective-permute-done.13.refs_5_), channel_id=1, source_target_pairs={{0,3},{1,0},{2,1},{3,2},{4,7},{5,4},{6,5},{7,6},{8,11},{9,8},{10,9... | collective-permute-start | bytes 3145736 | tf_op jit(solution)/shard_map/ppermute | solution.py:659
  88.5 8.0 %collective-permute-done.16.before_0 = bf16[256,1024]{1,0:T(8,128)(2,1)} collective-permute-done((bf16[256,1024]{1,0:T(8,128)(2,1)}, bf16[256,1024]{1,0:T(8,128)(2,1)}, u32[]{:S(2)}, u32[]{:S(2)}) %collective-permute-start.16) | collective-permute-done | bytes 524320 | tf_op jit(solution)/shard_map/ppermute | solution.py:659
  98.3 42.4 %collective-permute-done.19.after_1 = bf16[256,1024]{1,0:T(8,128)(2,1)} collective-permute-done((bf16[256,1024]{1,0:T(8,128)(2,1)}, bf16[256,1024]{1,0:T(8,128)(2,1)}, u32[]{:S(2)}, u32[]{:S(2)}) %collective-permute-start.19) | collective-permute-done | bytes 524320 | tf_op jit(solution)/shard_map/ppermute | solution.py:659
  143.9 2.9 %enter_states.1 = bf16[8,64,128]{2,1,0:T(8,128)(2,1)} custom-call(s32[1]{0:T(128)} %bitcast.1.here_ref, bf16[8,80,128]{2,1,0:T(8,128)(2,1)S(1)} %all-to-all-done.in_ref, f32[8,128,64]{2,1,0:T(8,128)} %get-tuple-element.34.prefix_ref), custom_call_target="tpu_custom_call" | custom-call | flops 2000000000 | bytes 1048576 | tf_op jit(solution)/shard_map/enter_states/pallas_call | solution.py:534
  146.8 4.8 %all-to-all-start.1 = ((bf16[8,64,128]{2,1,0:T(8,128)(2,1)}), bf16[8,64,128]{2,1,0:T(8,128)(2,1)S(1)}, u32[]{:S(2)}, u32[]{:S(2)}) async-start(bf16[8,64,128]{2,1,0:T(8,128)(2,1)} %enter_states.1), calls=%async_computation.1 | async-start | bytes 262144 | tf_op jit(solution)/shard_map/all_to_all | solution.py:671
  152.0 2.9 %collective-permute-start.21 = (bf16[256,1024]{1,0:T(8,128)(2,1)}, bf16[256,1024]{1,0:T(8,128)(2,1)S(1)}, u32[]{:S(2)}, u32[]{:S(2)}) collective-permute-start(bf16[256,1024]{1,0:T(8,128)(2,1)} %collective-permute-done.19.after_1), channel_id=1, source_target_pairs={{0,3},{1,0},{2,1},{3,2},{4,7},{5,4},{6,5},{7,6},{8,11},{9,8},{10,9... | collective-permute-start | bytes 1572872 | tf_op jit(solution)/shard_map/ppermute | solution.py:659
  154.9 8.3 %hidden.1.hidden_ref = bf16[512,1024]{1,0:T(8,128)(2,1)} custom-call(bf16[512,2048]{1,0:T(8,128)(2,1)} %bitcast.18, bf16[2048,256]{1,0:T(8,128)(2,1)} %bitcast.11.refs_0_, bf16[2048,256]{1,0:T(8,128)(2,1)} %bitcast.12.refs_1_, bf16[2048,256]{1,0:T(8,128)(2,1)} %collective-permute-done.10.refs_2_, bf16[2048,256]{1,0:T(8,128)(2,1)} %copy-done.3, ...), custom_call_target="tpu_custom_call" | custom-call | flops 4294967296 | bytes 11534336 | tf_op jit(solution)/shard_map/hidden/pallas_call | solution.py:581
  163.2 4.8 %down_early.1 = (bf16[512,2048]{1,0:T(8,128)(2,1)S(1)}, bf16[512,256]{1,0:T(8,128)(2,1)S(1)}) custom-call(bf16[512,1024]{1,0:T(8,128)(2,1)} %hidden.1.hidden_ref, bf16[256,2048]{1,0:T(8,128)(2,1)} %bitcast.20, bf16[256,1024]{1,0:T(8,128)(2,1)} %collective-permute-done.16.before_0, bf16[256,1024]{1,0:T(8,128)(2,1)} %collective-permute-done.17.before_1, ...), custom_call_target="tpu_custom_call" | custom-call | flops 1610612736 | bytes 6291456 | tf_op jit(solution)/shard_map/down_early/pallas_call | solution.py:599
  169.8 10.5 %all-to-all-start.3 = ((bf16[64,8,2048]{2,1,0:T(8,128)(2,1)}), bf16[64,8,2048]{2,1,0:T(8,128)(2,1)S(1)}, u32[]{:S(2)}, u32[]{:S(2)}) async-start(bf16[64,8,2048]{2,1,0:T(8,128)(2,1)} %bitcast.17), calls=%async_computation.3 | async-start | bytes 4194304 | tf_op jit(solution)/shard_map/all_to_all | solution.py:671
  180.3 8.9 %readout.1 = (bf16[128,2048]{1,0:T(8,128)(2,1)}, bf16[128,2048]{1,0:T(8,128)(2,1)}, bf16[128,2048]{1,0:T(8,128)(2,1)}, bf16[128,2048]{1,0:T(8,128)(2,1)}) custom-call(s32[1]{0:T(128)} %bitcast.here_ref, bf16[8,64,128]{2,1,0:T(8,128)(2,1)S(1)} %all-to-all-done.1.enter_ref, bf16[512,512]{1,0:T(8,128)(2,1)} %get-tuple-element.35.reader_ref, ...), custom_call_target="tpu_custom_call" | custom-call | flops 5000000000 | bytes 8388608 | tf_op jit(solution)/shard_map/readout/pallas_call | solution.py:550
  189.2 2.0 collective-permute-start.9
  192.1 22.1 %collective-permute-done.9 = bf16[128,2048]{1,0:T(8,128)(2,1)S(1)} collective-permute-done((bf16[128,2048]{1,0:T(8,128)(2,1)}, bf16[128,2048]{1,0:T(8,128)(2,1)S(1)}, u32[]{:S(2)}, u32[]{:S(2)}) %collective-permute-start.9) | collective-permute-done | bytes 524320 | tf_op jit(solution)/shard_map/ppermute | solution.py:659
  214.2 3.3 %collective-permute-done.7 = bf16[128,2048]{1,0:T(8,128)(2,1)S(1)} collective-permute-done((bf16[128,2048]{1,0:T(8,128)(2,1)}, bf16[128,2048]{1,0:T(8,128)(2,1)S(1)}, u32[]{:S(2)}, u32[]{:S(2)}) %collective-permute-start.7) | collective-permute-done | bytes 524320 | tf_op jit(solution)/shard_map/ppermute | solution.py:659
  217.5 2.2 add_convert_fusion
  219.7 11.9 %all-to-all-done.3 = bf16[64,8,2048]{2,1,0:T(8,128)(2,1)S(1)} async-done(((bf16[64,8,2048]{2,1,0:T(8,128)(2,1)}), bf16[64,8,2048]{2,1,0:T(8,128)(2,1)S(1)}, u32[]{:S(2)}, u32[]{:S(2)}) %all-to-all-start.3) | async-done | bytes 2097184 | tf_op jit(solution)/shard_map/all_to_all | solution.py:671
  231.6 2.0 combine.1
  (47 shorter events, 25.3 us)
Async XLA Ops:
  20.2 7.4 %collective-permute-start = (bf16[80,128]{1,0:T(8,128)(2,1)}, bf16[80,128]{1,0:T(8,128)(2,1)S(1)}, u32[]{:S(2)}, u32[]{:S(2)}) collective-permute-start(bf16[80,128]{1,0:T(8,128)(2,1)} %get-tuple-element.26), channel_id=1, source_target_pairs={{0,4},{4,8},{8,12},{12,16},{16,20},{20,24},{24,28},{28,0},{1,5},{5... | collective-permute-start | bytes 61448 | tf_op jit(solution)/shard_map/ppermute | solution.py:659
  20.2 7.8 %collective-permute-start.1 = (bf16[80,128]{1,0:T(8,128)(2,1)}, bf16[80,128]{1,0:T(8,128)(2,1)S(1)}, u32[]{:S(2)}, u32[]{:S(2)}) collective-permute-start(bf16[80,128]{1,0:T(8,128)(2,1)} %get-tuple-element.27), channel_id=1, source_target_pairs={{0,8},{4,12},{8,16},{12,20},{16,24},{20,28},{24,0},{28,4},{1,9},{5... | collective-permute-start | bytes 61448 | tf_op jit(solution)/shard_map/ppermute | solution.py:659
  21.7 7.2 %collective-permute-start.2 = (bf16[80,128]{1,0:T(8,128)(2,1)}, bf16[80,128]{1,0:T(8,128)(2,1)S(1)}, u32[]{:S(2)}, u32[]{:S(2)}) collective-permute-start(bf16[80,128]{1,0:T(8,128)(2,1)} %get-tuple-element.28), channel_id=1, source_target_pairs={{0,12},{4,16},{8,20},{12,24},{16,28},{20,0},{24,4},{28,8},{1,13},{... | collective-permute-start | bytes 61448 | tf_op jit(solution)/shard_map/ppermute | solution.py:659
  24.5 5.6 %collective-permute-start.3 = (bf16[80,128]{1,0:T(8,128)(2,1)}, bf16[80,128]{1,0:T(8,128)(2,1)S(1)}, u32[]{:S(2)}, u32[]{:S(2)}) collective-permute-start(bf16[80,128]{1,0:T(8,128)(2,1)} %get-tuple-element.29), channel_id=1, source_target_pairs={{0,16},{4,20},{8,24},{12,28},{16,0},{20,4},{24,8},{28,12},{1,17},{... | collective-permute-start | bytes 61448 | tf_op jit(solution)/shard_map/ppermute | solution.py:659
  25.2 4.9 %collective-permute-start.4 = (bf16[80,128]{1,0:T(8,128)(2,1)}, bf16[80,128]{1,0:T(8,128)(2,1)S(1)}, u32[]{:S(2)}, u32[]{:S(2)}) collective-permute-start(bf16[80,128]{1,0:T(8,128)(2,1)} %get-tuple-element.30), channel_id=1, source_target_pairs={{0,20},{4,24},{8,28},{12,0},{16,4},{20,8},{24,12},{28,16},{1,21},{... | collective-permute-start | bytes 61448 | tf_op jit(solution)/shard_map/ppermute | solution.py:659
  34.0 17.6 %all-to-all-start = ((bf16[8,80,128]{2,1,0:T(8,128)(2,1)}), bf16[8,80,128]{2,1,0:T(8,128)(2,1)S(1)}, u32[]{:S(2)}, u32[]{:S(2)}) async-start(bf16[8,80,128]{2,1,0:T(8,128)(2,1)} %get-tuple-element.33), calls=%async_computation | async-start | bytes 327680 | tf_op jit(solution)/shard_map/all_to_all | solution.py:671
  51.6 95.2 %all-to-all-start.2 = ((bf16[64,8,2048]{2,1,0:T(8,128)(2,1)}), bf16[64,8,2048]{2,1,0:T(8,128)(2,1)S(1)}, u32[]{:S(2)}, u32[]{:S(2)}) async-start(bf16[64,8,2048]{2,1,0:T(8,128)(2,1)} %bitcast.19), calls=%async_computation.2 | async-start | bytes 4194304 | tf_op jit(solution)/shard_map/all_to_all | solution.py:671
  57.6 27.6 %collective-permute-start.10 = (bf16[2048,256]{1,0:T(8,128)(2,1)}, bf16[2048,256]{1,0:T(8,128)(2,1)}, u32[]{:S(2)}, u32[]{:S(2)}) collective-permute-start(bf16[2048,256]{1,0:T(8,128)(2,1)} %bitcast.11.refs_0_), channel_id=1, source_target_pairs={{0,1},{1,2},{2,3},{3,0},{4,5},{5,6},{6,7},{7,4},{8,9},{9,10},{10,1... | collective-permute-start | bytes 3145736 | tf_op jit(solution)/shard_map/ppermute | solution.py:659
  59.3 26.3 %collective-permute-start.13 = (bf16[2048,256]{1,0:T(8,128)(2,1)}, bf16[2048,256]{1,0:T(8,128)(2,1)}, u32[]{:S(2)}, u32[]{:S(2)}) collective-permute-start(bf16[2048,256]{1,0:T(8,128)(2,1)} %bitcast.12.refs_1_), channel_id=1, source_target_pairs={{0,3},{1,0},{2,1},{3,2},{4,7},{5,4},{6,5},{7,6},{8,11},{9,8},{10,9... | collective-permute-start | bytes 3145736 | tf_op jit(solution)/shard_map/ppermute | solution.py:659
  62.0 34.4 %collective-permute-start.16 = (bf16[256,1024]{1,0:T(8,128)(2,1)}, bf16[256,1024]{1,0:T(8,128)(2,1)}, u32[]{:S(2)}, u32[]{:S(2)}) collective-permute-start(bf16[256,1024]{1,0:T(8,128)(2,1)} %get-tuple-element.49), channel_id=1, source_target_pairs={{0,1},{1,2},{2,3},{3,0},{4,5},{5,6},{6,7},{7,4},{8,9},{9,10},{10,1... | collective-permute-start | bytes 1572872 | tf_op jit(solution)/shard_map/ppermute | solution.py:659
  62.4 79.8 %collective-permute-start.11 = (bf16[2048,256]{1,0:T(8,128)(2,1)}, bf16[2048,256]{1,0:T(8,128)(2,1)S(1)}, u32[]{:S(2)}, u32[]{:S(2)}) collective-permute-start(bf16[2048,256]{1,0:T(8,128)(2,1)} %bitcast.12.refs_1_), channel_id=1, source_target_pairs={{0,1},{1,2},{2,3},{3,0},{4,5},{5,6},{6,7},{7,4},{8,9},{9,10},{10,1... | collective-permute-start | bytes 3145736 | tf_op jit(solution)/shard_map/ppermute | solution.py:659
  64.0 87.6 %collective-permute-start.12 = (bf16[2048,256]{1,0:T(8,128)(2,1)}, bf16[2048,256]{1,0:T(8,128)(2,1)}, u32[]{:S(2)}, u32[]{:S(2)}) collective-permute-start(bf16[2048,256]{1,0:T(8,128)(2,1)} %bitcast.11.refs_0_), channel_id=1, source_target_pairs={{0,3},{1,0},{2,1},{3,2},{4,7},{5,4},{6,5},{7,6},{8,11},{9,8},{10,9... | collective-permute-start | bytes 3145736 | tf_op jit(solution)/shard_map/ppermute | solution.py:659
  85.2 66.8 %collective-permute-start.14 = (bf16[2048,256]{1,0:T(8,128)(2,1)}, bf16[2048,256]{1,0:T(8,128)(2,1)}, u32[]{:S(2)}, u32[]{:S(2)}) collective-permute-start(bf16[2048,256]{1,0:T(8,128)(2,1)} %collective-permute-done.10.refs_2_), channel_id=1, source_target_pairs={{0,1},{1,2},{2,3},{3,0},{4,5},{5,6},{6,7},{7,4},{8,9},{9,10},{10,1... | collective-permute-start | bytes 3145736 | tf_op jit(solution)/shard_map/ppermute | solution.py:659
  85.6 69.3 %collective-permute-start.15 = (bf16[2048,256]{1,0:T(8,128)(2,1)}, bf16[2048,256]{1,0:T(8,128)(2,1)}, u32[]{:S(2)}, u32[]{:S(2)}) collective-permute-start(bf16[2048,256]{1,0:T(8,128)(2,1)} %collective-permute-done.13.refs_5_), channel_id=1, source_target_pairs={{0,3},{1,0},{2,1},{3,2},{4,7},{5,4},{6,5},{7,6},{8,11},{9,8},{10,9... | collective-permute-start | bytes 3145736 | tf_op jit(solution)/shard_map/ppermute | solution.py:659
  96.5 44.2 %collective-permute-start.19 = (bf16[256,1024]{1,0:T(8,128)(2,1)}, bf16[256,1024]{1,0:T(8,128)(2,1)}, u32[]{:S(2)}, u32[]{:S(2)}) collective-permute-start(bf16[256,1024]{1,0:T(8,128)(2,1)} %get-tuple-element.48), channel_id=1, source_target_pairs={{0,3},{1,0},{2,1},{3,2},{4,7},{5,4},{6,5},{7,6},{8,11},{9,8},{10,9... | collective-permute-start | bytes 1572872 | tf_op jit(solution)/shard_map/ppermute | solution.py:659
  140.6 22.6 %collective-permute-start.17 = (bf16[256,1024]{1,0:T(8,128)(2,1)}, bf16[256,1024]{1,0:T(8,128)(2,1)}, u32[]{:S(2)}, u32[]{:S(2)}) collective-permute-start(bf16[256,1024]{1,0:T(8,128)(2,1)} %get-tuple-element.48), channel_id=1, source_target_pairs={{0,1},{1,2},{2,3},{3,0},{4,5},{5,6},{6,7},{7,4},{8,9},{9,10},{10,1... | collective-permute-start | bytes 1572872 | tf_op jit(solution)/shard_map/ppermute | solution.py:659
  142.2 21.0 %collective-permute-start.18 = (bf16[256,1024]{1,0:T(8,128)(2,1)}, bf16[256,1024]{1,0:T(8,128)(2,1)}, u32[]{:S(2)}, u32[]{:S(2)}) collective-permute-start(bf16[256,1024]{1,0:T(8,128)(2,1)} %get-tuple-element.49), channel_id=1, source_target_pairs={{0,3},{1,0},{2,1},{3,2},{4,7},{5,4},{6,5},{7,6},{8,11},{9,8},{10,9... | collective-permute-start | bytes 1572872 | tf_op jit(solution)/shard_map/ppermute | solution.py:659
  146.8 23.0 %all-to-all-start.1 = ((bf16[8,64,128]{2,1,0:T(8,128)(2,1)}), bf16[8,64,128]{2,1,0:T(8,128)(2,1)S(1)}, u32[]{:S(2)}, u32[]{:S(2)}) async-start(bf16[8,64,128]{2,1,0:T(8,128)(2,1)} %enter_states.1), calls=%async_computation.1 | async-start | bytes 262144 | tf_op jit(solution)/shard_map/all_to_all | solution.py:671
  151.6 16.4 %collective-permute-start.20 = (bf16[256,1024]{1,0:T(8,128)(2,1)}, bf16[256,1024]{1,0:T(8,128)(2,1)S(1)}, u32[]{:S(2)}, u32[]{:S(2)}) collective-permute-start(bf16[256,1024]{1,0:T(8,128)(2,1)} %collective-permute-done.16.before_0), channel_id=1, source_target_pairs={{0,1},{1,2},{2,3},{3,0},{4,5},{5,6},{6,7},{7,4},{8,9},{9,10},{10,1... | collective-permute-start | bytes 1572872 | tf_op jit(solution)/shard_map/ppermute | solution.py:659
  152.0 16.0 %collective-permute-start.21 = (bf16[256,1024]{1,0:T(8,128)(2,1)}, bf16[256,1024]{1,0:T(8,128)(2,1)S(1)}, u32[]{:S(2)}, u32[]{:S(2)}) collective-permute-start(bf16[256,1024]{1,0:T(8,128)(2,1)} %collective-permute-done.19.after_1), channel_id=1, source_target_pairs={{0,3},{1,0},{2,1},{3,2},{4,7},{5,4},{6,5},{7,6},{8,11},{9,8},{10,9... | collective-permute-start | bytes 1572872 | tf_op jit(solution)/shard_map/ppermute | solution.py:659
  169.8 61.8 %all-to-all-start.3 = ((bf16[64,8,2048]{2,1,0:T(8,128)(2,1)}), bf16[64,8,2048]{2,1,0:T(8,128)(2,1)S(1)}, u32[]{:S(2)}, u32[]{:S(2)}) async-start(bf16[64,8,2048]{2,1,0:T(8,128)(2,1)} %bitcast.17), calls=%async_computation.3 | async-start | bytes 4194304 | tf_op jit(solution)/shard_map/all_to_all | solution.py:671
  189.2 25.0 %collective-permute-start.9 = (bf16[128,2048]{1,0:T(8,128)(2,1)}, bf16[128,2048]{1,0:T(8,128)(2,1)S(1)}, u32[]{:S(2)}, u32[]{:S(2)}) collective-permute-start(bf16[128,2048]{1,0:T(8,128)(2,1)} %get-tuple-element.43), channel_id=1, source_target_pairs={{0,3},{1,0},{2,1},{3,2},{4,7},{5,4},{6,5},{7,6},{8,11},{9,8},{10,9... | collective-permute-start | bytes 1572872 | tf_op jit(solution)/shard_map/ppermute | solution.py:659
  191.2 23.0 %collective-permute-start.8 = (bf16[128,2048]{1,0:T(8,128)(2,1)}, bf16[128,2048]{1,0:T(8,128)(2,1)S(1)}, u32[]{:S(2)}, u32[]{:S(2)}) collective-permute-start(bf16[128,2048]{1,0:T(8,128)(2,1)} %get-tuple-element.42), channel_id=1, source_target_pairs={{0,2},{1,3},{2,0},{3,1},{4,6},{5,7},{6,4},{7,5},{8,10},{9,11},{10,... | collective-permute-start | bytes 1572872 | tf_op jit(solution)/shard_map/ppermute | solution.py:659
  191.2 26.3 %collective-permute-start.7 = (bf16[128,2048]{1,0:T(8,128)(2,1)}, bf16[128,2048]{1,0:T(8,128)(2,1)S(1)}, u32[]{:S(2)}, u32[]{:S(2)}) collective-permute-start(bf16[128,2048]{1,0:T(8,128)(2,1)} %get-tuple-element.41), channel_id=1, source_target_pairs={{0,1},{1,2},{2,3},{3,0},{4,5},{5,6},{6,7},{7,4},{8,9},{9,10},{10,1... | collective-permute-start | bytes 1572872 | tf_op jit(solution)/shard_map/ppermute | solution.py:659
  (6 other events, 26.9 us)
